TPU v7x, 256 devices: a whole 4x4x8 slice. The times are simulated.
256 devices in a mesh: ep: 16 (over y, x), tp: 16 (over z, core).
Axes of the slice: x: 4, y: 4, z: 8, core: 2. Of those that a mesh axis runs over, the one named last changes fastest.
Arguments:
- tokens: bfloat16 [16384, 2048], P('ep', 'tp'), may hold values from -48 to 48
- pre_gain: bfloat16 [2048], P('tp'), may hold values from 0.099609375 to 1.8984375
- route_ids: int32 [16384, 2], P('ep'), may hold values from 0 to 15, all different within a row; in each aligned block of 1024 rows (0 to 1023, 1024 to 2047, ...) at most 144 rows name the same one
- route_weights: float32 [16384, 2], P('ep'), may hold values from 0.1 to 1
- gate_weight: bfloat16 [16, 2048, 7168], P('ep', None, 'tp'), may hold values from -0.125 to 0.125
- up_weight: bfloat16 [16, 2048, 7168], P('ep', None, 'tp'), may hold values from -0.125 to 0.125
- down_weight: bfloat16 [16, 7168, 2048], P('ep', 'tp')
- post_gain: bfloat16 [2048], P('tp'), may hold values from 0.099609375 to 1.8984375
Outputs:
- mixed: bfloat16 [16384, 2048], P('ep', 'tp')
Inputs may be any that keep to these rules, and one draw needn't show every extreme that they name: `route_ids`: each row names 2 different experts; among the rows of one index of ep no expert is named more than 144 times, a bound that some block reaches.
All inputs are finite; a program needn't handle non-finite values.
Results may differ from a plain program's by a relative error of at most 0.02.
Values may be sent and summed in bfloat16 or wider, within the bound.
No kernel may reach another device: no remote copies, remote signals or barrier semaphores. Data moves between devices by JAX's collectives and lax.ppermute only.
A program may use at most 128 MiB of HBM per device.

v0:
```python
import jax
import jax.numpy as jnp
from jax import lax
from jax.experimental import pallas as pl
from jax.experimental.pallas import tpu as pltpu
from jax.sharding import Mesh, PartitionSpec as P

D = 2048
EPS = 1e-06
LANES = 128
CHUNKS = 2
EXTRA = 16
MIB = 1024 * 1024
UP_VMEM = 26 * MIB
DOWN_VMEM = 12 * MIB
NORM_UNROLL = 1
SMALL_VMEM = 12 * MIB
F32 = jnp.float32
BF16 = jnp.bfloat16


def route_kernel(ids_ref, weight_ref, tok_ref, out_ref, pos_ref, pick_scr):
    rows = tok_ref.shape[0]
    half = out_ref.shape[0] // 32
    block = LANES
    blocks = rows // block
    lane = lax.broadcasted_iota(jnp.int32, (block, LANES), 1).astype(F32)
    lower = (
        (
            lax.broadcasted_iota(jnp.int32, (block, block), 0)
            > lax.broadcasted_iota(jnp.int32, (block, block), 1)
        )
        .astype(F32)
        .astype(BF16)
    )
    before = jnp.zeros((1, LANES), F32)
    fill = jnp.zeros((4, block), F32)
    for b in range(blocks):
        span = slice(b * block, (b + 1) * block)
        given = jnp.concatenate(
            [ids_ref[:, span].astype(F32), weight_ref[:, span], fill], axis=0
        )
        turned = jnp.concatenate([given] * (LANES // 8), axis=0).T
        is_first = lane == turned[:, 0:1]
        is_second = lane == turned[:, 1:2]
        named = jnp.where(is_first | is_second, 1.0, 0.0)
        rank = jnp.dot(lower, named.astype(BF16), preferred_element_type=F32) + before
        before = before + jnp.sum(named, axis=0, keepdims=True)
        place = rank + lane * half + jnp.where(rank >= half, 15.0 * half, 0.0)
        place0 = jnp.sum(jnp.where(is_first, place, 0.0), axis=1, keepdims=True)
        place1 = jnp.sum(jnp.where(is_second, place, 0.0), axis=1, keepdims=True)
        both = jnp.where(lane == 0, place0, jnp.where(lane == 1, place1, turned))
        pos_ref[span, :] = both
        pick_scr[:, span] = both.T[0:8, :]
    step = 2 * half
    row0 = pick_scr[0:1, :]
    row1 = pick_scr[1:2, :]
    base = lax.broadcasted_iota(jnp.int32, (step, rows), 0).astype(F32)
    tok = tok_ref[...]

    def one(b, carry):
        start = pl.multiple_of(b * step, step)
        at = base + start.astype(F32)
        pick = jnp.where((at == row0) | (at == row1), 1.0, 0.0).astype(BF16)
        out_ref[pl.ds(start, step), :] = jnp.dot(pick, tok, preferred_element_type=F32).astype(BF16)
        return carry

    lax.fori_loop(0, out_ref.shape[0] // step, one, 0, unroll=2)


def combine_kernel(ret_ref, pos_ref, out_ref, square_ref):
    rows = pos_ref.shape[0]
    slots = ret_ref.shape[0]
    block = LANES
    base = lax.broadcasted_iota(jnp.int32, (block, slots), 1).astype(F32)

    def one(b, carry):
        span = pl.ds(pl.multiple_of(b * block, block), block)
        given = pos_ref[span, :]
        total = None
        for k in range(2):
            pick = jnp.where(base == given[:, k : k + 1], 1.0, 0.0).astype(BF16)
            part = jnp.dot(pick, ret_ref[...], preferred_element_type=F32) * given[:, k + 2 : k + 3]
            total = part if total is None else total + part
        out_ref[span, :] = total
        squares = jnp.sum(total * total, axis=1, keepdims=True)
        row = jnp.broadcast_to(squares, (block, LANES)).T[0:1, :]
        square_ref[:, pl.ds(b, 1), :] = jnp.broadcast_to(row[None], (square_ref.shape[0], 1, LANES))
        return carry

    lax.fori_loop(0, rows // block, one, 0, unroll=2)


def finish_kernel(comb_ref, squares_ref, gain_ref, out_ref):
    totals = jnp.sum(squares_ref[...], axis=0)
    scale = lax.rsqrt(totals / D + EPS)
    gain = gain_ref[...].astype(F32)
    for b in range(scale.shape[0]):
        span = slice(b * LANES, (b + 1) * LANES)
        per_row = jnp.broadcast_to(scale[b : b + 1, :], (LANES, LANES)).T
        out_ref[span, :] = (comb_ref[span, :] * per_row * gain).astype(BF16)


NEAR = (0, -1, 1, -2, 2, -3, 3, -4)
FIRST = (7, 5, 6)
LATER = (3, 4, 1, 2, 0)


def near(z_ref):
    z = z_ref[0]
    return [pl.multiple_of(lax.rem(z + (off + 8), 8) * 256, 256) for off in NEAR]


def load_down(own, other, scr, sem):
    hidden = scr.shape[0] // 2
    for n, src in enumerate((own, other)):
        pltpu.make_async_copy(
            src.at[pl.ds(2 * hidden, hidden), :], scr.at[pl.ds(n * hidden, hidden), :], sem
        ).start()


def put_down(h_ref, scr, order, outs):
    step = h_ref.shape[0] // 2
    outs = list(outs)

    def tile(r, carry):
        span = pl.ds(pl.multiple_of(r * step, step), step)
        for j, out in outs:
            part = jnp.dot(
                h_ref[span, :], scr[:, pl.ds(order[j], 256)], preferred_element_type=F32
            ).astype(BF16)
            out[0, span, :] = part[:, :LANES]
            out[1, span, :] = part[:, LANES:]
        return carry

    lax.fori_loop(0, 2, tile, 0)


def up_kernel(
    z_ref, x0, p1, m1, p2, m2, p3, m3, x4, own, other, h_ref, o4, op3, om3,
    piece_scr, x_scr, in_scr, down_scr, sems,
):
    rows = o4.shape[1]
    hidden = h_ref.shape[1] // 2
    order = near(z_ref)
    for j, src in enumerate((x0, p1, m1, p2, m2, p3, m3, x4)):
        pltpu.make_async_copy(src, piece_scr.at[j], sems.at[0]).start()
    for n, (src, at) in enumerate(((own, 0), (other, 0), (own, hidden), (other, hidden))):
        pltpu.make_async_copy(
            src.at[pl.ds(at, hidden), :], in_scr.at[pl.ds(n * hidden, hidden), :], sems.at[1]
        ).start()
    load_down(own, other, down_scr, sems.at[2])
    pltpu.make_async_copy(piece_scr, piece_scr, sems.at[0]).wait()
    tile = 32
    gains = [
        [piece_scr[j, c, pl.ds(rows, EXTRA), :].astype(F32)[0:1, :] for c in range(2)]
        for j in range(8)
    ]

    def norm_tile(t, carry):
        start = pl.multiple_of(t * tile, tile)
        acc = jnp.zeros((tile, LANES), F32)
        for j in range(8):
            for c in range(2):
                v = piece_scr[j, c, pl.ds(start, tile), :].astype(F32)
                acc = acc + v * v
        scale = lax.rsqrt(jnp.sum(acc, axis=1, keepdims=True) / D + EPS)
        for j in range(8):
            both = [
                (piece_scr[j, c, pl.ds(start, tile), :].astype(F32) * scale * gains[j][c]).astype(BF16)
                for c in range(2)
            ]
            x_scr[pl.ds(start, tile), pl.ds(order[j], 256)] = jnp.concatenate(both, axis=1)
        return carry

    lax.fori_loop(0, rows // tile, norm_tile, 0, unroll=NORM_UNROLL)
    pltpu.make_async_copy(in_scr, in_scr, sems.at[1]).wait()
    step = rows // 2

    def up_tile(r, carry):
        span = pl.ds(pl.multiple_of(r * step, step), step)
        both = lax.dot_general(
            x_scr[span, :], in_scr[...], (((1,), (1,)), ((), ())), preferred_element_type=F32
        )
        gate = both[:, : 2 * hidden]
        up = both[:, 2 * hidden :]
        h_ref[span, :] = (gate / (1.0 + jnp.exp(-gate)) * up).astype(BF16)
        return carry

    lax.fori_loop(0, 2, up_tile, 0)
    pltpu.make_async_copy(down_scr, down_scr, sems.at[2]).wait()
    put_down(h_ref, down_scr, order, zip(FIRST, (o4, op3, om3)))


def down_kernel(z_ref, h_ref, own, other, op2, om2, op1, om1, o0, down_scr, sem):
    load_down(own, other, down_scr, sem)
    pltpu.make_async_copy(down_scr, down_scr, sem).wait()
    put_down(h_ref, down_scr, near(z_ref), zip(LATER, (op2, om2, op1, om1, o0)))


def ffn(z, pieces, own, other):
    rows = pieces[0].shape[1] - EXTRA
    hidden = own.shape[0] // 3
    vm = pl.BlockSpec(memory_space=pltpu.VMEM)
    sm = pl.BlockSpec(memory_space=pltpu.SMEM)
    hbm = pl.BlockSpec(memory_space=pltpu.HBM)
    full = jax.ShapeDtypeStruct((2, rows, LANES), BF16)
    wide = 2 * rows * D * 2 * hidden
    h, o4, op3, om3 = pl.pallas_call(
        up_kernel,
        name="ffn_up",
        in_specs=[sm] + [hbm] * 10,
        out_specs=[vm] * 4,
        out_shape=[jax.ShapeDtypeStruct((rows, 2 * hidden), BF16)] + [full] * 3,
        scratch_shapes=[
            pltpu.VMEM((8, 2, rows + EXTRA, LANES), BF16),
            pltpu.VMEM((rows, D), BF16),
            pltpu.VMEM((4 * hidden, D), BF16),
            pltpu.VMEM((2 * hidden, D), BF16),
            pltpu.SemaphoreType.DMA((3,)),
        ],
        cost_estimate=pl.CostEstimate(
            flops=2 * wide + wide * 3 // 8,
            bytes_accessed=12 * D * hidden + 4 * rows * D,
            transcendentals=rows * hidden * 2,
        ),
        compiler_params=pltpu.CompilerParams(vmem_limit_bytes=UP_VMEM),
    )(z, *pieces, own, other)
    op2, om2, op1, om1, o0 = pl.pallas_call(
        down_kernel,
        name="ffn_down",
        in_specs=[sm, vm, hbm, hbm],
        out_specs=[vm] * 5,
        out_shape=[full] * 5,
        scratch_shapes=[pltpu.VMEM((2 * hidden, D), BF16), pltpu.SemaphoreType.DMA],
        cost_estimate=pl.CostEstimate(
            flops=wide * 5 // 8,
            bytes_accessed=4 * D * hidden + 2 * rows * D,
            transcendentals=0,
        ),
        compiler_params=pltpu.CompilerParams(vmem_limit_bytes=DOWN_VMEM),
    )(z, h, own, other)
    return o0, (om1, om2, om3), (op1, op2, op3), o4


def join_kernel(*refs):
    *given, out, sems = refs
    size = given[0].shape[0]
    copies = [
        pltpu.make_async_copy(src, out.at[pl.ds(n * size, size), :], sems.at[n])
        for n, src in enumerate(given)
    ]
    for copy in copies:
        copy.start()
    for copy in copies:
        copy.wait()


def join(parts):
    rows, columns = parts[0].shape
    hbm = pl.BlockSpec(memory_space=pltpu.HBM)
    return pl.pallas_call(
        join_kernel,
        name="join",
        in_specs=[hbm] * len(parts),
        out_specs=hbm,
        out_shape=jax.ShapeDtypeStruct((len(parts) * rows, columns), BF16),
        scratch_shapes=[pltpu.SemaphoreType.DMA((len(parts),))],
        compiler_params=pltpu.CompilerParams(vmem_limit_bytes=60 * MIB),
    )(*parts)


def turn(value, axis, by):
    count = lax.axis_size(axis)
    return lax.ppermute(value, axis, [(i, (i + by) % count) for i in range(count)])


def add(*parts):
    total = parts[0].astype(F32)
    for part in parts[1:]:
        total = total + part.astype(F32)
    return total.astype(BF16)


def gather_ring(own, far):
    ahead = [own]
    back = [own]
    for i in range(4):
        if i < 3 or far == 1:
            ahead.append(turn(ahead[-1], "z", 1))
        if i < 3 or far == -1:
            back.append(turn(back[-1], "z", -1))
    last = ahead[4] if far == 1 else back[4]
    return [own, ahead[1], back[1], ahead[2], back[2], ahead[3], back[3], last]


def scatter_ring(own, plus, minus, last, far):
    ends = []
    for by, parts in ((1, plus), (-1, minus)):
        moving = None
        for part in ((last,) if far == by else ()) + parts[::-1]:
            part = part if moving is None else add(part, moving)
            moving = turn(part, "z", by)
        ends.append(moving)
    return add(own, *ends)


def layer(
    tokens, pre_gain, route_ids, route_weights, gate_weight, up_weight, down_weight, post_gain
):
    tok_rows = tokens.shape[0]
    groups = lax.axis_size("y") * lax.axis_size("x")
    slots = 9 * tok_rows * route_ids.shape[1] // (8 * groups)
    half = slots // 2
    total = groups * slots

    own = join([gate_weight[0].T, up_weight[0].T, down_weight[0]])
    other = turn(own, "c", 1)
    gain_rows = jnp.broadcast_to(pre_gain[None, :], (EXTRA, LANES))
    gain_other = turn(gain_rows, "c", 1)
    c = lax.axis_index("c")
    gain_both = jnp.where(
        c == 0, jnp.stack([gain_rows, gain_other]), jnp.stack([gain_other, gain_rows])
    )

    outgoing, places = pl.pallas_call(
        route_kernel,
        name="route",
        compiler_params=pltpu.CompilerParams(vmem_limit_bytes=SMALL_VMEM),
        out_shape=[
            jax.ShapeDtypeStruct((total, LANES), BF16),
            jax.ShapeDtypeStruct((tok_rows, LANES), F32),
        ],
        scratch_shapes=[pltpu.VMEM((8, tok_rows), F32)],
    )(route_ids.T, route_weights.T, tokens)
    exchange = ("c", "y", "x")
    arrived = lax.all_to_all(
        outgoing.reshape(2 * groups, half, LANES), exchange, 0, 0, tiled=True
    ).reshape(2, groups * half, LANES)
    z = lax.axis_index("z").astype(jnp.int32).reshape(1)
    rows = groups * half // CHUNKS
    results = []
    for i in range(CHUNKS):
        piece = jnp.concatenate([arrived[:, i * rows : (i + 1) * rows], gain_both], axis=1)
        far = 1 if i % 2 == 0 else -1
        results.append(scatter_ring(*ffn(z, gather_ring(piece, far), own, other), far))
    result = jnp.concatenate(results, axis=1)
    returned = lax.all_to_all(
        result.reshape(2 * groups, half, LANES), exchange, 0, 0, tiled=True
    ).reshape(total, LANES)
    everyone = lax.axis_size("z") * lax.axis_size("c")
    combined, squares = pl.pallas_call(
        combine_kernel,
        name="combine",
        compiler_params=pltpu.CompilerParams(vmem_limit_bytes=SMALL_VMEM),
        out_shape=[
            jax.ShapeDtypeStruct((tok_rows, LANES), F32),
            jax.ShapeDtypeStruct((everyone, tok_rows // LANES, LANES), F32),
        ],
    )(returned, places)
    gathered = lax.all_to_all(squares, ("z", "c"), 0, 0, tiled=True)
    return pl.pallas_call(
        finish_kernel,
        name="finish",
        compiler_params=pltpu.CompilerParams(vmem_limit_bytes=SMALL_VMEM),
        out_shape=jax.ShapeDtypeStruct((tok_rows, LANES), BF16),
    )(combined, gathered, post_gain.reshape(1, LANES))


def solution(mesh):
    names = ("y", "x", "z", "c")
    fine = Mesh(mesh.devices.reshape(4, 4, 8, 2), names)
    ep, tp = ("y", "x"), ("z", "c")
    placed = (
        P(ep, tp),
        P(tp),
        P(ep, None),
        P(ep, None),
        P(ep, None, tp),
        P(ep, None, tp),
        P(ep, tp, None),
        P(tp),
    )
    return jax.shard_map(layer, mesh=fine, in_specs=placed, out_specs=P(ep, tp), check_vma=False)
```

profile of v0, /device:TPU:1, one launch (start us, length us, event | category | flops | bytes accessed | tf_op | source)
XLA Modules:
  0.0 352.8 jit_solution(12549437901287288008)
XLA Ops:
  0.0 167.9 %join.1.own = bf16[1344,2048]{1,0:T(8,128)(2,1)} custom-call(bf16[448,2048]{1,0:T(8,128)(2,1)} %bitcast.22, bf16[448,2048]{1,0:T(8,128)(2,1)} %bitcast.23, bf16[448,2048]{1,0:T(8,128)(2,1)} %bitcast.24), custom_call_target="tpu_custom_call" | custom-call | tf_op jit(solution)/shard_map/join/pallas_call | solution.py:262
  167.9 3.3 collective-permute-start.8
  171.2 6.1 %route.1 = (bf16[2304,128]{1,0:T(8,128)(2,1)}, f32[1024,128]{1,0:T(8,128)S(1)}) custom-call(s32[2,1024]{1,0:T(2,128)S(1)} %bitcast.17, f32[2,1024]{1,0:T(2,128)S(1)} %bitcast.18, bf16[1024,128]{1,0:T(8,128)(2,1)S(1)} %copy-done.1), custom_call_target="tpu_custom_call" | custom-call | tf_op jit(solution)/shard_map/route/pallas_call | solution.py:326
  177.3 5.5 %all-to-all-start = ((bf16[32,72,128]{2,1,0:T(8,128)(2,1)}), bf16[32,72,128]{2,1,0:T(8,128)(2,1)S(1)}, u32[]{:S(2)}, u32[]{:S(2)}) async-start(bf16[32,72,128]{2,1,0:T(8,128)(2,1)} %bitcast.3), calls=%async_computation | async-start | bytes 1179648 | tf_op jit(solution)/shard_map/all_to_all | solution.py:337
  184.1 10.4 %all-to-all-done = bf16[32,72,128]{2,1,0:T(8,128)(2,1)S(1)} async-done(((bf16[32,72,128]{2,1,0:T(8,128)(2,1)}), bf16[32,72,128]{2,1,0:T(8,128)(2,1)S(1)}, u32[]{:S(2)}, u32[]{:S(2)}) %all-to-all-start) | async-done | bytes 589856 | tf_op jit(solution)/shard_map/all_to_all | solution.py:337
  196.3 4.0 %collective-permute-start.17 = (bf16[2,592,128]{2,1,0:T(8,128)(2,1)S(1)}, bf16[2,592,128]{2,1,0:T(8,128)(2,1)S(1)}, u32[]{:S(2)}, u32[]{:S(2)}) collective-permute-start(bf16[2,592,128]{2,1,0:T(8,128)(2,1)S(1)} %get-tuple-element.52.x0), channel_id=1, source_target_pairs={{0,14},{2,0},{4,2},{6,4},{8,6},{10,8},{12,10},{14,12},{1,15},{3,1}... | collective-permute-start | bytes 909320 | tf_op jit(solution)/shard_map/ppermute | solution.py:275
  201.7 4.9 %collective-permute-done.1.p1 = bf16[2,592,128]{2,1,0:T(8,128)(2,1)S(1)} collective-permute-done((bf16[2,592,128]{2,1,0:T(8,128)(2,1)S(1)}, bf16[2,592,128]{2,1,0:T(8,128)(2,1)S(1)}, u32[]{:S(2)}, u32[]{:S(2)}) %collective-permute-start.1) | collective-permute-done | bytes 303136 | tf_op jit(solution)/shard_map/ppermute | solution.py:275
  206.7 2.7 collective-permute-start.19
  209.4 2.9 collective-permute-done.2.m1
  212.2 3.4 collective-permute-start.4
  215.7 5.7 %collective-permute-done.16.p1 = bf16[2,592,128]{2,1,0:T(8,128)(2,1)S(1)} collective-permute-done((bf16[2,592,128]{2,1,0:T(8,128)(2,1)S(1)}, bf16[2,592,128]{2,1,0:T(8,128)(2,1)S(1)}, u32[]{:S(2)}, u32[]{:S(2)}) %collective-permute-start.16) | collective-permute-done | bytes 303136 | tf_op jit(solution)/shard_map/ppermute | solution.py:275
  221.4 2.7 collective-permute-start.21
  225.2 3.5 collective-permute-start.6
  228.8 5.6 %collective-permute-done.18.p2 = bf16[2,592,128]{2,1,0:T(8,128)(2,1)S(1)} collective-permute-done((bf16[2,592,128]{2,1,0:T(8,128)(2,1)S(1)}, bf16[2,592,128]{2,1,0:T(8,128)(2,1)S(1)}, u32[]{:S(2)}, u32[]{:S(2)}) %collective-permute-start.18) | collective-permute-done | bytes 303136 | tf_op jit(solution)/shard_map/ppermute | solution.py:275
  234.4 2.7 collective-permute-start.22
  237.1 3.9 %collective-permute-done.7.x4 = bf16[2,592,128]{2,1,0:T(8,128)(2,1)} collective-permute-done((bf16[2,592,128]{2,1,0:T(8,128)(2,1)}, bf16[2,592,128]{2,1,0:T(8,128)(2,1)}, u32[]{:S(2)}, u32[]{:S(2)}) %collective-permute-start.7) | collective-permute-done | bytes 303136 | tf_op jit(solution)/shard_map/ppermute | solution.py:275
  243.6 9.9 %ffn_up.2 = (bf16[576,896]{1,0:T(8,128)(2,1)S(1)}, bf16[2,576,128]{2,1,0:T(8,128)(2,1)S(1)}, bf16[2,576,128]{2,1,0:T(8,128)(2,1)S(1)}, bf16[2,576,128]{2,1,0:T(8,128)(2,1)S(1)}) custom-call(s32[1]{0:T(128)} %bitcast.z_ref, bf16[2,592,128]{2,1,0:T(8,128)(2,1)S(1)} %get-tuple-element.51.x0, bf16[2,592,128]{2,1,0:T(8,128)(2,1)S(1)} %collective-permute-done.1.p1, ...), custom_call_target="tpu_custom_call" | custom-call | flops 5020581888 | bytes 15728640 | tf_op jit(solution)/shard_map/ffn_up/pallas_call | solution.py:209
  256.2 9.3 %ffn_up.3 = (bf16[576,896]{1,0:T(8,128)(2,1)S(1)}, bf16[2,576,128]{2,1,0:T(8,128)(2,1)S(1)}, bf16[2,576,128]{2,1,0:T(8,128)(2,1)S(1)}, bf16[2,576,128]{2,1,0:T(8,128)(2,1)S(1)}) custom-call(s32[1]{0:T(128)} %bitcast.z_ref, bf16[2,592,128]{2,1,0:T(8,128)(2,1)S(1)} %get-tuple-element.52.x0, bf16[2,592,128]{2,1,0:T(8,128)(2,1)S(1)} %collective-permute-done.16.p1, ...), custom_call_target="tpu_custom_call" | custom-call | flops 5020581888 | bytes 15728640 | tf_op jit(solution)/shard_map/ffn_up/pallas_call | solution.py:209
  268.2 3.5 ffn_down.2
  271.8 3.5 %ffn_down.3 = (bf16[2,576,128]{2,1,0:T(8,128)(2,1)S(1)}, bf16[2,576,128]{2,1,0:T(8,128)(2,1)S(1)}, bf16[2,576,128]{2,1,0:T(8,128)(2,1)S(1)}, bf16[2,576,128]{2,1,0:T(8,128)(2,1)S(1)}, bf16[2,576,128]{2,1,0:T(8,128)(2,1)S(1)}) custom-call(s32[1]{0:T(128)} %bitcast.z_ref, bf16[576,896]{1,0:T(8,128)(2,1)S(1)} %get-tuple-element.37.h_ref, ...), custom_call_target="tpu_custom_call" | custom-call | flops 1321205760 | bytes 6029312 | tf_op jit(solution)/shard_map/ffn_down/pallas_call | solution.py:229
  275.8 2.7 collective-permute-start.14
  278.8 2.7 collective-permute-start.27
  282.8 2.7 collective-permute-start.15
  285.6 3.1 collective-permute-start.28
  288.6 4.2 %collective-permute-done.11 = bf16[2,576,128]{2,1,0:T(8,128)(2,1)S(1)} collective-permute-done((bf16[2,576,128]{2,1,0:T(8,128)(2,1)S(1)}, bf16[2,576,128]{2,1,0:T(8,128)(2,1)S(1)}, u32[]{:S(2)}, u32[]{:S(2)}) %collective-permute-start.11) | collective-permute-done | bytes 294944 | tf_op jit(solution)/shard_map/ppermute | solution.py:275
  293.2 5.4 %collective-permute-done.28 = bf16[2,576,128]{2,1,0:T(8,128)(2,1)S(1)} collective-permute-done((bf16[2,576,128]{2,1,0:T(8,128)(2,1)S(1)}, bf16[2,576,128]{2,1,0:T(8,128)(2,1)S(1)}, u32[]{:S(2)}, u32[]{:S(2)}) %collective-permute-start.28) | collective-permute-done | bytes 294944 | tf_op jit(solution)/shard_map/ppermute | solution.py:275
  298.7 3.5 collective-permute-start.29
  302.8 3.0 collective-permute-done.25
  305.9 2.9 collective-permute-done.29
  308.9 23.6 %all_to_all.15 = bf16[32,72,128]{2,1,0:T(8,128)(2,1)S(1)} all-to-all(bf16[32,72,128]{2,1,0:T(8,128)(2,1)S(1)} %bitcast.21), channel_id=1, replica_groups=mesh['y'=4,'x'=4,'z'=8,'c'=2] {'c','y','x'}, dimensions={0} | all-to-all | bytes 1179648 | tf_op jit(solution)/shard_map/all_to_all | solution.py:348
  332.5 3.8 %combine.1 = (f32[1024,128]{1,0:T(8,128)S(1)}, f32[16,8,128]{2,1,0:T(8,128)S(1)}) custom-call(bf16[2304,128]{1,0:T(8,128)(2,1)S(1)} %bitcast.16, f32[1024,128]{1,0:T(8,128)S(1)} %get-tuple-element.46.pos_ref), custom_call_target="tpu_custom_call" | custom-call | tf_op jit(solution)/shard_map/combine/pallas_call | solution.py:352
  336.3 15.5 %all_to_all.16.squares_ref = f32[16,8,128]{2,1,0:T(8,128)S(1)} all-to-all(f32[16,8,128]{2,1,0:T(8,128)S(1)} %get-tuple-element.48), channel_id=1, replica_groups=mesh['y'=4,'x'=4,'z'=8,'c'=2] {'z','c'}, dimensions={0} | all-to-all | bytes 131072 | tf_op jit(solution)/shard_map/all_to_all | solution.py:361
  (70 shorter events, 17.8 us)
Async XLA Ops:
  0.0 182.8 %copy-start.5 = (bf16[128]{0:T(256)(128)(2,1)S(1)}, bf16[128]{0:T(256)(128)(2,1)}, u32[]{:S(2)}) copy-start(bf16[128]{0:T(256)(128)(2,1)} %param.9) | copy-start | bytes 772
  167.9 73.1 %collective-permute-start.8 = (bf16[1344,2048]{1,0:T(8,128)(2,1)}, bf16[1344,2048]{1,0:T(8,128)(2,1)}, u32[]{:S(2)}, u32[]{:S(2)}) collective-permute-start(bf16[1344,2048]{1,0:T(8,128)(2,1)} %join.1.own), channel_id=1, source_target_pairs={{0,1},{1,0},{2,3},{3,2},{4,5},{5,4},{6,7},{7,6},{8,9},{9,8},{10,11... | collective-permute-start | bytes 16515080 | tf_op jit(solution)/shard_map/ppermute | solution.py:275
  177.3 17.2 %all-to-all-start = ((bf16[32,72,128]{2,1,0:T(8,128)(2,1)}), bf16[32,72,128]{2,1,0:T(8,128)(2,1)S(1)}, u32[]{:S(2)}, u32[]{:S(2)}) async-start(bf16[32,72,128]{2,1,0:T(8,128)(2,1)} %bitcast.3), calls=%async_computation | async-start | bytes 1179648 | tf_op jit(solution)/shard_map/all_to_all | solution.py:337
  182.8 1.3 collective-permute-start
  194.6 12.1 %collective-permute-start.1 = (bf16[2,592,128]{2,1,0:T(8,128)(2,1)S(1)}, bf16[2,592,128]{2,1,0:T(8,128)(2,1)S(1)}, u32[]{:S(2)}, u32[]{:S(2)}) collective-permute-start(bf16[2,592,128]{2,1,0:T(8,128)(2,1)S(1)} %get-tuple-element.51.x0), channel_id=1, source_target_pairs={{0,2},{2,4},{4,6},{6,8},{8,10},{10,12},{12,14},{14,0},{1,3},{3,5},... | collective-permute-start | bytes 909320 | tf_op jit(solution)/shard_map/ppermute | solution.py:275
  196.3 10.4 %collective-permute-start.17 = (bf16[2,592,128]{2,1,0:T(8,128)(2,1)S(1)}, bf16[2,592,128]{2,1,0:T(8,128)(2,1)S(1)}, u32[]{:S(2)}, u32[]{:S(2)}) collective-permute-start(bf16[2,592,128]{2,1,0:T(8,128)(2,1)S(1)} %get-tuple-element.52.x0), channel_id=1, source_target_pairs={{0,14},{2,0},{4,2},{6,4},{8,6},{10,8},{12,10},{14,12},{1,15},{3,1}... | collective-permute-start | bytes 909320 | tf_op jit(solution)/shard_map/ppermute | solution.py:275
  200.4 11.9 %collective-permute-start.2 = (bf16[2,592,128]{2,1,0:T(8,128)(2,1)S(1)}, bf16[2,592,128]{2,1,0:T(8,128)(2,1)S(1)}, u32[]{:S(2)}, u32[]{:S(2)}) collective-permute-start(bf16[2,592,128]{2,1,0:T(8,128)(2,1)S(1)} %get-tuple-element.51.x0), channel_id=1, source_target_pairs={{0,14},{2,0},{4,2},{6,4},{8,6},{10,8},{12,10},{14,12},{1,15},{3,1}... | collective-permute-start | bytes 909320 | tf_op jit(solution)/shard_map/ppermute | solution.py:275
  206.7 9.0 %collective-permute-start.3 = (bf16[2,592,128]{2,1,0:T(8,128)(2,1)S(1)}, bf16[2,592,128]{2,1,0:T(8,128)(2,1)S(1)}, u32[]{:S(2)}, u32[]{:S(2)}) collective-permute-start(bf16[2,592,128]{2,1,0:T(8,128)(2,1)S(1)} %collective-permute-done.1.p1), channel_id=1, source_target_pairs={{0,2},{2,4},{4,6},{6,8},{8,10},{10,12},{12,14},{14,0},{1,3},{3,5},... | collective-permute-start | bytes 909320 | tf_op jit(solution)/shard_map/ppermute | solution.py:275
  206.7 14.7 %collective-permute-start.16 = (bf16[2,592,128]{2,1,0:T(8,128)(2,1)S(1)}, bf16[2,592,128]{2,1,0:T(8,128)(2,1)S(1)}, u32[]{:S(2)}, u32[]{:S(2)}) collective-permute-start(bf16[2,592,128]{2,1,0:T(8,128)(2,1)S(1)} %get-tuple-element.52.x0), channel_id=1, source_target_pairs={{0,2},{2,4},{4,6},{6,8},{8,10},{10,12},{12,14},{14,0},{1,3},{3,5},... | collective-permute-start | bytes 909320 | tf_op jit(solution)/shard_map/ppermute | solution.py:275
  206.7 14.7 %collective-permute-start.19 = (bf16[2,592,128]{2,1,0:T(8,128)(2,1)S(1)}, bf16[2,592,128]{2,1,0:T(8,128)(2,1)S(1)}, u32[]{:S(2)}, u32[]{:S(2)}) collective-permute-start(bf16[2,592,128]{2,1,0:T(8,128)(2,1)S(1)} %collective-permute-done.17.m1), channel_id=1, source_target_pairs={{0,14},{2,0},{4,2},{6,4},{8,6},{10,8},{12,10},{14,12},{1,15},{3,1}... | collective-permute-start | bytes 909320 | tf_op jit(solution)/shard_map/ppermute | solution.py:275
  212.2 13.0 %collective-permute-start.4 = (bf16[2,592,128]{2,1,0:T(8,128)(2,1)S(1)}, bf16[2,592,128]{2,1,0:T(8,128)(2,1)}, u32[]{:S(2)}, u32[]{:S(2)}) collective-permute-start(bf16[2,592,128]{2,1,0:T(8,128)(2,1)S(1)} %collective-permute-done.2.m1), channel_id=1, source_target_pairs={{0,14},{2,0},{4,2},{6,4},{8,6},{10,8},{12,10},{14,12},{1,15},{3,1}... | collective-permute-start | bytes 909320 | tf_op jit(solution)/shard_map/ppermute | solution.py:275
  215.7 13.1 %collective-permute-start.5 = (bf16[2,592,128]{2,1,0:T(8,128)(2,1)S(1)}, bf16[2,592,128]{2,1,0:T(8,128)(2,1)}, u32[]{:S(2)}, u32[]{:S(2)}) collective-permute-start(bf16[2,592,128]{2,1,0:T(8,128)(2,1)S(1)} %collective-permute-done.3.p2), channel_id=1, source_target_pairs={{0,2},{2,4},{4,6},{6,8},{8,10},{10,12},{12,14},{14,0},{1,3},{3,5},... | collective-permute-start | bytes 909320 | tf_op jit(solution)/shard_map/ppermute | solution.py:275
  221.4 13.0 %collective-permute-start.18 = (bf16[2,592,128]{2,1,0:T(8,128)(2,1)S(1)}, bf16[2,592,128]{2,1,0:T(8,128)(2,1)S(1)}, u32[]{:S(2)}, u32[]{:S(2)}) collective-permute-start(bf16[2,592,128]{2,1,0:T(8,128)(2,1)S(1)} %collective-permute-done.16.p1), channel_id=1, source_target_pairs={{0,2},{2,4},{4,6},{6,8},{8,10},{10,12},{12,14},{14,0},{1,3},{3,5},... | collective-permute-start | bytes 909320 | tf_op jit(solution)/shard_map/ppermute | solution.py:275
  221.4 13.0 %collective-permute-start.21 = (bf16[2,592,128]{2,1,0:T(8,128)(2,1)S(1)}, bf16[2,592,128]{2,1,0:T(8,128)(2,1)S(1)}, u32[]{:S(2)}, u32[]{:S(2)}) collective-permute-start(bf16[2,592,128]{2,1,0:T(8,128)(2,1)S(1)} %collective-permute-done.19.m2), channel_id=1, source_target_pairs={{0,14},{2,0},{4,2},{6,4},{8,6},{10,8},{12,10},{14,12},{1,15},{3,1}... | collective-permute-start | bytes 909320 | tf_op jit(solution)/shard_map/ppermute | solution.py:275
  225.2 11.8 %collective-permute-start.6 = (bf16[2,592,128]{2,1,0:T(8,128)(2,1)}, bf16[2,592,128]{2,1,0:T(8,128)(2,1)}, u32[]{:S(2)}, u32[]{:S(2)}) collective-permute-start(bf16[2,592,128]{2,1,0:T(8,128)(2,1)} %collective-permute-done.4.m2), channel_id=1, source_target_pairs={{0,14},{2,0},{4,2},{6,4},{8,6},{10,8},{12,10},{14,12},{1,15},{3,1}... | collective-permute-start | bytes 909320 | tf_op jit(solution)/shard_map/ppermute | solution.py:275
  228.8 12.2 %collective-permute-start.7 = (bf16[2,592,128]{2,1,0:T(8,128)(2,1)}, bf16[2,592,128]{2,1,0:T(8,128)(2,1)}, u32[]{:S(2)}, u32[]{:S(2)}) collective-permute-start(bf16[2,592,128]{2,1,0:T(8,128)(2,1)} %collective-permute-done.5.p3), channel_id=1, source_target_pairs={{0,2},{2,4},{4,6},{6,8},{8,10},{10,12},{12,14},{14,0},{1,3},{3,5},... | collective-permute-start | bytes 909320 | tf_op jit(solution)/shard_map/ppermute | solution.py:275
  234.4 21.8 %collective-permute-start.20 = (bf16[2,592,128]{2,1,0:T(8,128)(2,1)S(1)}, bf16[2,592,128]{2,1,0:T(8,128)(2,1)S(1)}, u32[]{:S(2)}, u32[]{:S(2)}) collective-permute-start(bf16[2,592,128]{2,1,0:T(8,128)(2,1)S(1)} %collective-permute-done.18.p2), channel_id=1, source_target_pairs={{0,2},{2,4},{4,6},{6,8},{8,10},{10,12},{12,14},{14,0},{1,3},{3,5},... | collective-permute-start | bytes 909320 | tf_op jit(solution)/shard_map/ppermute | solution.py:275
  234.4 21.8 %collective-permute-start.22 = (bf16[2,592,128]{2,1,0:T(8,128)(2,1)S(1)}, bf16[2,592,128]{2,1,0:T(8,128)(2,1)S(1)}, u32[]{:S(2)}, u32[]{:S(2)}) collective-permute-start(bf16[2,592,128]{2,1,0:T(8,128)(2,1)S(1)} %collective-permute-done.21.m3), channel_id=1, source_target_pairs={{0,14},{2,0},{4,2},{6,4},{8,6},{10,8},{12,10},{14,12},{1,15},{3,1}... | collective-permute-start | bytes 909320 | tf_op jit(solution)/shard_map/ppermute | solution.py:275
  253.4 21.9 %collective-permute-start.9 = (bf16[2,576,128]{2,1,0:T(8,128)(2,1)S(1)}, bf16[2,576,128]{2,1,0:T(8,128)(2,1)S(1)}, u32[]{:S(2)}, u32[]{:S(2)}) collective-permute-start(bf16[2,576,128]{2,1,0:T(8,128)(2,1)S(1)} %get-tuple-element.33), channel_id=1, source_target_pairs={{0,2},{2,4},{4,6},{6,8},{8,10},{10,12},{12,14},{14,0},{1,3},{3,5},... | collective-permute-start | bytes 884744 | tf_op jit(solution)/shard_map/ppermute | solution.py:275
  253.5 22.2 %collective-permute-start.13 = (bf16[2,576,128]{2,1,0:T(8,128)(2,1)S(1)}, bf16[2,576,128]{2,1,0:T(8,128)(2,1)S(1)}, u32[]{:S(2)}, u32[]{:S(2)}) collective-permute-start(bf16[2,576,128]{2,1,0:T(8,128)(2,1)S(1)} %get-tuple-element.36), channel_id=1, source_target_pairs={{0,14},{2,0},{4,2},{6,4},{8,6},{10,8},{12,10},{14,12},{1,15},{3,1}... | collective-permute-start | bytes 884744 | tf_op jit(solution)/shard_map/ppermute | solution.py:275
  265.5 13.1 %collective-permute-start.23 = (bf16[2,576,128]{2,1,0:T(8,128)(2,1)S(1)}, bf16[2,576,128]{2,1,0:T(8,128)(2,1)S(1)}, u32[]{:S(2)}, u32[]{:S(2)}) collective-permute-start(bf16[2,576,128]{2,1,0:T(8,128)(2,1)S(1)} %get-tuple-element.41), channel_id=1, source_target_pairs={{0,2},{2,4},{4,6},{6,8},{8,10},{10,12},{12,14},{14,0},{1,3},{3,5},... | collective-permute-start | bytes 884744 | tf_op jit(solution)/shard_map/ppermute | solution.py:275
  265.6 13.2 %collective-permute-start.26 = (bf16[2,576,128]{2,1,0:T(8,128)(2,1)S(1)}, bf16[2,576,128]{2,1,0:T(8,128)(2,1)S(1)}, u32[]{:S(2)}, u32[]{:S(2)}) collective-permute-start(bf16[2,576,128]{2,1,0:T(8,128)(2,1)S(1)} %get-tuple-element.45), channel_id=1, source_target_pairs={{0,14},{2,0},{4,2},{6,4},{8,6},{10,8},{12,10},{14,12},{1,15},{3,1}... | collective-permute-start | bytes 884744 | tf_op jit(solution)/shard_map/ppermute | solution.py:275
  275.4 7.1 %collective-permute-start.10 = (bf16[2,576,128]{2,1,0:T(8,128)(2,1)S(1)}, bf16[2,576,128]{2,1,0:T(8,128)(2,1)S(1)}, u32[]{:S(2)}, u32[]{:S(2)}) collective-permute-start(bf16[2,576,128]{2,1,0:T(8,128)(2,1)S(1)} %add_convert_fusion.11), channel_id=1, source_target_pairs={{0,2},{2,4},{4,6},{6,8},{8,10},{10,12},{12,14},{14,0},{1,3},{3,5},... | collective-permute-start | bytes 884744 | tf_op jit(solution)/shard_map/ppermute | solution.py:275
  275.8 6.8 %collective-permute-start.14 = (bf16[2,576,128]{2,1,0:T(8,128)(2,1)S(1)}, bf16[2,576,128]{2,1,0:T(8,128)(2,1)S(1)}, u32[]{:S(2)}, u32[]{:S(2)}) collective-permute-start(bf16[2,576,128]{2,1,0:T(8,128)(2,1)S(1)} %add_convert_fusion.8), channel_id=1, source_target_pairs={{0,14},{2,0},{4,2},{6,4},{8,6},{10,8},{12,10},{14,12},{1,15},{3,1}... | collective-permute-start | bytes 884744 | tf_op jit(solution)/shard_map/ppermute | solution.py:275
  278.6 14.4 %collective-permute-start.24 = (bf16[2,576,128]{2,1,0:T(8,128)(2,1)S(1)}, bf16[2,576,128]{2,1,0:T(8,128)(2,1)S(1)}, u32[]{:S(2)}, u32[]{:S(2)}) collective-permute-start(bf16[2,576,128]{2,1,0:T(8,128)(2,1)S(1)} %add_convert_fusion.5), channel_id=1, source_target_pairs={{0,2},{2,4},{4,6},{6,8},{8,10},{10,12},{12,14},{14,0},{1,3},{3,5},... | collective-permute-start | bytes 884744 | tf_op jit(solution)/shard_map/ppermute | solution.py:275
  278.8 6.7 %collective-permute-start.27 = (bf16[2,576,128]{2,1,0:T(8,128)(2,1)S(1)}, bf16[2,576,128]{2,1,0:T(8,128)(2,1)S(1)}, u32[]{:S(2)}, u32[]{:S(2)}) collective-permute-start(bf16[2,576,128]{2,1,0:T(8,128)(2,1)S(1)} %add_convert_fusion.3), channel_id=1, source_target_pairs={{0,14},{2,0},{4,2},{6,4},{8,6},{10,8},{12,10},{14,12},{1,15},{3,1}... | collective-permute-start | bytes 884744 | tf_op jit(solution)/shard_map/ppermute | solution.py:275
  282.6 10.3 %collective-permute-start.11 = (bf16[2,576,128]{2,1,0:T(8,128)(2,1)S(1)}, bf16[2,576,128]{2,1,0:T(8,128)(2,1)S(1)}, u32[]{:S(2)}, u32[]{:S(2)}) collective-permute-start(bf16[2,576,128]{2,1,0:T(8,128)(2,1)S(1)} %add_convert_fusion.10), channel_id=1, source_target_pairs={{0,2},{2,4},{4,6},{6,8},{8,10},{10,12},{12,14},{14,0},{1,3},{3,5},... | collective-permute-start | bytes 884744 | tf_op jit(solution)/shard_map/ppermute | solution.py:275
  282.8 19.4 %collective-permute-start.15 = (bf16[2,576,128]{2,1,0:T(8,128)(2,1)S(1)}, bf16[2,576,128]{2,1,0:T(8,128)(2,1)S(1)}, u32[]{:S(2)}, u32[]{:S(2)}) collective-permute-start(bf16[2,576,128]{2,1,0:T(8,128)(2,1)S(1)} %add_convert_fusion.7), channel_id=1, source_target_pairs={{0,14},{2,0},{4,2},{6,4},{8,6},{10,8},{12,10},{14,12},{1,15},{3,1}... | collective-permute-start | bytes 884744 | tf_op jit(solution)/shard_map/ppermute | solution.py:275
  285.6 13.1 %collective-permute-start.28 = (bf16[2,576,128]{2,1,0:T(8,128)(2,1)S(1)}, bf16[2,576,128]{2,1,0:T(8,128)(2,1)S(1)}, u32[]{:S(2)}, u32[]{:S(2)}) collective-permute-start(bf16[2,576,128]{2,1,0:T(8,128)(2,1)S(1)} %add_convert_fusion.2), channel_id=1, source_target_pairs={{0,14},{2,0},{4,2},{6,4},{8,6},{10,8},{12,10},{14,12},{1,15},{3,1}... | collective-permute-start | bytes 884744 | tf_op jit(solution)/shard_map/ppermute | solution.py:275
  293.0 9.7 %collective-permute-start.12 = (bf16[2,576,128]{2,1,0:T(8,128)(2,1)S(1)}, bf16[2,576,128]{2,1,0:T(8,128)(2,1)S(1)}, u32[]{:S(2)}, u32[]{:S(2)}) collective-permute-start(bf16[2,576,128]{2,1,0:T(8,128)(2,1)S(1)} %add_convert_fusion.9), channel_id=1, source_target_pairs={{0,2},{2,4},{4,6},{6,8},{8,10},{10,12},{12,14},{14,0},{1,3},{3,5},... | collective-permute-start | bytes 884744 | tf_op jit(solution)/shard_map/ppermute | solution.py:275
  293.2 12.7 %collective-permute-start.25 = (bf16[2,576,128]{2,1,0:T(8,128)(2,1)S(1)}, bf16[2,576,128]{2,1,0:T(8,128)(2,1)S(1)}, u32[]{:S(2)}, u32[]{:S(2)}) collective-permute-start(bf16[2,576,128]{2,1,0:T(8,128)(2,1)S(1)} %add_convert_fusion.4), channel_id=1, source_target_pairs={{0,2},{2,4},{4,6},{6,8},{8,10},{10,12},{12,14},{14,0},{1,3},{3,5},... | collective-permute-start | bytes 884744 | tf_op jit(solution)/shard_map/ppermute | solution.py:275
  298.7 10.0 %collective-permute-start.29 = (bf16[2,576,128]{2,1,0:T(8,128)(2,1)S(1)}, bf16[2,576,128]{2,1,0:T(8,128)(2,1)S(1)}, u32[]{:S(2)}, u32[]{:S(2)}) collective-permute-start(bf16[2,576,128]{2,1,0:T(8,128)(2,1)S(1)} %add_convert_fusion.1), channel_id=1, source_target_pairs={{0,14},{2,0},{4,2},{6,4},{8,6},{10,8},{12,10},{14,12},{1,15},{3,1}... | collective-permute-start | bytes 884744 | tf_op jit(solution)/shard_map/ppermute | solution.py:275
  (5 other events, 559.1 us)
where the time goes:
time: 353 us
  Pallas kernels  205 us (58%)
  waiting for transfers between devices  52.6 us (15%)
  starting transfers between devices  52.1 us (15%)
  blocking collectives  39.1 us (11%)
    pallas_call x1, Pallas kernels, join(): pl.pallas_call(join_kernel, name='join', in_specs=[hbm] * len(parts), out...  168 us
    ppermute x30, starting transfers between devices, turn(): lax.ppermute(value, axis, [(i, (i + by) % count) for i in range(count)])  46.6 us
    ppermute x30, waiting for transfers between devices, turn(): lax.ppermute(value, axis, [(i, (i + by) % count) for i in range(count)])  42.2 us
    all_to_all x1, blocking collectives, layer(): lax.all_to_all(result.reshape(2 * groups, half, LANES), exchange, 0, 0, t...  23.6 us
    pallas_call x2, Pallas kernels, ffn(): pl.pallas_call(up_kernel, name='ffn_up', in_specs=[sm] + [hbm] * 10, out_...  19.1 us
    all_to_all x1, blocking collectives, layer(): gathered = lax.all_to_all(squares, ('z', 'c'), 0, 0, tiled=True)  15.5 us
    all_to_all x1, waiting for transfers between devices, layer(): lax.all_to_all(outgoing.reshape(2 * groups, half, LANES), exchange, 0, 0,...  10.4 us
    pallas_call x2, Pallas kernels, ffn(): pl.pallas_call(down_kernel, name='ffn_down', in_specs=[sm, vm, hbm, hbm],...  7.07 us
  transfers between devices with their start and end apart: 31, of which 14 were waited for; matrix products, arithmetic and copies ran while one was open for 0% of the time, Pallas kernels for 9%

commit v1 on v0

--- a/solution.py
+++ b/solution.py
@@ -11,9 +11,8 @@
 CHUNKS = 2
 EXTRA = 16
 MIB = 1024 * 1024
-UP_VMEM = 26 * MIB
-DOWN_VMEM = 12 * MIB
-NORM_UNROLL = 1
+UP_VMEM = 46 * MIB
+PART_VMEM = 46 * MIB
 SMALL_VMEM = 12 * MIB
 F32 = jnp.float32
 BF16 = jnp.bfloat16
@@ -102,8 +101,12 @@
 
 
 NEAR = (0, -1, 1, -2, 2, -3, 3, -4)
-FIRST = (7, 5, 6)
-LATER = (3, 4, 1, 2, 0)
+FAR_FIRST = (7, 5, 6, 3, 4, 1, 2, 0)
+
+
+EARLY = (0, 1, 2, 3, 4)
+LATE = (5, 6, 7)
+UNITS = 64
 
 
 def near(z_ref):
@@ -111,24 +114,92 @@
     return [pl.multiple_of(lax.rem(z + (off + 8), 8) * 256, 256) for off in NEAR]
 
 
+def load_in(own, other, scr, columns, sem):
+    blocks = scr.shape[0]
+    for q in range(4):
+        src = (own, other)[q % 2]
+        for n, column in enumerate(columns):
+            pltpu.make_async_copy(
+                src.at[pl.ds(q // 2 * blocks, blocks), :, pl.ds(column, 256)],
+                scr.at[:, q, :, pl.ds(n * 256, 256)],
+                sem,
+            ).start()
+
+
 def load_down(own, other, scr, sem):
-    hidden = scr.shape[0] // 2
+    blocks = scr.shape[0]
     for n, src in enumerate((own, other)):
-        pltpu.make_async_copy(
-            src.at[pl.ds(2 * hidden, hidden), :], scr.at[pl.ds(n * hidden, hidden), :], sem
-        ).start()
+        pltpu.make_async_copy(src.at[pl.ds(2 * blocks, blocks)], scr.at[:, n], sem).start()
+
+
+def gained(piece_scr, x_scr, sums_ref, start_sums):
+    count = piece_scr.shape[0]
+    rows = x_scr.shape[0]
+    tile = 32
+    gains = [
+        [piece_scr[j, c, pl.ds(rows, EXTRA), :].astype(F32)[0:1, :] for c in range(2)]
+        for j in range(count)
+    ]
+
+    def one(t, carry):
+        span = pl.ds(pl.multiple_of(t * tile, tile), tile)
+        acc = jnp.zeros((tile, LANES), F32) if start_sums is None else start_sums[span, :]
+        for j in range(count):
+            for c in range(2):
+                v = piece_scr[j, c, span, :].astype(F32)
+                acc = acc + v * v
+                x_scr[span, (2 * j + c) * LANES : (2 * j + c + 1) * LANES] = (
+                    v * gains[j][c]
+                ).astype(BF16)
+        if start_sums is not None:
+            scale = lax.rsqrt(jnp.sum(acc, axis=1, keepdims=True) / D + EPS)
+            acc = jnp.broadcast_to(scale, (tile, LANES))
+        sums_ref[span, :] = acc
+        return carry
+
+    lax.fori_loop(0, rows // tile, one, 0)
+
+
+def product(x_scr, in_scr, n):
+    columns = x_scr.shape[1]
+    w = in_scr[n].reshape(4 * UNITS, columns)
+    return lax.dot_general(
+        x_scr[...], w, (((1,), (1,)), ((), ())), preferred_element_type=F32
+    )
+
+
+def load_pieces(given, piece_scr, sem):
+    for j, src in enumerate(given):
+        pltpu.make_async_copy(src, piece_scr.at[j], sem).start()
+
+
+def part_kernel(
+    z_ref, x0, p1, m1, p2, m2, own, other, acc_ref, sums_ref, piece_scr, x_scr, in_scr, sems
+):
+    order = near(z_ref)
+    load_pieces((x0, p1, m1, p2, m2), piece_scr, sems.at[0])
+    load_in(own, other, in_scr, [order[j] for j in EARLY], sems.at[1])
+    pltpu.make_async_copy(piece_scr, piece_scr, sems.at[0]).wait()
+    gained(piece_scr, x_scr, sums_ref, None)
+    pltpu.make_async_copy(in_scr, in_scr, sems.at[1]).wait()
+
+    def one(n, carry):
+        acc_ref[n] = product(x_scr, in_scr, n)
+        return carry
+
+    lax.fori_loop(0, in_scr.shape[0], one, 0)
 
 
 def put_down(h_ref, scr, order, outs):
     step = h_ref.shape[0] // 2
+    blocks = scr.shape[0]
     outs = list(outs)
 
     def tile(r, carry):
         span = pl.ds(pl.multiple_of(r * step, step), step)
         for j, out in outs:
-            part = jnp.dot(
-                h_ref[span, :], scr[:, pl.ds(order[j], 256)], preferred_element_type=F32
-            ).astype(BF16)
+            w = scr[:, :, :, pl.ds(order[j], 256)].reshape(blocks * 2 * UNITS, 256)
+            part = jnp.dot(h_ref[span, :], w, preferred_element_type=F32).astype(BF16)
             out[0, span, :] = part[:, :LANES]
             out[1, span, :] = part[:, LANES:]
         return carry
@@ -137,135 +208,126 @@
 
 
 def up_kernel(
-    z_ref, x0, p1, m1, p2, m2, p3, m3, x4, own, other, h_ref, o4, op3, om3,
-    piece_scr, x_scr, in_scr, down_scr, sems,
+    z_ref, p3, m3, x4, acc_ref, sums_ref, own, other,
+    o4, op3, om3, op2, om2, op1, om1, o0,
+    piece_scr, x_scr, scale_scr, in_scr, down_scr, h_ref, sems,
 ):
-    rows = o4.shape[1]
-    hidden = h_ref.shape[1] // 2
     order = near(z_ref)
-    for j, src in enumerate((x0, p1, m1, p2, m2, p3, m3, x4)):
-        pltpu.make_async_copy(src, piece_scr.at[j], sems.at[0]).start()
-    for n, (src, at) in enumerate(((own, 0), (other, 0), (own, hidden), (other, hidden))):
-        pltpu.make_async_copy(
-            src.at[pl.ds(at, hidden), :], in_scr.at[pl.ds(n * hidden, hidden), :], sems.at[1]
-        ).start()
+    load_pieces((p3, m3, x4), piece_scr, sems.at[0])
+    load_in(own, other, in_scr, [order[j] for j in LATE], sems.at[1])
     load_down(own, other, down_scr, sems.at[2])
     pltpu.make_async_copy(piece_scr, piece_scr, sems.at[0]).wait()
-    tile = 32
-    gains = [
-        [piece_scr[j, c, pl.ds(rows, EXTRA), :].astype(F32)[0:1, :] for c in range(2)]
-        for j in range(8)
-    ]
-
-    def norm_tile(t, carry):
-        start = pl.multiple_of(t * tile, tile)
-        acc = jnp.zeros((tile, LANES), F32)
-        for j in range(8):
-            for c in range(2):
-                v = piece_scr[j, c, pl.ds(start, tile), :].astype(F32)
-                acc = acc + v * v
-        scale = lax.rsqrt(jnp.sum(acc, axis=1, keepdims=True) / D + EPS)
-        for j in range(8):
-            both = [
-                (piece_scr[j, c, pl.ds(start, tile), :].astype(F32) * scale * gains[j][c]).astype(BF16)
-                for c in range(2)
-            ]
-            x_scr[pl.ds(start, tile), pl.ds(order[j], 256)] = jnp.concatenate(both, axis=1)
-        return carry
-
-    lax.fori_loop(0, rows // tile, norm_tile, 0, unroll=NORM_UNROLL)
+    gained(piece_scr, x_scr, scale_scr, sums_ref)
     pltpu.make_async_copy(in_scr, in_scr, sems.at[1]).wait()
-    step = rows // 2
-
-    def up_tile(r, carry):
-        span = pl.ds(pl.multiple_of(r * step, step), step)
-        both = lax.dot_general(
-            x_scr[span, :], in_scr[...], (((1,), (1,)), ((), ())), preferred_element_type=F32
-        )
-        gate = both[:, : 2 * hidden]
-        up = both[:, 2 * hidden :]
-        h_ref[span, :] = (gate / (1.0 + jnp.exp(-gate)) * up).astype(BF16)
-        return carry
-
-    lax.fori_loop(0, 2, up_tile, 0)
+
+    def one(n, carry):
+        both = product(x_scr, in_scr, n) + acc_ref[n]
+        scale = scale_scr[...]
+        gate = both[:, :LANES] * scale
+        up = both[:, LANES:] * scale
+        hidden = (gate / (1.0 + jnp.exp(-gate)) * up).astype(BF16)
+        h_ref[:, pl.ds(pl.multiple_of(n * LANES, LANES), LANES)] = hidden
+        return carry
+
+    lax.fori_loop(0, in_scr.shape[0], one, 0)
     pltpu.make_async_copy(down_scr, down_scr, sems.at[2]).wait()
-    put_down(h_ref, down_scr, order, zip(FIRST, (o4, op3, om3)))
-
-
-def down_kernel(z_ref, h_ref, own, other, op2, om2, op1, om1, o0, down_scr, sem):
-    load_down(own, other, down_scr, sem)
-    pltpu.make_async_copy(down_scr, down_scr, sem).wait()
-    put_down(h_ref, down_scr, near(z_ref), zip(LATER, (op2, om2, op1, om1, o0)))
+    put_down(h_ref, down_scr, order, zip(FAR_FIRST, (o4, op3, om3, op2, om2, op1, om1, o0)))
 
 
 def ffn(z, pieces, own, other):
     rows = pieces[0].shape[1] - EXTRA
     hidden = own.shape[0] // 3
+    blocks = hidden // UNITS
+    own, other = (w.reshape(3 * blocks, UNITS, D) for w in (own, other))
     vm = pl.BlockSpec(memory_space=pltpu.VMEM)
     sm = pl.BlockSpec(memory_space=pltpu.SMEM)
     hbm = pl.BlockSpec(memory_space=pltpu.HBM)
     full = jax.ShapeDtypeStruct((2, rows, LANES), BF16)
     wide = 2 * rows * D * 2 * hidden
-    h, o4, op3, om3 = pl.pallas_call(
+    early, late = len(EARLY), len(LATE)
+    acc, sums = pl.pallas_call(
+        part_kernel,
+        name="ffn_part",
+        in_specs=[sm] + [hbm] * (early + 2),
+        out_specs=[vm] * 2,
+        out_shape=[
+            jax.ShapeDtypeStruct((blocks, rows, 4 * UNITS), F32),
+            jax.ShapeDtypeStruct((rows, LANES), F32),
+        ],
+        scratch_shapes=[
+            pltpu.VMEM((early, 2, rows + EXTRA, LANES), BF16),
+            pltpu.VMEM((rows, early * 256), BF16),
+            pltpu.VMEM((blocks, 4, UNITS, early * 256), BF16),
+            pltpu.SemaphoreType.DMA((2,)),
+        ],
+        cost_estimate=pl.CostEstimate(
+            flops=2 * wide * early // 8,
+            bytes_accessed=early * D * hidden + 4 * rows * D,
+            transcendentals=0,
+        ),
+        compiler_params=pltpu.CompilerParams(vmem_limit_bytes=PART_VMEM),
+    )(z, *(pieces[j] for j in EARLY), own, other)
+    o4, op3, om3, op2, om2, op1, om1, o0 = pl.pallas_call(
         up_kernel,
         name="ffn_up",
-        in_specs=[sm] + [hbm] * 10,
-        out_specs=[vm] * 4,
-        out_shape=[jax.ShapeDtypeStruct((rows, 2 * hidden), BF16)] + [full] * 3,
+        in_specs=[sm] + [hbm] * late + [vm] * 2 + [hbm] * 2,
+        out_specs=[vm] * 8,
+        out_shape=[full] * 8,
         scratch_shapes=[
-            pltpu.VMEM((8, 2, rows + EXTRA, LANES), BF16),
-            pltpu.VMEM((rows, D), BF16),
-            pltpu.VMEM((4 * hidden, D), BF16),
-            pltpu.VMEM((2 * hidden, D), BF16),
+            pltpu.VMEM((late, 2, rows + EXTRA, LANES), BF16),
+            pltpu.VMEM((rows, late * 256), BF16),
+            pltpu.VMEM((rows, LANES), F32),
+            pltpu.VMEM((blocks, 4, UNITS, late * 256), BF16),
+            pltpu.VMEM((blocks, 2, UNITS, D), BF16),
+            pltpu.VMEM((rows, 2 * hidden), BF16),
             pltpu.SemaphoreType.DMA((3,)),
         ],
         cost_estimate=pl.CostEstimate(
-            flops=2 * wide + wide * 3 // 8,
-            bytes_accessed=12 * D * hidden + 4 * rows * D,
+            flops=2 * wide * late // 8 + wide,
+            bytes_accessed=7 * D * hidden + 4 * rows * D,
             transcendentals=rows * hidden * 2,
         ),
         compiler_params=pltpu.CompilerParams(vmem_limit_bytes=UP_VMEM),
-    )(z, *pieces, own, other)
-    op2, om2, op1, om1, o0 = pl.pallas_call(
-        down_kernel,
-        name="ffn_down",
-        in_specs=[sm, vm, hbm, hbm],
-        out_specs=[vm] * 5,
-        out_shape=[full] * 5,
-        scratch_shapes=[pltpu.VMEM((2 * hidden, D), BF16), pltpu.SemaphoreType.DMA],
-        cost_estimate=pl.CostEstimate(
-            flops=wide * 5 // 8,
-            bytes_accessed=4 * D * hidden + 2 * rows * D,
-            transcendentals=0,
-        ),
-        compiler_params=pltpu.CompilerParams(vmem_limit_bytes=DOWN_VMEM),
-    )(z, h, own, other)
+    )(z, *(pieces[j] for j in LATE), acc, sums, own, other)
     return o0, (om1, om2, om3), (op1, op2, op3), o4
 
 
 def join_kernel(*refs):
-    *given, out, sems = refs
+    *given, out, scr, ins, outs = refs
     size = given[0].shape[0]
-    copies = [
-        pltpu.make_async_copy(src, out.at[pl.ds(n * size, size), :], sems.at[n])
-        for n, src in enumerate(given)
-    ]
-    for copy in copies:
-        copy.start()
-    for copy in copies:
-        copy.wait()
+    stages = []
+    for n, src in enumerate(given):
+        here = scr.at[pl.ds(n * size, size), :]
+        stages.append(
+            (
+                pltpu.make_async_copy(src, here, ins.at[n]),
+                pltpu.make_async_copy(here, out.at[pl.ds(n * size, size), :], outs.at[n]),
+            )
+        )
+    for first, _ in stages:
+        first.start()
+    for first, second in stages:
+        first.wait()
+        second.start()
+    for _, second in stages:
+        second.wait()
 
 
 def join(parts):
     rows, columns = parts[0].shape
+    count = len(parts)
     hbm = pl.BlockSpec(memory_space=pltpu.HBM)
     return pl.pallas_call(
         join_kernel,
         name="join",
-        in_specs=[hbm] * len(parts),
+        in_specs=[hbm] * count,
         out_specs=hbm,
-        out_shape=jax.ShapeDtypeStruct((len(parts) * rows, columns), BF16),
-        scratch_shapes=[pltpu.SemaphoreType.DMA((len(parts),))],
+        out_shape=jax.ShapeDtypeStruct((count * rows, columns), BF16),
+        scratch_shapes=[
+            pltpu.VMEM((count * rows, columns), BF16),
+            pltpu.SemaphoreType.DMA((count,)),
+            pltpu.SemaphoreType.DMA((count,)),
+        ],
         compiler_params=pltpu.CompilerParams(vmem_limit_bytes=60 * MIB),
     )(*parts)
 
@@ -326,7 +388,7 @@
     outgoing, places = pl.pallas_call(
         route_kernel,
         name="route",
-        compiler_params=pltpu.CompilerParams(vmem_limit_bytes=SMALL_VMEM),
+        compiler_params=pltpu.CompilerParams(vmem_limit_bytes=60 * MIB),
         out_shape=[
             jax.ShapeDtypeStruct((total, LANES), BF16),
             jax.ShapeDtypeStruct((tok_rows, LANES), F32),

time: 353 us -> 191 us (0.54)
  Pallas kernels: 205 us -> 46.2 us
    pallas_call x5, Pallas kernels: 194 us -> 34.4 us  [the longest x2 16.4 us: ffn(): pl.pallas_call(up_kernel, name='ffn_up', in_specs=[sm] + [hbm] * late + [...]
  transfers between devices with their start and end apart: 31 -> 31, of which waited for: 14 -> 14; matrix products, arithmetic and copies ran while one was open for 0% -> 1% of each run, Pallas kernels for 9% -> 19%
where the time goes in v1:
time: 191 us
  starting transfers between devices  52.5 us (27%)
  waiting for transfers between devices  50.9 us (27%)
  Pallas kernels  46.2 us (24%)
  blocking collectives  38.2 us (20%)
    ppermute x30, starting transfers between devices, turn(): lax.ppermute(value, axis, [(i, (i + by) % count) for i in range(count)])  47 us
    ppermute x30, waiting for transfers between devices, turn(): lax.ppermute(value, axis, [(i, (i + by) % count) for i in range(count)])  40.5 us
    all_to_all x1, blocking collectives, layer(): lax.all_to_all(result.reshape(2 * groups, half, LANES), exchange, 0, 0, t...  23.1 us
    pallas_call x2, Pallas kernels, ffn(): pl.pallas_call(up_kernel, name='ffn_up', in_specs=[sm] + [hbm] * late + [...  16.4 us
    all_to_all x1, blocking collectives, layer(): gathered = lax.all_to_all(squares, ('z', 'c'), 0, 0, tiled=True)  15.1 us
    pallas_call x2, Pallas kernels, ffn(): pl.pallas_call(part_kernel, name='ffn_part', in_specs=[sm] + [hbm] * (ear...  13.7 us
    all_to_all x1, waiting for transfers between devices, layer(): lax.all_to_all(outgoing.reshape(2 * groups, half, LANES), exchange, 0, 0,...  10.4 us
    pallas_call x1, Pallas kernels, layer(): pl.pallas_call(route_kernel, name='route', compiler_params=pltpu.Compiler...  7.09 us
  transfers between devices with their start and end apart: 31, of which 14 were waited for; matrix products, arithmetic and copies ran while one was open for 1% of the time, Pallas kernels for 19%

profile of v1, /device:TPU:1, one launch (start us, length us, event | category | flops | bytes accessed | tf_op | source)
XLA Modules:
  0.0 191.0 jit_solution(5067297018859376920)
XLA Ops:
  0.0 4.3 %join.1 = bf16[1344,2048]{1,0:T(8,128)(2,1)} custom-call(bf16[448,2048]{1,0:T(8,128)(2,1)} %bitcast.26, bf16[448,2048]{1,0:T(8,128)(2,1)} %bitcast.27, bf16[448,2048]{1,0:T(8,128)(2,1)} %bitcast.28), custom_call_target="tpu_custom_call" | custom-call | tf_op jit(solution)/shard_map/join/pallas_call | solution.py:320
  4.3 3.3 %collective-permute-start.8 = (bf16[1344,2048]{1,0:T(8,128)(2,1)}, bf16[1344,2048]{1,0:T(8,128)(2,1)}, u32[]{:S(2)}, u32[]{:S(2)}) collective-permute-start(bf16[1344,2048]{1,0:T(8,128)(2,1)} %join.1), channel_id=1, source_target_pairs={{0,1},{1,0},{2,3},{3,2},{4,5},{5,4},{6,7},{7,6},{8,9},{9,8},{10,11... | collective-permute-start | bytes 16515080 | tf_op jit(solution)/shard_map/ppermute | solution.py:337
  7.6 7.1 %route.1 = (bf16[2304,128]{1,0:T(8,128)(2,1)}, f32[1024,128]{1,0:T(8,128)}) custom-call(s32[2,1024]{1,0:T(2,128)} %bitcast.30, f32[2,1024]{1,0:T(2,128)} %bitcast.31, bf16[1024,128]{1,0:T(8,128)(2,1)} %tok_ref.1), custom_call_target="tpu_custom_call" | custom-call | tf_op jit(solution)/shard_map/route/pallas_call | solution.py:388
  14.6 5.5 %all-to-all-start = ((bf16[32,72,128]{2,1,0:T(8,128)(2,1)}), bf16[32,72,128]{2,1,0:T(8,128)(2,1)S(1)}, u32[]{:S(2)}, u32[]{:S(2)}) async-start(bf16[32,72,128]{2,1,0:T(8,128)(2,1)} %bitcast.29), calls=%async_computation | async-start | bytes 1179648 | tf_op jit(solution)/shard_map/all_to_all | solution.py:399
  21.4 10.4 %all-to-all-done = bf16[32,72,128]{2,1,0:T(8,128)(2,1)S(1)} async-done(((bf16[32,72,128]{2,1,0:T(8,128)(2,1)}), bf16[32,72,128]{2,1,0:T(8,128)(2,1)S(1)}, u32[]{:S(2)}, u32[]{:S(2)}) %all-to-all-start) | async-done | bytes 589856 | tf_op jit(solution)/shard_map/all_to_all | solution.py:399
  33.7 4.0 %collective-permute-start.19 = (bf16[2,592,128]{2,1,0:T(8,128)(2,1)S(1)}, bf16[2,592,128]{2,1,0:T(8,128)(2,1)S(1)}, u32[]{:S(2)}, u32[]{:S(2)}) collective-permute-start(bf16[2,592,128]{2,1,0:T(8,128)(2,1)S(1)} %get-tuple-element.56.x0), channel_id=1, source_target_pairs={{0,14},{2,0},{4,2},{6,4},{8,6},{10,8},{12,10},{14,12},{1,15},{3,1}... | collective-permute-start | bytes 909320 | tf_op jit(solution)/shard_map/ppermute | solution.py:337
  39.1 4.9 %collective-permute-done.1.p1 = bf16[2,592,128]{2,1,0:T(8,128)(2,1)S(1)} collective-permute-done((bf16[2,592,128]{2,1,0:T(8,128)(2,1)S(1)}, bf16[2,592,128]{2,1,0:T(8,128)(2,1)S(1)}, u32[]{:S(2)}, u32[]{:S(2)}) %collective-permute-start.1) | collective-permute-done | bytes 303136 | tf_op jit(solution)/shard_map/ppermute | solution.py:337
  44.0 2.7 %collective-permute-start.20 = (bf16[2,592,128]{2,1,0:T(8,128)(2,1)S(1)}, bf16[2,592,128]{2,1,0:T(8,128)(2,1)S(1)}, u32[]{:S(2)}, u32[]{:S(2)}) collective-permute-start(bf16[2,592,128]{2,1,0:T(8,128)(2,1)S(1)} %collective-permute-done.19.m1), channel_id=1, source_target_pairs={{0,14},{2,0},{4,2},{6,4},{8,6},{10,8},{12,10},{14,12},{1,15},{3,1}... | collective-permute-start | bytes 909320 | tf_op jit(solution)/shard_map/ppermute | solution.py:337
  46.7 2.9 %collective-permute-done.4.m1 = bf16[2,592,128]{2,1,0:T(8,128)(2,1)S(1)} collective-permute-done((bf16[2,592,128]{2,1,0:T(8,128)(2,1)S(1)}, bf16[2,592,128]{2,1,0:T(8,128)(2,1)S(1)}, u32[]{:S(2)}, u32[]{:S(2)}) %collective-permute-start.4) | collective-permute-done | bytes 303136 | tf_op jit(solution)/shard_map/ppermute | solution.py:337
  49.6 3.4 %collective-permute-start.5 = (bf16[2,592,128]{2,1,0:T(8,128)(2,1)S(1)}, bf16[2,592,128]{2,1,0:T(8,128)(2,1)}, u32[]{:S(2)}, u32[]{:S(2)}) collective-permute-start(bf16[2,592,128]{2,1,0:T(8,128)(2,1)S(1)} %collective-permute-done.4.m1), channel_id=1, source_target_pairs={{0,14},{2,0},{4,2},{6,4},{8,6},{10,8},{12,10},{14,12},{1,15},{3,1}... | collective-permute-start | bytes 909320 | tf_op jit(solution)/shard_map/ppermute | solution.py:337
  53.8 5.0 %collective-permute-done.16.p1 = bf16[2,592,128]{2,1,0:T(8,128)(2,1)S(1)} collective-permute-done((bf16[2,592,128]{2,1,0:T(8,128)(2,1)S(1)}, bf16[2,592,128]{2,1,0:T(8,128)(2,1)S(1)}, u32[]{:S(2)}, u32[]{:S(2)}) %collective-permute-start.16) | collective-permute-done | bytes 303136 | tf_op jit(solution)/shard_map/ppermute | solution.py:337
  58.8 2.7 %collective-permute-start.21 = (bf16[2,592,128]{2,1,0:T(8,128)(2,1)S(1)}, bf16[2,592,128]{2,1,0:T(8,128)(2,1)S(1)}, u32[]{:S(2)}, u32[]{:S(2)}) collective-permute-start(bf16[2,592,128]{2,1,0:T(8,128)(2,1)S(1)} %collective-permute-done.20.m2), channel_id=1, source_target_pairs={{0,14},{2,0},{4,2},{6,4},{8,6},{10,8},{12,10},{14,12},{1,15},{3,1}... | collective-permute-start | bytes 909320 | tf_op jit(solution)/shard_map/ppermute | solution.py:337
  62.6 3.5 %collective-permute-start.6 = (bf16[2,592,128]{2,1,0:T(8,128)(2,1)}, bf16[2,592,128]{2,1,0:T(8,128)(2,1)S(1)}, u32[]{:S(2)}, u32[]{:S(2)}) collective-permute-start(bf16[2,592,128]{2,1,0:T(8,128)(2,1)} %collective-permute-done.5.m2), channel_id=1, source_target_pairs={{0,14},{2,0},{4,2},{6,4},{8,6},{10,8},{12,10},{14,12},{1,15},{3,1}... | collective-permute-start | bytes 909320 | tf_op jit(solution)/shard_map/ppermute | solution.py:337
  66.1 5.7 %collective-permute-done.17.p2 = bf16[2,592,128]{2,1,0:T(8,128)(2,1)} collective-permute-done((bf16[2,592,128]{2,1,0:T(8,128)(2,1)S(1)}, bf16[2,592,128]{2,1,0:T(8,128)(2,1)}, u32[]{:S(2)}, u32[]{:S(2)}) %collective-permute-start.17) | collective-permute-done | bytes 303136 | tf_op jit(solution)/shard_map/ppermute | solution.py:337
  71.8 2.7 %collective-permute-start.22 = (bf16[2,592,128]{2,1,0:T(8,128)(2,1)S(1)}, bf16[2,592,128]{2,1,0:T(8,128)(2,1)S(1)}, u32[]{:S(2)}, u32[]{:S(2)}) collective-permute-start(bf16[2,592,128]{2,1,0:T(8,128)(2,1)S(1)} %collective-permute-done.21.m3), channel_id=1, source_target_pairs={{0,14},{2,0},{4,2},{6,4},{8,6},{10,8},{12,10},{14,12},{1,15},{3,1}... | collective-permute-start | bytes 909320 | tf_op jit(solution)/shard_map/ppermute | solution.py:337
  75.5 6.9 %ffn_part.2 = (f32[7,576,256]{2,1,0:T(8,128)S(1)}, f32[576,128]{1,0:T(8,128)S(1)}) custom-call(s32[1]{0:T(128)} %bitcast.z_ref, bf16[2,592,128]{2,1,0:T(8,128)(2,1)S(1)} %get-tuple-element.55.x0, bf16[2,592,128]{2,1,0:T(8,128)(2,1)S(1)} %collective-permute-done.1.p1, bf16[2,592,128]{2,1,0:T(8,128)(2,1)S(1)} %collective-permute-done.4.m1, ...), custom_call_target="tpu_custom_call" | custom-call | flops 2642411520 | bytes 9306112 | tf_op jit(solution)/shard_map/ffn_part/pallas_call | solution.py:248
  82.4 8.2 %ffn_up.2 = (bf16[2,576,128]{2,1,0:T(8,128)(2,1)S(1)}, bf16[2,576,128]{2,1,0:T(8,128)(2,1)S(1)}, bf16[2,576,128]{2,1,0:T(8,128)(2,1)S(1)}, bf16[2,576,128]{2,1,0...) custom-call(s32[1]{0:T(128)} %bitcast.z_ref, ...), custom_call_target="tpu_custom_call" | custom-call | flops 3699376128 | bytes 11141120 | tf_op jit(solution)/shard_map/ffn_up/pallas_call | solution.py:270
  93.4 6.8 %ffn_part.3 = (f32[7,576,256]{2,1,0:T(8,128)S(1)}, f32[576,128]{1,0:T(8,128)S(1)}) custom-call(s32[1]{0:T(128)} %bitcast.z_ref, bf16[2,592,128]{2,1,0:T(8,128)(2,1)S(1)} %get-tuple-element.56.x0, bf16[2,592,128]{2,1,0:T(8,128)(2,1)S(1)} %collective-permute-done.16.p1, bf16[2,592,128]{2,1,0:T(8,128)(2,1)S(1)} %collective-permute-done.19.m1, ...), custom_call_target="tpu_custom_call" | custom-call | flops 2642411520 | bytes 9306112 | tf_op jit(solution)/shard_map/ffn_part/pallas_call | solution.py:248
  100.2 8.2 %ffn_up.3 = (bf16[2,576,128]{2,1,0:T(8,128)(2,1)S(1)}, bf16[2,576,128]{2,1,0:T(8,128)(2,1)S(1)}, bf16[2,576,128]{2,1,0:T(8,128)(2,1)S(1)}, bf16[2,576,128]{2,1,0...) custom-call(s32[1]{0:T(128)} %bitcast.z_ref, ...), custom_call_target="tpu_custom_call" | custom-call | flops 3699376128 | bytes 11141120 | tf_op jit(solution)/shard_map/ffn_up/pallas_call | solution.py:270
  111.5 2.7 %collective-permute-start.14 = (bf16[2,576,128]{2,1,0:T(8,128)(2,1)S(1)}, bf16[2,576,128]{2,1,0:T(8,128)(2,1)S(1)}, u32[]{:S(2)}, u32[]{:S(2)}) collective-permute-start(bf16[2,576,128]{2,1,0:T(8,128)(2,1)S(1)} %add_convert_fusion.8), channel_id=1, source_target_pairs={{0,14},{2,0},{4,2},{6,4},{8,6},{10,8},{12,10},{14,12},{1,15},{3,1}... | collective-permute-start | bytes 884744 | tf_op jit(solution)/shard_map/ppermute | solution.py:337
  115.6 2.9 %collective-permute-start.27 = (bf16[2,576,128]{2,1,0:T(8,128)(2,1)S(1)}, bf16[2,576,128]{2,1,0:T(8,128)(2,1)S(1)}, u32[]{:S(2)}, u32[]{:S(2)}) collective-permute-start(bf16[2,576,128]{2,1,0:T(8,128)(2,1)S(1)} %add_convert_fusion.3), channel_id=1, source_target_pairs={{0,14},{2,0},{4,2},{6,4},{8,6},{10,8},{12,10},{14,12},{1,15},{3,1}... | collective-permute-start | bytes 884744 | tf_op jit(solution)/shard_map/ppermute | solution.py:337
  118.8 2.7 %collective-permute-start.15 = (bf16[2,576,128]{2,1,0:T(8,128)(2,1)S(1)}, bf16[2,576,128]{2,1,0:T(8,128)(2,1)S(1)}, u32[]{:S(2)}, u32[]{:S(2)}) collective-permute-start(bf16[2,576,128]{2,1,0:T(8,128)(2,1)S(1)} %add_convert_fusion.7), channel_id=1, source_target_pairs={{0,14},{2,0},{4,2},{6,4},{8,6},{10,8},{12,10},{14,12},{1,15},{3,1}... | collective-permute-start | bytes 884744 | tf_op jit(solution)/shard_map/ppermute | solution.py:337
  121.5 3.8 %collective-permute-done.27 = bf16[2,576,128]{2,1,0:T(8,128)(2,1)S(1)} collective-permute-done((bf16[2,576,128]{2,1,0:T(8,128)(2,1)S(1)}, bf16[2,576,128]{2,1,0:T(8,128)(2,1)S(1)}, u32[]{:S(2)}, u32[]{:S(2)}) %collective-permute-start.27) | collective-permute-done | bytes 294944 | tf_op jit(solution)/shard_map/ppermute | solution.py:337
  125.4 3.5 %collective-permute-start.28 = (bf16[2,576,128]{2,1,0:T(8,128)(2,1)S(1)}, bf16[2,576,128]{2,1,0:T(8,128)(2,1)S(1)}, u32[]{:S(2)}, u32[]{:S(2)}) collective-permute-start(bf16[2,576,128]{2,1,0:T(8,128)(2,1)S(1)} %add_convert_fusion.2), channel_id=1, source_target_pairs={{0,14},{2,0},{4,2},{6,4},{8,6},{10,8},{12,10},{14,12},{1,15},{3,1}... | collective-permute-start | bytes 884744 | tf_op jit(solution)/shard_map/ppermute | solution.py:337
  128.9 3.1 %collective-permute-done.11 = bf16[2,576,128]{2,1,0:T(8,128)(2,1)S(1)} collective-permute-done((bf16[2,576,128]{2,1,0:T(8,128)(2,1)S(1)}, bf16[2,576,128]{2,1,0:T(8,128)(2,1)S(1)}, u32[]{:S(2)}, u32[]{:S(2)}) %collective-permute-start.11) | collective-permute-done | bytes 294944 | tf_op jit(solution)/shard_map/ppermute | solution.py:337
  132.4 5.6 %collective-permute-done.28 = bf16[2,576,128]{2,1,0:T(8,128)(2,1)S(1)} collective-permute-done((bf16[2,576,128]{2,1,0:T(8,128)(2,1)S(1)}, bf16[2,576,128]{2,1,0:T(8,128)(2,1)S(1)}, u32[]{:S(2)}, u32[]{:S(2)}) %collective-permute-start.28) | collective-permute-done | bytes 294944 | tf_op jit(solution)/shard_map/ppermute | solution.py:337
  138.1 3.5 %collective-permute-start.29 = (bf16[2,576,128]{2,1,0:T(8,128)(2,1)S(1)}, bf16[2,576,128]{2,1,0:T(8,128)(2,1)S(1)}, u32[]{:S(2)}, u32[]{:S(2)}) collective-permute-start(bf16[2,576,128]{2,1,0:T(8,128)(2,1)S(1)} %add_convert_fusion.1), channel_id=1, source_target_pairs={{0,14},{2,0},{4,2},{6,4},{8,6},{10,8},{12,10},{14,12},{1,15},{3,1}... | collective-permute-start | bytes 884744 | tf_op jit(solution)/shard_map/ppermute | solution.py:337
  141.9 3.0 %collective-permute-done.25 = bf16[2,576,128]{2,1,0:T(8,128)(2,1)S(1)} collective-permute-done((bf16[2,576,128]{2,1,0:T(8,128)(2,1)S(1)}, bf16[2,576,128]{2,1,0:T(8,128)(2,1)S(1)}, u32[]{:S(2)}, u32[]{:S(2)}) %collective-permute-start.25) | collective-permute-done | bytes 294944 | tf_op jit(solution)/shard_map/ppermute | solution.py:337
  145.0 2.9 %collective-permute-done.29 = bf16[2,576,128]{2,1,0:T(8,128)(2,1)S(1)} collective-permute-done((bf16[2,576,128]{2,1,0:T(8,128)(2,1)S(1)}, bf16[2,576,128]{2,1,0:T(8,128)(2,1)S(1)}, u32[]{:S(2)}, u32[]{:S(2)}) %collective-permute-start.29) | collective-permute-done | bytes 294944 | tf_op jit(solution)/shard_map/ppermute | solution.py:337
  148.0 23.1 %all_to_all.15 = bf16[32,72,128]{2,1,0:T(8,128)(2,1)S(1)} all-to-all(bf16[32,72,128]{2,1,0:T(8,128)(2,1)S(1)} %bitcast.25), channel_id=1, replica_groups=mesh['y'=4,'x'=4,'z'=8,'c'=2] {'c','y','x'}, dimensions={0} | all-to-all | bytes 1179648 | tf_op jit(solution)/shard_map/all_to_all | solution.py:410
  171.2 3.8 %combine.1 = (f32[1024,128]{1,0:T(8,128)S(1)}, f32[16,8,128]{2,1,0:T(8,128)S(1)}) custom-call(bf16[2304,128]{1,0:T(8,128)(2,1)S(1)} %bitcast.18, f32[1024,128]{1,0:T(8,128)S(1)} %copy-done), custom_call_target="tpu_custom_call" | custom-call | tf_op jit(solution)/shard_map/combine/pallas_call | solution.py:414
  175.0 15.1 %all_to_all.16.squares_ref = f32[16,8,128]{2,1,0:T(8,128)S(1)} all-to-all(f32[16,8,128]{2,1,0:T(8,128)S(1)} %get-tuple-element.52), channel_id=1, replica_groups=mesh['y'=4,'x'=4,'z'=8,'c'=2] {'z','c'}, dimensions={0} | all-to-all | bytes 131072 | tf_op jit(solution)/shard_map/all_to_all | solution.py:423
  (68 shorter events, 16.7 us)
Async XLA Ops:
  4.3 70.3 %collective-permute-start.8 = (bf16[1344,2048]{1,0:T(8,128)(2,1)}, bf16[1344,2048]{1,0:T(8,128)(2,1)}, u32[]{:S(2)}, u32[]{:S(2)}) collective-permute-start(bf16[1344,2048]{1,0:T(8,128)(2,1)} %join.1), channel_id=1, source_target_pairs={{0,1},{1,0},{2,3},{3,2},{4,5},{5,4},{6,7},{7,6},{8,9},{9,8},{10,11... | collective-permute-start | bytes 16515080 | tf_op jit(solution)/shard_map/ppermute | solution.py:337
  14.6 17.2 %all-to-all-start = ((bf16[32,72,128]{2,1,0:T(8,128)(2,1)}), bf16[32,72,128]{2,1,0:T(8,128)(2,1)S(1)}, u32[]{:S(2)}, u32[]{:S(2)}) async-start(bf16[32,72,128]{2,1,0:T(8,128)(2,1)} %bitcast.29), calls=%async_computation | async-start | bytes 1179648 | tf_op jit(solution)/shard_map/all_to_all | solution.py:399
  20.2 1.3 collective-permute-start
  32.0 12.1 %collective-permute-start.1 = (bf16[2,592,128]{2,1,0:T(8,128)(2,1)S(1)}, bf16[2,592,128]{2,1,0:T(8,128)(2,1)S(1)}, u32[]{:S(2)}, u32[]{:S(2)}) collective-permute-start(bf16[2,592,128]{2,1,0:T(8,128)(2,1)S(1)} %get-tuple-element.55.x0), channel_id=1, source_target_pairs={{0,2},{2,4},{4,6},{6,8},{8,10},{10,12},{12,14},{14,0},{1,3},{3,5},... | collective-permute-start | bytes 909320 | tf_op jit(solution)/shard_map/ppermute | solution.py:337
  33.7 10.4 %collective-permute-start.19 = (bf16[2,592,128]{2,1,0:T(8,128)(2,1)S(1)}, bf16[2,592,128]{2,1,0:T(8,128)(2,1)S(1)}, u32[]{:S(2)}, u32[]{:S(2)}) collective-permute-start(bf16[2,592,128]{2,1,0:T(8,128)(2,1)S(1)} %get-tuple-element.56.x0), channel_id=1, source_target_pairs={{0,14},{2,0},{4,2},{6,4},{8,6},{10,8},{12,10},{14,12},{1,15},{3,1}... | collective-permute-start | bytes 909320 | tf_op jit(solution)/shard_map/ppermute | solution.py:337
  37.7 11.9 %collective-permute-start.4 = (bf16[2,592,128]{2,1,0:T(8,128)(2,1)S(1)}, bf16[2,592,128]{2,1,0:T(8,128)(2,1)S(1)}, u32[]{:S(2)}, u32[]{:S(2)}) collective-permute-start(bf16[2,592,128]{2,1,0:T(8,128)(2,1)S(1)} %get-tuple-element.55.x0), channel_id=1, source_target_pairs={{0,14},{2,0},{4,2},{6,4},{8,6},{10,8},{12,10},{14,12},{1,15},{3,1}... | collective-permute-start | bytes 909320 | tf_op jit(solution)/shard_map/ppermute | solution.py:337
  44.0 9.0 %collective-permute-start.2 = (bf16[2,592,128]{2,1,0:T(8,128)(2,1)S(1)}, bf16[2,592,128]{2,1,0:T(8,128)(2,1)S(1)}, u32[]{:S(2)}, u32[]{:S(2)}) collective-permute-start(bf16[2,592,128]{2,1,0:T(8,128)(2,1)S(1)} %collective-permute-done.1.p1), channel_id=1, source_target_pairs={{0,2},{2,4},{4,6},{6,8},{8,10},{10,12},{12,14},{14,0},{1,3},{3,5},... | collective-permute-start | bytes 909320 | tf_op jit(solution)/shard_map/ppermute | solution.py:337
  44.0 14.7 %collective-permute-start.16 = (bf16[2,592,128]{2,1,0:T(8,128)(2,1)S(1)}, bf16[2,592,128]{2,1,0:T(8,128)(2,1)S(1)}, u32[]{:S(2)}, u32[]{:S(2)}) collective-permute-start(bf16[2,592,128]{2,1,0:T(8,128)(2,1)S(1)} %get-tuple-element.56.x0), channel_id=1, source_target_pairs={{0,2},{2,4},{4,6},{6,8},{8,10},{10,12},{12,14},{14,0},{1,3},{3,5},... | collective-permute-start | bytes 909320 | tf_op jit(solution)/shard_map/ppermute | solution.py:337
  44.0 14.7 %collective-permute-start.20 = (bf16[2,592,128]{2,1,0:T(8,128)(2,1)S(1)}, bf16[2,592,128]{2,1,0:T(8,128)(2,1)S(1)}, u32[]{:S(2)}, u32[]{:S(2)}) collective-permute-start(bf16[2,592,128]{2,1,0:T(8,128)(2,1)S(1)} %collective-permute-done.19.m1), channel_id=1, source_target_pairs={{0,14},{2,0},{4,2},{6,4},{8,6},{10,8},{12,10},{14,12},{1,15},{3,1}... | collective-permute-start | bytes 909320 | tf_op jit(solution)/shard_map/ppermute | solution.py:337
  49.6 13.0 %collective-permute-start.5 = (bf16[2,592,128]{2,1,0:T(8,128)(2,1)S(1)}, bf16[2,592,128]{2,1,0:T(8,128)(2,1)}, u32[]{:S(2)}, u32[]{:S(2)}) collective-permute-start(bf16[2,592,128]{2,1,0:T(8,128)(2,1)S(1)} %collective-permute-done.4.m1), channel_id=1, source_target_pairs={{0,14},{2,0},{4,2},{6,4},{8,6},{10,8},{12,10},{14,12},{1,15},{3,1}... | collective-permute-start | bytes 909320 | tf_op jit(solution)/shard_map/ppermute | solution.py:337
  53.0 13.1 %collective-permute-start.3 = (bf16[2,592,128]{2,1,0:T(8,128)(2,1)S(1)}, bf16[2,592,128]{2,1,0:T(8,128)(2,1)S(1)}, u32[]{:S(2)}, u32[]{:S(2)}) collective-permute-start(bf16[2,592,128]{2,1,0:T(8,128)(2,1)S(1)} %collective-permute-done.2.p2), channel_id=1, source_target_pairs={{0,2},{2,4},{4,6},{6,8},{8,10},{10,12},{12,14},{14,0},{1,3},{3,5},... | collective-permute-start | bytes 909320 | tf_op jit(solution)/shard_map/ppermute | solution.py:337
  58.7 13.1 %collective-permute-start.17 = (bf16[2,592,128]{2,1,0:T(8,128)(2,1)S(1)}, bf16[2,592,128]{2,1,0:T(8,128)(2,1)}, u32[]{:S(2)}, u32[]{:S(2)}) collective-permute-start(bf16[2,592,128]{2,1,0:T(8,128)(2,1)S(1)} %collective-permute-done.16.p1), channel_id=1, source_target_pairs={{0,2},{2,4},{4,6},{6,8},{8,10},{10,12},{12,14},{14,0},{1,3},{3,5},... | collective-permute-start | bytes 909320 | tf_op jit(solution)/shard_map/ppermute | solution.py:337
  58.8 13.1 %collective-permute-start.21 = (bf16[2,592,128]{2,1,0:T(8,128)(2,1)S(1)}, bf16[2,592,128]{2,1,0:T(8,128)(2,1)S(1)}, u32[]{:S(2)}, u32[]{:S(2)}) collective-permute-start(bf16[2,592,128]{2,1,0:T(8,128)(2,1)S(1)} %collective-permute-done.20.m2), channel_id=1, source_target_pairs={{0,14},{2,0},{4,2},{6,4},{8,6},{10,8},{12,10},{14,12},{1,15},{3,1}... | collective-permute-start | bytes 909320 | tf_op jit(solution)/shard_map/ppermute | solution.py:337
  62.6 19.8 %collective-permute-start.6 = (bf16[2,592,128]{2,1,0:T(8,128)(2,1)}, bf16[2,592,128]{2,1,0:T(8,128)(2,1)S(1)}, u32[]{:S(2)}, u32[]{:S(2)}) collective-permute-start(bf16[2,592,128]{2,1,0:T(8,128)(2,1)} %collective-permute-done.5.m2), channel_id=1, source_target_pairs={{0,14},{2,0},{4,2},{6,4},{8,6},{10,8},{12,10},{14,12},{1,15},{3,1}... | collective-permute-start | bytes 909320 | tf_op jit(solution)/shard_map/ppermute | solution.py:337
  66.1 16.3 %collective-permute-start.7 = (bf16[2,592,128]{2,1,0:T(8,128)(2,1)S(1)}, bf16[2,592,128]{2,1,0:T(8,128)(2,1)S(1)}, u32[]{:S(2)}, u32[]{:S(2)}) collective-permute-start(bf16[2,592,128]{2,1,0:T(8,128)(2,1)S(1)} %collective-permute-done.3.p3), channel_id=1, source_target_pairs={{0,2},{2,4},{4,6},{6,8},{8,10},{10,12},{12,14},{14,0},{1,3},{3,5},... | collective-permute-start | bytes 909320 | tf_op jit(solution)/shard_map/ppermute | solution.py:337
  71.8 28.3 %collective-permute-start.18 = (bf16[2,592,128]{2,1,0:T(8,128)(2,1)}, bf16[2,592,128]{2,1,0:T(8,128)(2,1)S(1)}, u32[]{:S(2)}, u32[]{:S(2)}) collective-permute-start(bf16[2,592,128]{2,1,0:T(8,128)(2,1)} %collective-permute-done.17.p2), channel_id=1, source_target_pairs={{0,2},{2,4},{4,6},{6,8},{8,10},{10,12},{12,14},{14,0},{1,3},{3,5},... | collective-permute-start | bytes 909320 | tf_op jit(solution)/shard_map/ppermute | solution.py:337
  71.8 28.3 %collective-permute-start.22 = (bf16[2,592,128]{2,1,0:T(8,128)(2,1)S(1)}, bf16[2,592,128]{2,1,0:T(8,128)(2,1)S(1)}, u32[]{:S(2)}, u32[]{:S(2)}) collective-permute-start(bf16[2,592,128]{2,1,0:T(8,128)(2,1)S(1)} %collective-permute-done.21.m3), channel_id=1, source_target_pairs={{0,14},{2,0},{4,2},{6,4},{8,6},{10,8},{12,10},{14,12},{1,15},{3,1}... | collective-permute-start | bytes 909320 | tf_op jit(solution)/shard_map/ppermute | solution.py:337
  90.6 20.6 %collective-permute-start.9 = (bf16[2,576,128]{2,1,0:T(8,128)(2,1)S(1)}, bf16[2,576,128]{2,1,0:T(8,128)(2,1)S(1)}, u32[]{:S(2)}, u32[]{:S(2)}) collective-permute-start(bf16[2,576,128]{2,1,0:T(8,128)(2,1)S(1)} %get-tuple-element.36), channel_id=1, source_target_pairs={{0,2},{2,4},{4,6},{6,8},{8,10},{10,12},{12,14},{14,0},{1,3},{3,5},... | collective-permute-start | bytes 884744 | tf_op jit(solution)/shard_map/ppermute | solution.py:337
  90.7 20.7 %collective-permute-start.13 = (bf16[2,576,128]{2,1,0:T(8,128)(2,1)S(1)}, bf16[2,576,128]{2,1,0:T(8,128)(2,1)S(1)}, u32[]{:S(2)}, u32[]{:S(2)}) collective-permute-start(bf16[2,576,128]{2,1,0:T(8,128)(2,1)S(1)} %get-tuple-element.39), channel_id=1, source_target_pairs={{0,14},{2,0},{4,2},{6,4},{8,6},{10,8},{12,10},{14,12},{1,15},{3,1}... | collective-permute-start | bytes 884744 | tf_op jit(solution)/shard_map/ppermute | solution.py:337
  108.4 6.9 %collective-permute-start.23 = (bf16[2,576,128]{2,1,0:T(8,128)(2,1)S(1)}, bf16[2,576,128]{2,1,0:T(8,128)(2,1)S(1)}, u32[]{:S(2)}, u32[]{:S(2)}) collective-permute-start(bf16[2,576,128]{2,1,0:T(8,128)(2,1)S(1)} %get-tuple-element.45), channel_id=1, source_target_pairs={{0,2},{2,4},{4,6},{6,8},{8,10},{10,12},{12,14},{14,0},{1,3},{3,5},... | collective-permute-start | bytes 884744 | tf_op jit(solution)/shard_map/ppermute | solution.py:337
  108.5 6.9 %collective-permute-start.26 = (bf16[2,576,128]{2,1,0:T(8,128)(2,1)S(1)}, bf16[2,576,128]{2,1,0:T(8,128)(2,1)S(1)}, u32[]{:S(2)}, u32[]{:S(2)}) collective-permute-start(bf16[2,576,128]{2,1,0:T(8,128)(2,1)S(1)} %get-tuple-element.49), channel_id=1, source_target_pairs={{0,14},{2,0},{4,2},{6,4},{8,6},{10,8},{12,10},{14,12},{1,15},{3,1}... | collective-permute-start | bytes 884744 | tf_op jit(solution)/shard_map/ppermute | solution.py:337
  111.3 7.2 %collective-permute-start.10 = (bf16[2,576,128]{2,1,0:T(8,128)(2,1)S(1)}, bf16[2,576,128]{2,1,0:T(8,128)(2,1)S(1)}, u32[]{:S(2)}, u32[]{:S(2)}) collective-permute-start(bf16[2,576,128]{2,1,0:T(8,128)(2,1)S(1)} %add_convert_fusion.11), channel_id=1, source_target_pairs={{0,2},{2,4},{4,6},{6,8},{8,10},{10,12},{12,14},{14,0},{1,3},{3,5},... | collective-permute-start | bytes 884744 | tf_op jit(solution)/shard_map/ppermute | solution.py:337
  111.5 7.2 %collective-permute-start.14 = (bf16[2,576,128]{2,1,0:T(8,128)(2,1)S(1)}, bf16[2,576,128]{2,1,0:T(8,128)(2,1)S(1)}, u32[]{:S(2)}, u32[]{:S(2)}) collective-permute-start(bf16[2,576,128]{2,1,0:T(8,128)(2,1)S(1)} %add_convert_fusion.8), channel_id=1, source_target_pairs={{0,14},{2,0},{4,2},{6,4},{8,6},{10,8},{12,10},{14,12},{1,15},{3,1}... | collective-permute-start | bytes 884744 | tf_op jit(solution)/shard_map/ppermute | solution.py:337
  115.4 16.8 %collective-permute-start.24 = (bf16[2,576,128]{2,1,0:T(8,128)(2,1)S(1)}, bf16[2,576,128]{2,1,0:T(8,128)(2,1)S(1)}, u32[]{:S(2)}, u32[]{:S(2)}) collective-permute-start(bf16[2,576,128]{2,1,0:T(8,128)(2,1)S(1)} %add_convert_fusion.5), channel_id=1, source_target_pairs={{0,2},{2,4},{4,6},{6,8},{8,10},{10,12},{12,14},{14,0},{1,3},{3,5},... | collective-permute-start | bytes 884744 | tf_op jit(solution)/shard_map/ppermute | solution.py:337
  115.6 9.8 %collective-permute-start.27 = (bf16[2,576,128]{2,1,0:T(8,128)(2,1)S(1)}, bf16[2,576,128]{2,1,0:T(8,128)(2,1)S(1)}, u32[]{:S(2)}, u32[]{:S(2)}) collective-permute-start(bf16[2,576,128]{2,1,0:T(8,128)(2,1)S(1)} %add_convert_fusion.3), channel_id=1, source_target_pairs={{0,14},{2,0},{4,2},{6,4},{8,6},{10,8},{12,10},{14,12},{1,15},{3,1}... | collective-permute-start | bytes 884744 | tf_op jit(solution)/shard_map/ppermute | solution.py:337
  118.6 13.4 %collective-permute-start.11 = (bf16[2,576,128]{2,1,0:T(8,128)(2,1)S(1)}, bf16[2,576,128]{2,1,0:T(8,128)(2,1)S(1)}, u32[]{:S(2)}, u32[]{:S(2)}) collective-permute-start(bf16[2,576,128]{2,1,0:T(8,128)(2,1)S(1)} %add_convert_fusion.10), channel_id=1, source_target_pairs={{0,2},{2,4},{4,6},{6,8},{8,10},{10,12},{12,14},{14,0},{1,3},{3,5},... | collective-permute-start | bytes 884744 | tf_op jit(solution)/shard_map/ppermute | solution.py:337
  118.8 22.8 %collective-permute-start.15 = (bf16[2,576,128]{2,1,0:T(8,128)(2,1)S(1)}, bf16[2,576,128]{2,1,0:T(8,128)(2,1)S(1)}, u32[]{:S(2)}, u32[]{:S(2)}) collective-permute-start(bf16[2,576,128]{2,1,0:T(8,128)(2,1)S(1)} %add_convert_fusion.7), channel_id=1, source_target_pairs={{0,14},{2,0},{4,2},{6,4},{8,6},{10,8},{12,10},{14,12},{1,15},{3,1}... | collective-permute-start | bytes 884744 | tf_op jit(solution)/shard_map/ppermute | solution.py:337
  125.4 12.6 %collective-permute-start.28 = (bf16[2,576,128]{2,1,0:T(8,128)(2,1)S(1)}, bf16[2,576,128]{2,1,0:T(8,128)(2,1)S(1)}, u32[]{:S(2)}, u32[]{:S(2)}) collective-permute-start(bf16[2,576,128]{2,1,0:T(8,128)(2,1)S(1)} %add_convert_fusion.2), channel_id=1, source_target_pairs={{0,14},{2,0},{4,2},{6,4},{8,6},{10,8},{12,10},{14,12},{1,15},{3,1}... | collective-permute-start | bytes 884744 | tf_op jit(solution)/shard_map/ppermute | solution.py:337
  132.1 9.7 %collective-permute-start.12 = (bf16[2,576,128]{2,1,0:T(8,128)(2,1)S(1)}, bf16[2,576,128]{2,1,0:T(8,128)(2,1)S(1)}, u32[]{:S(2)}, u32[]{:S(2)}) collective-permute-start(bf16[2,576,128]{2,1,0:T(8,128)(2,1)S(1)} %add_convert_fusion.9), channel_id=1, source_target_pairs={{0,2},{2,4},{4,6},{6,8},{8,10},{10,12},{12,14},{14,0},{1,3},{3,5},... | collective-permute-start | bytes 884744 | tf_op jit(solution)/shard_map/ppermute | solution.py:337
  132.3 12.7 %collective-permute-start.25 = (bf16[2,576,128]{2,1,0:T(8,128)(2,1)S(1)}, bf16[2,576,128]{2,1,0:T(8,128)(2,1)S(1)}, u32[]{:S(2)}, u32[]{:S(2)}) collective-permute-start(bf16[2,576,128]{2,1,0:T(8,128)(2,1)S(1)} %add_convert_fusion.4), channel_id=1, source_target_pairs={{0,2},{2,4},{4,6},{6,8},{8,10},{10,12},{12,14},{14,0},{1,3},{3,5},... | collective-permute-start | bytes 884744 | tf_op jit(solution)/shard_map/ppermute | solution.py:337
  138.1 9.8 %collective-permute-start.29 = (bf16[2,576,128]{2,1,0:T(8,128)(2,1)S(1)}, bf16[2,576,128]{2,1,0:T(8,128)(2,1)S(1)}, u32[]{:S(2)}, u32[]{:S(2)}) collective-permute-start(bf16[2,576,128]{2,1,0:T(8,128)(2,1)S(1)} %add_convert_fusion.1), channel_id=1, source_target_pairs={{0,14},{2,0},{4,2},{6,4},{8,6},{10,8},{12,10},{14,12},{1,15},{3,1}... | collective-permute-start | bytes 884744 | tf_op jit(solution)/shard_map/ppermute | solution.py:337
  148.0 42.1 %copy-start.3 = (bf16[128]{0:T(256)(128)(2,1)S(1)}, bf16[128]{0:T(256)(128)(2,1)}, u32[]{:S(2)}) copy-start(bf16[128]{0:T(256)(128)(2,1)} %param.15) | copy-start | bytes 772
  (4 other events, 51.1 us)

commit v2 on v1

--- a/solution.py
+++ b/solution.py
@@ -9,7 +9,7 @@
 EPS = 1e-06
 LANES = 128
 CHUNKS = 2
-EXTRA = 16
+EXTRA = 8
 MIB = 1024 * 1024
 UP_VMEM = 46 * MIB
 PART_VMEM = 46 * MIB
@@ -64,7 +64,7 @@
         out_ref[pl.ds(start, step), :] = jnp.dot(pick, tok, preferred_element_type=F32).astype(BF16)
         return carry
 
-    lax.fori_loop(0, out_ref.shape[0] // step, one, 0, unroll=2)
+    lax.fori_loop(0, out_ref.shape[0] // step, one, 0, unroll=4)
 
 
 def combine_kernel(ret_ref, pos_ref, out_ref, square_ref):
@@ -87,7 +87,7 @@
         square_ref[:, pl.ds(b, 1), :] = jnp.broadcast_to(row[None], (square_ref.shape[0], 1, LANES))
         return carry
 
-    lax.fori_loop(0, rows // block, one, 0, unroll=2)
+    lax.fori_loop(0, rows // block, one, 0, unroll=4)
 
 
 def finish_kernel(comb_ref, squares_ref, gain_ref, out_ref):
@@ -132,21 +132,20 @@
         pltpu.make_async_copy(src.at[pl.ds(2 * blocks, blocks)], scr.at[:, n], sem).start()
 
 
-def gained(piece_scr, x_scr, sums_ref, start_sums):
-    count = piece_scr.shape[0]
+def gained(pieces, x_scr, sums_ref, start_sums):
     rows = x_scr.shape[0]
     tile = 32
     gains = [
-        [piece_scr[j, c, pl.ds(rows, EXTRA), :].astype(F32)[0:1, :] for c in range(2)]
-        for j in range(count)
+        [piece[c, pl.ds(rows, EXTRA), :].astype(F32)[0:1, :] for c in range(2)]
+        for piece in pieces
     ]
 
     def one(t, carry):
         span = pl.ds(pl.multiple_of(t * tile, tile), tile)
         acc = jnp.zeros((tile, LANES), F32) if start_sums is None else start_sums[span, :]
-        for j in range(count):
+        for j, piece in enumerate(pieces):
             for c in range(2):
-                v = piece_scr[j, c, span, :].astype(F32)
+                v = piece[c, span, :].astype(F32)
                 acc = acc + v * v
                 x_scr[span, (2 * j + c) * LANES : (2 * j + c + 1) * LANES] = (
                     v * gains[j][c]
@@ -168,19 +167,15 @@
     )
 
 
-def load_pieces(given, piece_scr, sem):
-    for j, src in enumerate(given):
-        pltpu.make_async_copy(src, piece_scr.at[j], sem).start()
-
-
 def part_kernel(
     z_ref, x0, p1, m1, p2, m2, own, other, acc_ref, sums_ref, piece_scr, x_scr, in_scr, sems
 ):
     order = near(z_ref)
-    load_pieces((x0, p1, m1, p2, m2), piece_scr, sems.at[0])
+    for j, src in enumerate((x0, p1, m1, p2, m2)):
+        pltpu.make_async_copy(src, piece_scr.at[j], sems.at[0]).start()
     load_in(own, other, in_scr, [order[j] for j in EARLY], sems.at[1])
     pltpu.make_async_copy(piece_scr, piece_scr, sems.at[0]).wait()
-    gained(piece_scr, x_scr, sums_ref, None)
+    gained([piece_scr.at[j] for j in range(len(EARLY))], x_scr, sums_ref, None)
     pltpu.make_async_copy(in_scr, in_scr, sems.at[1]).wait()
 
     def one(n, carry):
@@ -210,15 +205,13 @@
 def up_kernel(
     z_ref, p3, m3, x4, acc_ref, sums_ref, own, other,
     o4, op3, om3, op2, om2, op1, om1, o0,
-    piece_scr, x_scr, scale_scr, in_scr, down_scr, h_ref, sems,
+    x_scr, scale_scr, in_scr, down_scr, h_ref, sems,
 ):
     order = near(z_ref)
-    load_pieces((p3, m3, x4), piece_scr, sems.at[0])
-    load_in(own, other, in_scr, [order[j] for j in LATE], sems.at[1])
-    load_down(own, other, down_scr, sems.at[2])
-    pltpu.make_async_copy(piece_scr, piece_scr, sems.at[0]).wait()
-    gained(piece_scr, x_scr, scale_scr, sums_ref)
-    pltpu.make_async_copy(in_scr, in_scr, sems.at[1]).wait()
+    load_in(own, other, in_scr, [order[j] for j in LATE], sems.at[0])
+    load_down(own, other, down_scr, sems.at[1])
+    gained((p3, m3, x4), x_scr, scale_scr, sums_ref)
+    pltpu.make_async_copy(in_scr, in_scr, sems.at[0]).wait()
 
     def one(n, carry):
         both = product(x_scr, in_scr, n) + acc_ref[n]
@@ -229,8 +222,8 @@
         h_ref[:, pl.ds(pl.multiple_of(n * LANES, LANES), LANES)] = hidden
         return carry
 
-    lax.fori_loop(0, in_scr.shape[0], one, 0)
-    pltpu.make_async_copy(down_scr, down_scr, sems.at[2]).wait()
+    lax.fori_loop(0, in_scr.shape[0], one, 0, unroll=True)
+    pltpu.make_async_copy(down_scr, down_scr, sems.at[1]).wait()
     put_down(h_ref, down_scr, order, zip(FAR_FIRST, (o4, op3, om3, op2, om2, op1, om1, o0)))
 
 
@@ -270,17 +263,16 @@
     o4, op3, om3, op2, om2, op1, om1, o0 = pl.pallas_call(
         up_kernel,
         name="ffn_up",
-        in_specs=[sm] + [hbm] * late + [vm] * 2 + [hbm] * 2,
+        in_specs=[sm] + [vm] * (late + 2) + [hbm] * 2,
         out_specs=[vm] * 8,
         out_shape=[full] * 8,
         scratch_shapes=[
-            pltpu.VMEM((late, 2, rows + EXTRA, LANES), BF16),
             pltpu.VMEM((rows, late * 256), BF16),
             pltpu.VMEM((rows, LANES), F32),
             pltpu.VMEM((blocks, 4, UNITS, late * 256), BF16),
             pltpu.VMEM((blocks, 2, UNITS, D), BF16),
             pltpu.VMEM((rows, 2 * hidden), BF16),
-            pltpu.SemaphoreType.DMA((3,)),
+            pltpu.SemaphoreType.DMA((2,)),
         ],
         cost_estimate=pl.CostEstimate(
             flops=2 * wide * late // 8 + wide,

time: 191 us -> 188 us (0.984)
  Pallas kernels: 46.2 us -> 42.3 us
    pallas_call x2, Pallas kernels: 16.4 us -> 13.8 us  [ffn(): pl.pallas_call(up_kernel, name='ffn_up', in_specs=[sm] + [vm] * (late + 2...]
  transfers between devices with their start and end apart: 31 -> 31, of which waited for: 14 -> 15; matrix products, arithmetic and copies ran while one was open for 1% -> 1% of each run, Pallas kernels for 19% -> 18%
where the time goes in v2:
time: 188 us; the launch traced here: 187 us
  starting transfers between devices  52.5 us (28%)
  waiting for transfers between devices  50.7 us (27%)
  Pallas kernels  42.3 us (22%)
  blocking collectives  38.5 us (20%)
    ppermute x30, starting transfers between devices, turn(): lax.ppermute(value, axis, [(i, (i + by) % count) for i in range(count)])  47 us
    ppermute x30, waiting for transfers between devices, turn(): lax.ppermute(value, axis, [(i, (i + by) % count) for i in range(count)])  40.3 us
    all_to_all x1, blocking collectives, layer(): lax.all_to_all(result.reshape(2 * groups, half, LANES), exchange, 0, 0, t...  23 us
    all_to_all x1, blocking collectives, layer(): gathered = lax.all_to_all(squares, ('z', 'c'), 0, 0, tiled=True)  15.5 us
    pallas_call x2, Pallas kernels, ffn(): pl.pallas_call(up_kernel, name='ffn_up', in_specs=[sm] + [vm] * (late + 2...  13.8 us
    pallas_call x2, Pallas kernels, ffn(): pl.pallas_call(part_kernel, name='ffn_part', in_specs=[sm] + [hbm] * (ear...  13.6 us
    all_to_all x1, waiting for transfers between devices, layer(): lax.all_to_all(outgoing.reshape(2 * groups, half, LANES), exchange, 0, 0,...  10.4 us
    pallas_call x1, Pallas kernels, layer(): pl.pallas_call(route_kernel, name='route', compiler_params=pltpu.Compiler...  6.53 us
  transfers between devices with their start and end apart: 31, of which 15 were waited for; matrix products, arithmetic and copies ran while one was open for 1% of the time, Pallas kernels for 18%

profile of v2, /device:TPU:1, one launch (start us, length us, event | category | flops | bytes accessed | tf_op | source)
XLA Modules:
  0.0 187.3 jit_solution(16945088906177156242)
XLA Ops:
  0.0 4.3 %join.1 = bf16[1344,2048]{1,0:T(8,128)(2,1)} custom-call(bf16[448,2048]{1,0:T(8,128)(2,1)} %bitcast.26, bf16[448,2048]{1,0:T(8,128)(2,1)} %bitcast.27, bf16[448,2048]{1,0:T(8,128)(2,1)} %bitcast.28), custom_call_target="tpu_custom_call" | custom-call | tf_op jit(solution)/shard_map/join/pallas_call | solution.py:312
  4.3 3.3 %collective-permute-start.8 = (bf16[1344,2048]{1,0:T(8,128)(2,1)}, bf16[1344,2048]{1,0:T(8,128)(2,1)}, u32[]{:S(2)}, u32[]{:S(2)}) collective-permute-start(bf16[1344,2048]{1,0:T(8,128)(2,1)} %join.1), channel_id=1, source_target_pairs={{0,1},{1,0},{2,3},{3,2},{4,5},{5,4},{6,7},{7,6},{8,9},{9,8},{10,11... | collective-permute-start | bytes 16515080 | tf_op jit(solution)/shard_map/ppermute | solution.py:329
  7.6 6.5 %route.1 = (bf16[2304,128]{1,0:T(8,128)(2,1)}, f32[1024,128]{1,0:T(8,128)}) custom-call(s32[2,1024]{1,0:T(2,128)} %bitcast.30, f32[2,1024]{1,0:T(2,128)} %bitcast.31, bf16[1024,128]{1,0:T(8,128)(2,1)} %tok_ref.1), custom_call_target="tpu_custom_call" | custom-call | tf_op jit(solution)/shard_map/route/pallas_call | solution.py:380
  14.1 5.5 %all-to-all-start = ((bf16[32,72,128]{2,1,0:T(8,128)(2,1)}), bf16[32,72,128]{2,1,0:T(8,128)(2,1)S(1)}, u32[]{:S(2)}, u32[]{:S(2)}) async-start(bf16[32,72,128]{2,1,0:T(8,128)(2,1)} %bitcast.29), calls=%async_computation | async-start | bytes 1179648 | tf_op jit(solution)/shard_map/all_to_all | solution.py:391
  20.9 10.4 %all-to-all-done = bf16[32,72,128]{2,1,0:T(8,128)(2,1)S(1)} async-done(((bf16[32,72,128]{2,1,0:T(8,128)(2,1)}), bf16[32,72,128]{2,1,0:T(8,128)(2,1)S(1)}, u32[]{:S(2)}, u32[]{:S(2)}) %all-to-all-start) | async-done | bytes 589856 | tf_op jit(solution)/shard_map/all_to_all | solution.py:391
  33.1 4.0 %collective-permute-start.19 = (bf16[2,584,128]{2,1,0:T(8,128)(2,1)S(1)}, bf16[2,584,128]{2,1,0:T(8,128)(2,1)S(1)}, u32[]{:S(2)}, u32[]{:S(2)}) collective-permute-start(bf16[2,584,128]{2,1,0:T(8,128)(2,1)S(1)} %get-tuple-element.56.x0), channel_id=1, source_target_pairs={{0,14},{2,0},{4,2},{6,4},{8,6},{10,8},{12,10},{14,12},{1,15},{3,1}... | collective-permute-start | bytes 897032 | tf_op jit(solution)/shard_map/ppermute | solution.py:329
  38.5 4.9 %collective-permute-done.1.p1 = bf16[2,584,128]{2,1,0:T(8,128)(2,1)S(1)} collective-permute-done((bf16[2,584,128]{2,1,0:T(8,128)(2,1)S(1)}, bf16[2,584,128]{2,1,0:T(8,128)(2,1)S(1)}, u32[]{:S(2)}, u32[]{:S(2)}) %collective-permute-start.1) | collective-permute-done | bytes 299040 | tf_op jit(solution)/shard_map/ppermute | solution.py:329
  43.4 2.7 %collective-permute-start.20 = (bf16[2,584,128]{2,1,0:T(8,128)(2,1)S(1)}, bf16[2,584,128]{2,1,0:T(8,128)(2,1)S(1)}, u32[]{:S(2)}, u32[]{:S(2)}) collective-permute-start(bf16[2,584,128]{2,1,0:T(8,128)(2,1)S(1)} %collective-permute-done.19.m1), channel_id=1, source_target_pairs={{0,14},{2,0},{4,2},{6,4},{8,6},{10,8},{12,10},{14,12},{1,15},{3,1}... | collective-permute-start | bytes 897032 | tf_op jit(solution)/shard_map/ppermute | solution.py:329
  46.1 2.8 %collective-permute-done.4.m1 = bf16[2,584,128]{2,1,0:T(8,128)(2,1)S(1)} collective-permute-done((bf16[2,584,128]{2,1,0:T(8,128)(2,1)S(1)}, bf16[2,584,128]{2,1,0:T(8,128)(2,1)S(1)}, u32[]{:S(2)}, u32[]{:S(2)}) %collective-permute-start.4) | collective-permute-done | bytes 299040 | tf_op jit(solution)/shard_map/ppermute | solution.py:329
  48.9 3.4 %collective-permute-start.5 = (bf16[2,584,128]{2,1,0:T(8,128)(2,1)S(1)}, bf16[2,584,128]{2,1,0:T(8,128)(2,1)}, u32[]{:S(2)}, u32[]{:S(2)}) collective-permute-start(bf16[2,584,128]{2,1,0:T(8,128)(2,1)S(1)} %collective-permute-done.4.m1), channel_id=1, source_target_pairs={{0,14},{2,0},{4,2},{6,4},{8,6},{10,8},{12,10},{14,12},{1,15},{3,1}... | collective-permute-start | bytes 897032 | tf_op jit(solution)/shard_map/ppermute | solution.py:329
  53.0 4.9 %collective-permute-done.16.p1 = bf16[2,584,128]{2,1,0:T(8,128)(2,1)S(1)} collective-permute-done((bf16[2,584,128]{2,1,0:T(8,128)(2,1)S(1)}, bf16[2,584,128]{2,1,0:T(8,128)(2,1)S(1)}, u32[]{:S(2)}, u32[]{:S(2)}) %collective-permute-start.16) | collective-permute-done | bytes 299040 | tf_op jit(solution)/shard_map/ppermute | solution.py:329
  57.9 2.7 %collective-permute-start.21 = (bf16[2,584,128]{2,1,0:T(8,128)(2,1)S(1)}, bf16[2,584,128]{2,1,0:T(8,128)(2,1)S(1)}, u32[]{:S(2)}, u32[]{:S(2)}) collective-permute-start(bf16[2,584,128]{2,1,0:T(8,128)(2,1)S(1)} %collective-permute-done.20.m2), channel_id=1, source_target_pairs={{0,14},{2,0},{4,2},{6,4},{8,6},{10,8},{12,10},{14,12},{1,15},{3,1}... | collective-permute-start | bytes 897032 | tf_op jit(solution)/shard_map/ppermute | solution.py:329
  61.7 3.5 %collective-permute-start.6 = (bf16[2,584,128]{2,1,0:T(8,128)(2,1)}, bf16[2,584,128]{2,1,0:T(8,128)(2,1)S(1)}, u32[]{:S(2)}, u32[]{:S(2)}) collective-permute-start(bf16[2,584,128]{2,1,0:T(8,128)(2,1)} %collective-permute-done.5.m2), channel_id=1, source_target_pairs={{0,14},{2,0},{4,2},{6,4},{8,6},{10,8},{12,10},{14,12},{1,15},{3,1}... | collective-permute-start | bytes 897032 | tf_op jit(solution)/shard_map/ppermute | solution.py:329
  65.2 5.6 %collective-permute-done.17.p2 = bf16[2,584,128]{2,1,0:T(8,128)(2,1)} collective-permute-done((bf16[2,584,128]{2,1,0:T(8,128)(2,1)S(1)}, bf16[2,584,128]{2,1,0:T(8,128)(2,1)}, u32[]{:S(2)}, u32[]{:S(2)}) %collective-permute-start.17) | collective-permute-done | bytes 299040 | tf_op jit(solution)/shard_map/ppermute | solution.py:329
  70.8 2.7 %collective-permute-start.22 = (bf16[2,584,128]{2,1,0:T(8,128)(2,1)S(1)}, bf16[2,584,128]{2,1,0:T(8,128)(2,1)S(1)}, u32[]{:S(2)}, u32[]{:S(2)}) collective-permute-start(bf16[2,584,128]{2,1,0:T(8,128)(2,1)S(1)} %collective-permute-done.21.m3), channel_id=1, source_target_pairs={{0,14},{2,0},{4,2},{6,4},{8,6},{10,8},{12,10},{14,12},{1,15},{3,1}... | collective-permute-start | bytes 897032 | tf_op jit(solution)/shard_map/ppermute | solution.py:329
  74.5 6.8 %ffn_part.2 = (f32[7,576,256]{2,1,0:T(8,128)S(1)}, f32[576,128]{1,0:T(8,128)S(1)}) custom-call(s32[1]{0:T(128)} %bitcast.z_ref, bf16[2,584,128]{2,1,0:T(8,128)(2,1)S(1)} %get-tuple-element.55.x0, bf16[2,584,128]{2,1,0:T(8,128)(2,1)S(1)} %collective-permute-done.1.p1, bf16[2,584,128]{2,1,0:T(8,128)(2,1)S(1)} %collective-permute-done.4.m1, ...), custom_call_target="tpu_custom_call" | custom-call | flops 2642411520 | bytes 9306112 | tf_op jit(solution)/shard_map/ffn_part/pallas_call | solution.py:241
  81.4 6.9 %ffn_up.2 = (bf16[2,576,128]{2,1,0:T(8,128)(2,1)S(1)}, bf16[2,576,128]{2,1,0:T(8,128)(2,1)S(1)}, bf16[2,576,128]{2,1,0:T(8,128)(2,1)S(1)}, bf16[2,576,128]{2,1,0...) custom-call(s32[1]{0:T(128)} %bitcast.z_ref, ...), custom_call_target="tpu_custom_call" | custom-call | flops 3699376128 | bytes 11141120 | tf_op jit(solution)/shard_map/ffn_up/pallas_call | solution.py:263
  91.0 6.8 %ffn_part.3 = (f32[7,576,256]{2,1,0:T(8,128)S(1)}, f32[576,128]{1,0:T(8,128)S(1)}) custom-call(s32[1]{0:T(128)} %bitcast.z_ref, bf16[2,584,128]{2,1,0:T(8,128)(2,1)S(1)} %get-tuple-element.56.x0, bf16[2,584,128]{2,1,0:T(8,128)(2,1)S(1)} %collective-permute-done.16.p1, bf16[2,584,128]{2,1,0:T(8,128)(2,1)S(1)} %collective-permute-done.19.m1, ...), custom_call_target="tpu_custom_call" | custom-call | flops 2642411520 | bytes 9306112 | tf_op jit(solution)/shard_map/ffn_part/pallas_call | solution.py:241
  97.9 6.9 %ffn_up.3 = (bf16[2,576,128]{2,1,0:T(8,128)(2,1)S(1)}, bf16[2,576,128]{2,1,0:T(8,128)(2,1)S(1)}, bf16[2,576,128]{2,1,0:T(8,128)(2,1)S(1)}, bf16[2,576,128]{2,1,0...) custom-call(s32[1]{0:T(128)} %bitcast.z_ref, ...), custom_call_target="tpu_custom_call" | custom-call | flops 3699376128 | bytes 11141120 | tf_op jit(solution)/shard_map/ffn_up/pallas_call | solution.py:263
  108.0 2.7 %collective-permute-start.14 = (bf16[2,576,128]{2,1,0:T(8,128)(2,1)S(1)}, bf16[2,576,128]{2,1,0:T(8,128)(2,1)S(1)}, u32[]{:S(2)}, u32[]{:S(2)}) collective-permute-start(bf16[2,576,128]{2,1,0:T(8,128)(2,1)S(1)} %add_convert_fusion.8), channel_id=1, source_target_pairs={{0,14},{2,0},{4,2},{6,4},{8,6},{10,8},{12,10},{14,12},{1,15},{3,1}... | collective-permute-start | bytes 884744 | tf_op jit(solution)/shard_map/ppermute | solution.py:329
  111.9 2.7 %collective-permute-start.27 = (bf16[2,576,128]{2,1,0:T(8,128)(2,1)S(1)}, bf16[2,576,128]{2,1,0:T(8,128)(2,1)S(1)}, u32[]{:S(2)}, u32[]{:S(2)}) collective-permute-start(bf16[2,576,128]{2,1,0:T(8,128)(2,1)S(1)} %add_convert_fusion.3), channel_id=1, source_target_pairs={{0,14},{2,0},{4,2},{6,4},{8,6},{10,8},{12,10},{14,12},{1,15},{3,1}... | collective-permute-start | bytes 884744 | tf_op jit(solution)/shard_map/ppermute | solution.py:329
  115.1 2.7 %collective-permute-start.15 = (bf16[2,576,128]{2,1,0:T(8,128)(2,1)S(1)}, bf16[2,576,128]{2,1,0:T(8,128)(2,1)S(1)}, u32[]{:S(2)}, u32[]{:S(2)}) collective-permute-start(bf16[2,576,128]{2,1,0:T(8,128)(2,1)S(1)} %add_convert_fusion.7), channel_id=1, source_target_pairs={{0,14},{2,0},{4,2},{6,4},{8,6},{10,8},{12,10},{14,12},{1,15},{3,1}... | collective-permute-start | bytes 884744 | tf_op jit(solution)/shard_map/ppermute | solution.py:329
  117.8 3.7 %collective-permute-done.27 = bf16[2,576,128]{2,1,0:T(8,128)(2,1)S(1)} collective-permute-done((bf16[2,576,128]{2,1,0:T(8,128)(2,1)S(1)}, bf16[2,576,128]{2,1,0:T(8,128)(2,1)S(1)}, u32[]{:S(2)}, u32[]{:S(2)}) %collective-permute-start.27) | collective-permute-done | bytes 294944 | tf_op jit(solution)/shard_map/ppermute | solution.py:329
  121.5 3.5 %collective-permute-start.28 = (bf16[2,576,128]{2,1,0:T(8,128)(2,1)S(1)}, bf16[2,576,128]{2,1,0:T(8,128)(2,1)S(1)}, u32[]{:S(2)}, u32[]{:S(2)}) collective-permute-start(bf16[2,576,128]{2,1,0:T(8,128)(2,1)S(1)} %add_convert_fusion.2), channel_id=1, source_target_pairs={{0,14},{2,0},{4,2},{6,4},{8,6},{10,8},{12,10},{14,12},{1,15},{3,1}... | collective-permute-start | bytes 884744 | tf_op jit(solution)/shard_map/ppermute | solution.py:329
  125.0 3.3 %collective-permute-done.11 = bf16[2,576,128]{2,1,0:T(8,128)(2,1)S(1)} collective-permute-done((bf16[2,576,128]{2,1,0:T(8,128)(2,1)S(1)}, bf16[2,576,128]{2,1,0:T(8,128)(2,1)S(1)}, u32[]{:S(2)}, u32[]{:S(2)}) %collective-permute-start.11) | collective-permute-done | bytes 294944 | tf_op jit(solution)/shard_map/ppermute | solution.py:329
  128.7 5.4 %collective-permute-done.28 = bf16[2,576,128]{2,1,0:T(8,128)(2,1)S(1)} collective-permute-done((bf16[2,576,128]{2,1,0:T(8,128)(2,1)S(1)}, bf16[2,576,128]{2,1,0:T(8,128)(2,1)S(1)}, u32[]{:S(2)}, u32[]{:S(2)}) %collective-permute-start.28) | collective-permute-done | bytes 294944 | tf_op jit(solution)/shard_map/ppermute | solution.py:329
  134.2 3.5 %collective-permute-start.29 = (bf16[2,576,128]{2,1,0:T(8,128)(2,1)S(1)}, bf16[2,576,128]{2,1,0:T(8,128)(2,1)S(1)}, u32[]{:S(2)}, u32[]{:S(2)}) collective-permute-start(bf16[2,576,128]{2,1,0:T(8,128)(2,1)S(1)} %add_convert_fusion.1), channel_id=1, source_target_pairs={{0,14},{2,0},{4,2},{6,4},{8,6},{10,8},{12,10},{14,12},{1,15},{3,1}... | collective-permute-start | bytes 884744 | tf_op jit(solution)/shard_map/ppermute | solution.py:329
  138.3 3.0 %collective-permute-done.25 = bf16[2,576,128]{2,1,0:T(8,128)(2,1)S(1)} collective-permute-done((bf16[2,576,128]{2,1,0:T(8,128)(2,1)S(1)}, bf16[2,576,128]{2,1,0:T(8,128)(2,1)S(1)}, u32[]{:S(2)}, u32[]{:S(2)}) %collective-permute-start.25) | collective-permute-done | bytes 294944 | tf_op jit(solution)/shard_map/ppermute | solution.py:329
  141.3 3.2 %collective-permute-done.29 = bf16[2,576,128]{2,1,0:T(8,128)(2,1)S(1)} collective-permute-done((bf16[2,576,128]{2,1,0:T(8,128)(2,1)S(1)}, bf16[2,576,128]{2,1,0:T(8,128)(2,1)S(1)}, u32[]{:S(2)}, u32[]{:S(2)}) %collective-permute-start.29) | collective-permute-done | bytes 294944 | tf_op jit(solution)/shard_map/ppermute | solution.py:329
  144.7 23.0 %all_to_all.15 = bf16[32,72,128]{2,1,0:T(8,128)(2,1)S(1)} all-to-all(bf16[32,72,128]{2,1,0:T(8,128)(2,1)S(1)} %bitcast.25), channel_id=1, replica_groups=mesh['y'=4,'x'=4,'z'=8,'c'=2] {'c','y','x'}, dimensions={0} | all-to-all | bytes 1179648 | tf_op jit(solution)/shard_map/all_to_all | solution.py:402
  167.7 3.1 %combine.1 = (f32[1024,128]{1,0:T(8,128)S(1)}, f32[16,8,128]{2,1,0:T(8,128)S(1)}) custom-call(bf16[2304,128]{1,0:T(8,128)(2,1)S(1)} %bitcast.18, f32[1024,128]{1,0:T(8,128)S(1)} %copy-done), custom_call_target="tpu_custom_call" | custom-call | tf_op jit(solution)/shard_map/combine/pallas_call | solution.py:406
  170.8 15.5 %all_to_all.16.squares_ref = f32[16,8,128]{2,1,0:T(8,128)S(1)} all-to-all(f32[16,8,128]{2,1,0:T(8,128)S(1)} %get-tuple-element.52), channel_id=1, replica_groups=mesh['y'=4,'x'=4,'z'=8,'c'=2] {'z','c'}, dimensions={0} | all-to-all | bytes 131072 | tf_op jit(solution)/shard_map/all_to_all | solution.py:415
  (68 shorter events, 16.9 us)
Async XLA Ops:
  4.3 69.3 %collective-permute-start.8 = (bf16[1344,2048]{1,0:T(8,128)(2,1)}, bf16[1344,2048]{1,0:T(8,128)(2,1)}, u32[]{:S(2)}, u32[]{:S(2)}) collective-permute-start(bf16[1344,2048]{1,0:T(8,128)(2,1)} %join.1), channel_id=1, source_target_pairs={{0,1},{1,0},{2,3},{3,2},{4,5},{5,4},{6,7},{7,6},{8,9},{9,8},{10,11... | collective-permute-start | bytes 16515080 | tf_op jit(solution)/shard_map/ppermute | solution.py:329
  14.1 17.2 %all-to-all-start = ((bf16[32,72,128]{2,1,0:T(8,128)(2,1)}), bf16[32,72,128]{2,1,0:T(8,128)(2,1)S(1)}, u32[]{:S(2)}, u32[]{:S(2)}) async-start(bf16[32,72,128]{2,1,0:T(8,128)(2,1)} %bitcast.29), calls=%async_computation | async-start | bytes 1179648 | tf_op jit(solution)/shard_map/all_to_all | solution.py:391
  19.6 1.3 collective-permute-start
  31.4 12.0 %collective-permute-start.1 = (bf16[2,584,128]{2,1,0:T(8,128)(2,1)S(1)}, bf16[2,584,128]{2,1,0:T(8,128)(2,1)S(1)}, u32[]{:S(2)}, u32[]{:S(2)}) collective-permute-start(bf16[2,584,128]{2,1,0:T(8,128)(2,1)S(1)} %get-tuple-element.55.x0), channel_id=1, source_target_pairs={{0,2},{2,4},{4,6},{6,8},{8,10},{10,12},{12,14},{14,0},{1,3},{3,5},... | collective-permute-start | bytes 897032 | tf_op jit(solution)/shard_map/ppermute | solution.py:329
  33.1 10.3 %collective-permute-start.19 = (bf16[2,584,128]{2,1,0:T(8,128)(2,1)S(1)}, bf16[2,584,128]{2,1,0:T(8,128)(2,1)S(1)}, u32[]{:S(2)}, u32[]{:S(2)}) collective-permute-start(bf16[2,584,128]{2,1,0:T(8,128)(2,1)S(1)} %get-tuple-element.56.x0), channel_id=1, source_target_pairs={{0,14},{2,0},{4,2},{6,4},{8,6},{10,8},{12,10},{14,12},{1,15},{3,1}... | collective-permute-start | bytes 897032 | tf_op jit(solution)/shard_map/ppermute | solution.py:329
  37.2 11.7 %collective-permute-start.4 = (bf16[2,584,128]{2,1,0:T(8,128)(2,1)S(1)}, bf16[2,584,128]{2,1,0:T(8,128)(2,1)S(1)}, u32[]{:S(2)}, u32[]{:S(2)}) collective-permute-start(bf16[2,584,128]{2,1,0:T(8,128)(2,1)S(1)} %get-tuple-element.55.x0), channel_id=1, source_target_pairs={{0,14},{2,0},{4,2},{6,4},{8,6},{10,8},{12,10},{14,12},{1,15},{3,1}... | collective-permute-start | bytes 897032 | tf_op jit(solution)/shard_map/ppermute | solution.py:329
  43.4 8.9 %collective-permute-start.2 = (bf16[2,584,128]{2,1,0:T(8,128)(2,1)S(1)}, bf16[2,584,128]{2,1,0:T(8,128)(2,1)S(1)}, u32[]{:S(2)}, u32[]{:S(2)}) collective-permute-start(bf16[2,584,128]{2,1,0:T(8,128)(2,1)S(1)} %collective-permute-done.1.p1), channel_id=1, source_target_pairs={{0,2},{2,4},{4,6},{6,8},{8,10},{10,12},{12,14},{14,0},{1,3},{3,5},... | collective-permute-start | bytes 897032 | tf_op jit(solution)/shard_map/ppermute | solution.py:329
  43.4 14.5 %collective-permute-start.16 = (bf16[2,584,128]{2,1,0:T(8,128)(2,1)S(1)}, bf16[2,584,128]{2,1,0:T(8,128)(2,1)S(1)}, u32[]{:S(2)}, u32[]{:S(2)}) collective-permute-start(bf16[2,584,128]{2,1,0:T(8,128)(2,1)S(1)} %get-tuple-element.56.x0), channel_id=1, source_target_pairs={{0,2},{2,4},{4,6},{6,8},{8,10},{10,12},{12,14},{14,0},{1,3},{3,5},... | collective-permute-start | bytes 897032 | tf_op jit(solution)/shard_map/ppermute | solution.py:329
  43.4 14.5 %collective-permute-start.20 = (bf16[2,584,128]{2,1,0:T(8,128)(2,1)S(1)}, bf16[2,584,128]{2,1,0:T(8,128)(2,1)S(1)}, u32[]{:S(2)}, u32[]{:S(2)}) collective-permute-start(bf16[2,584,128]{2,1,0:T(8,128)(2,1)S(1)} %collective-permute-done.19.m1), channel_id=1, source_target_pairs={{0,14},{2,0},{4,2},{6,4},{8,6},{10,8},{12,10},{14,12},{1,15},{3,1}... | collective-permute-start | bytes 897032 | tf_op jit(solution)/shard_map/ppermute | solution.py:329
  48.9 12.8 %collective-permute-start.5 = (bf16[2,584,128]{2,1,0:T(8,128)(2,1)S(1)}, bf16[2,584,128]{2,1,0:T(8,128)(2,1)}, u32[]{:S(2)}, u32[]{:S(2)}) collective-permute-start(bf16[2,584,128]{2,1,0:T(8,128)(2,1)S(1)} %collective-permute-done.4.m1), channel_id=1, source_target_pairs={{0,14},{2,0},{4,2},{6,4},{8,6},{10,8},{12,10},{14,12},{1,15},{3,1}... | collective-permute-start | bytes 897032 | tf_op jit(solution)/shard_map/ppermute | solution.py:329
  52.3 12.9 %collective-permute-start.3 = (bf16[2,584,128]{2,1,0:T(8,128)(2,1)S(1)}, bf16[2,584,128]{2,1,0:T(8,128)(2,1)S(1)}, u32[]{:S(2)}, u32[]{:S(2)}) collective-permute-start(bf16[2,584,128]{2,1,0:T(8,128)(2,1)S(1)} %collective-permute-done.2.p2), channel_id=1, source_target_pairs={{0,2},{2,4},{4,6},{6,8},{8,10},{10,12},{12,14},{14,0},{1,3},{3,5},... | collective-permute-start | bytes 897032 | tf_op jit(solution)/shard_map/ppermute | solution.py:329
  57.9 12.9 %collective-permute-start.17 = (bf16[2,584,128]{2,1,0:T(8,128)(2,1)S(1)}, bf16[2,584,128]{2,1,0:T(8,128)(2,1)}, u32[]{:S(2)}, u32[]{:S(2)}) collective-permute-start(bf16[2,584,128]{2,1,0:T(8,128)(2,1)S(1)} %collective-permute-done.16.p1), channel_id=1, source_target_pairs={{0,2},{2,4},{4,6},{6,8},{8,10},{10,12},{12,14},{14,0},{1,3},{3,5},... | collective-permute-start | bytes 897032 | tf_op jit(solution)/shard_map/ppermute | solution.py:329
  57.9 12.9 %collective-permute-start.21 = (bf16[2,584,128]{2,1,0:T(8,128)(2,1)S(1)}, bf16[2,584,128]{2,1,0:T(8,128)(2,1)S(1)}, u32[]{:S(2)}, u32[]{:S(2)}) collective-permute-start(bf16[2,584,128]{2,1,0:T(8,128)(2,1)S(1)} %collective-permute-done.20.m2), channel_id=1, source_target_pairs={{0,14},{2,0},{4,2},{6,4},{8,6},{10,8},{12,10},{14,12},{1,15},{3,1}... | collective-permute-start | bytes 897032 | tf_op jit(solution)/shard_map/ppermute | solution.py:329
  61.7 19.7 %collective-permute-start.6 = (bf16[2,584,128]{2,1,0:T(8,128)(2,1)}, bf16[2,584,128]{2,1,0:T(8,128)(2,1)S(1)}, u32[]{:S(2)}, u32[]{:S(2)}) collective-permute-start(bf16[2,584,128]{2,1,0:T(8,128)(2,1)} %collective-permute-done.5.m2), channel_id=1, source_target_pairs={{0,14},{2,0},{4,2},{6,4},{8,6},{10,8},{12,10},{14,12},{1,15},{3,1}... | collective-permute-start | bytes 897032 | tf_op jit(solution)/shard_map/ppermute | solution.py:329
  65.2 16.2 %collective-permute-start.7 = (bf16[2,584,128]{2,1,0:T(8,128)(2,1)S(1)}, bf16[2,584,128]{2,1,0:T(8,128)(2,1)S(1)}, u32[]{:S(2)}, u32[]{:S(2)}) collective-permute-start(bf16[2,584,128]{2,1,0:T(8,128)(2,1)S(1)} %collective-permute-done.3.p3), channel_id=1, source_target_pairs={{0,2},{2,4},{4,6},{6,8},{8,10},{10,12},{12,14},{14,0},{1,3},{3,5},... | collective-permute-start | bytes 897032 | tf_op jit(solution)/shard_map/ppermute | solution.py:329
  70.8 27.0 %collective-permute-start.18 = (bf16[2,584,128]{2,1,0:T(8,128)(2,1)}, bf16[2,584,128]{2,1,0:T(8,128)(2,1)S(1)}, u32[]{:S(2)}, u32[]{:S(2)}) collective-permute-start(bf16[2,584,128]{2,1,0:T(8,128)(2,1)} %collective-permute-done.17.p2), channel_id=1, source_target_pairs={{0,2},{2,4},{4,6},{6,8},{8,10},{10,12},{12,14},{14,0},{1,3},{3,5},... | collective-permute-start | bytes 897032 | tf_op jit(solution)/shard_map/ppermute | solution.py:329
  70.8 27.0 %collective-permute-start.22 = (bf16[2,584,128]{2,1,0:T(8,128)(2,1)S(1)}, bf16[2,584,128]{2,1,0:T(8,128)(2,1)S(1)}, u32[]{:S(2)}, u32[]{:S(2)}) collective-permute-start(bf16[2,584,128]{2,1,0:T(8,128)(2,1)S(1)} %collective-permute-done.21.m3), channel_id=1, source_target_pairs={{0,14},{2,0},{4,2},{6,4},{8,6},{10,8},{12,10},{14,12},{1,15},{3,1}... | collective-permute-start | bytes 897032 | tf_op jit(solution)/shard_map/ppermute | solution.py:329
  88.3 19.3 %collective-permute-start.9 = (bf16[2,576,128]{2,1,0:T(8,128)(2,1)S(1)}, bf16[2,576,128]{2,1,0:T(8,128)(2,1)S(1)}, u32[]{:S(2)}, u32[]{:S(2)}) collective-permute-start(bf16[2,576,128]{2,1,0:T(8,128)(2,1)S(1)} %get-tuple-element.36), channel_id=1, source_target_pairs={{0,2},{2,4},{4,6},{6,8},{8,10},{10,12},{12,14},{14,0},{1,3},{3,5},... | collective-permute-start | bytes 884744 | tf_op jit(solution)/shard_map/ppermute | solution.py:329
  88.4 19.6 %collective-permute-start.13 = (bf16[2,576,128]{2,1,0:T(8,128)(2,1)S(1)}, bf16[2,576,128]{2,1,0:T(8,128)(2,1)S(1)}, u32[]{:S(2)}, u32[]{:S(2)}) collective-permute-start(bf16[2,576,128]{2,1,0:T(8,128)(2,1)S(1)} %get-tuple-element.39), channel_id=1, source_target_pairs={{0,14},{2,0},{4,2},{6,4},{8,6},{10,8},{12,10},{14,12},{1,15},{3,1}... | collective-permute-start | bytes 884744 | tf_op jit(solution)/shard_map/ppermute | solution.py:329
  104.8 6.9 %collective-permute-start.23 = (bf16[2,576,128]{2,1,0:T(8,128)(2,1)S(1)}, bf16[2,576,128]{2,1,0:T(8,128)(2,1)S(1)}, u32[]{:S(2)}, u32[]{:S(2)}) collective-permute-start(bf16[2,576,128]{2,1,0:T(8,128)(2,1)S(1)} %get-tuple-element.45), channel_id=1, source_target_pairs={{0,2},{2,4},{4,6},{6,8},{8,10},{10,12},{12,14},{14,0},{1,3},{3,5},... | collective-permute-start | bytes 884744 | tf_op jit(solution)/shard_map/ppermute | solution.py:329
  104.9 6.9 %collective-permute-start.26 = (bf16[2,576,128]{2,1,0:T(8,128)(2,1)S(1)}, bf16[2,576,128]{2,1,0:T(8,128)(2,1)S(1)}, u32[]{:S(2)}, u32[]{:S(2)}) collective-permute-start(bf16[2,576,128]{2,1,0:T(8,128)(2,1)S(1)} %get-tuple-element.49), channel_id=1, source_target_pairs={{0,14},{2,0},{4,2},{6,4},{8,6},{10,8},{12,10},{14,12},{1,15},{3,1}... | collective-permute-start | bytes 884744 | tf_op jit(solution)/shard_map/ppermute | solution.py:329
  107.6 7.2 %collective-permute-start.10 = (bf16[2,576,128]{2,1,0:T(8,128)(2,1)S(1)}, bf16[2,576,128]{2,1,0:T(8,128)(2,1)S(1)}, u32[]{:S(2)}, u32[]{:S(2)}) collective-permute-start(bf16[2,576,128]{2,1,0:T(8,128)(2,1)S(1)} %add_convert_fusion.11), channel_id=1, source_target_pairs={{0,2},{2,4},{4,6},{6,8},{8,10},{10,12},{12,14},{14,0},{1,3},{3,5},... | collective-permute-start | bytes 884744 | tf_op jit(solution)/shard_map/ppermute | solution.py:329
  108.0 6.9 %collective-permute-start.14 = (bf16[2,576,128]{2,1,0:T(8,128)(2,1)S(1)}, bf16[2,576,128]{2,1,0:T(8,128)(2,1)S(1)}, u32[]{:S(2)}, u32[]{:S(2)}) collective-permute-start(bf16[2,576,128]{2,1,0:T(8,128)(2,1)S(1)} %add_convert_fusion.8), channel_id=1, source_target_pairs={{0,14},{2,0},{4,2},{6,4},{8,6},{10,8},{12,10},{14,12},{1,15},{3,1}... | collective-permute-start | bytes 884744 | tf_op jit(solution)/shard_map/ppermute | solution.py:329
  111.7 16.8 %collective-permute-start.24 = (bf16[2,576,128]{2,1,0:T(8,128)(2,1)S(1)}, bf16[2,576,128]{2,1,0:T(8,128)(2,1)S(1)}, u32[]{:S(2)}, u32[]{:S(2)}) collective-permute-start(bf16[2,576,128]{2,1,0:T(8,128)(2,1)S(1)} %add_convert_fusion.5), channel_id=1, source_target_pairs={{0,2},{2,4},{4,6},{6,8},{8,10},{10,12},{12,14},{14,0},{1,3},{3,5},... | collective-permute-start | bytes 884744 | tf_op jit(solution)/shard_map/ppermute | solution.py:329
  111.9 9.6 %collective-permute-start.27 = (bf16[2,576,128]{2,1,0:T(8,128)(2,1)S(1)}, bf16[2,576,128]{2,1,0:T(8,128)(2,1)S(1)}, u32[]{:S(2)}, u32[]{:S(2)}) collective-permute-start(bf16[2,576,128]{2,1,0:T(8,128)(2,1)S(1)} %add_convert_fusion.3), channel_id=1, source_target_pairs={{0,14},{2,0},{4,2},{6,4},{8,6},{10,8},{12,10},{14,12},{1,15},{3,1}... | collective-permute-start | bytes 884744 | tf_op jit(solution)/shard_map/ppermute | solution.py:329
  114.9 13.5 %collective-permute-start.11 = (bf16[2,576,128]{2,1,0:T(8,128)(2,1)S(1)}, bf16[2,576,128]{2,1,0:T(8,128)(2,1)S(1)}, u32[]{:S(2)}, u32[]{:S(2)}) collective-permute-start(bf16[2,576,128]{2,1,0:T(8,128)(2,1)S(1)} %add_convert_fusion.10), channel_id=1, source_target_pairs={{0,2},{2,4},{4,6},{6,8},{8,10},{10,12},{12,14},{14,0},{1,3},{3,5},... | collective-permute-start | bytes 884744 | tf_op jit(solution)/shard_map/ppermute | solution.py:329
  115.1 22.6 %collective-permute-start.15 = (bf16[2,576,128]{2,1,0:T(8,128)(2,1)S(1)}, bf16[2,576,128]{2,1,0:T(8,128)(2,1)S(1)}, u32[]{:S(2)}, u32[]{:S(2)}) collective-permute-start(bf16[2,576,128]{2,1,0:T(8,128)(2,1)S(1)} %add_convert_fusion.7), channel_id=1, source_target_pairs={{0,14},{2,0},{4,2},{6,4},{8,6},{10,8},{12,10},{14,12},{1,15},{3,1}... | collective-permute-start | bytes 884744 | tf_op jit(solution)/shard_map/ppermute | solution.py:329
  121.5 12.6 %collective-permute-start.28 = (bf16[2,576,128]{2,1,0:T(8,128)(2,1)S(1)}, bf16[2,576,128]{2,1,0:T(8,128)(2,1)S(1)}, u32[]{:S(2)}, u32[]{:S(2)}) collective-permute-start(bf16[2,576,128]{2,1,0:T(8,128)(2,1)S(1)} %add_convert_fusion.2), channel_id=1, source_target_pairs={{0,14},{2,0},{4,2},{6,4},{8,6},{10,8},{12,10},{14,12},{1,15},{3,1}... | collective-permute-start | bytes 884744 | tf_op jit(solution)/shard_map/ppermute | solution.py:329
  128.4 9.7 %collective-permute-start.12 = (bf16[2,576,128]{2,1,0:T(8,128)(2,1)S(1)}, bf16[2,576,128]{2,1,0:T(8,128)(2,1)S(1)}, u32[]{:S(2)}, u32[]{:S(2)}) collective-permute-start(bf16[2,576,128]{2,1,0:T(8,128)(2,1)S(1)} %add_convert_fusion.9), channel_id=1, source_target_pairs={{0,2},{2,4},{4,6},{6,8},{8,10},{10,12},{12,14},{14,0},{1,3},{3,5},... | collective-permute-start | bytes 884744 | tf_op jit(solution)/shard_map/ppermute | solution.py:329
  128.6 12.7 %collective-permute-start.25 = (bf16[2,576,128]{2,1,0:T(8,128)(2,1)S(1)}, bf16[2,576,128]{2,1,0:T(8,128)(2,1)S(1)}, u32[]{:S(2)}, u32[]{:S(2)}) collective-permute-start(bf16[2,576,128]{2,1,0:T(8,128)(2,1)S(1)} %add_convert_fusion.4), channel_id=1, source_target_pairs={{0,2},{2,4},{4,6},{6,8},{8,10},{10,12},{12,14},{14,0},{1,3},{3,5},... | collective-permute-start | bytes 884744 | tf_op jit(solution)/shard_map/ppermute | solution.py:329
  134.2 10.3 %collective-permute-start.29 = (bf16[2,576,128]{2,1,0:T(8,128)(2,1)S(1)}, bf16[2,576,128]{2,1,0:T(8,128)(2,1)S(1)}, u32[]{:S(2)}, u32[]{:S(2)}) collective-permute-start(bf16[2,576,128]{2,1,0:T(8,128)(2,1)S(1)} %add_convert_fusion.1), channel_id=1, source_target_pairs={{0,14},{2,0},{4,2},{6,4},{8,6},{10,8},{12,10},{14,12},{1,15},{3,1}... | collective-permute-start | bytes 884744 | tf_op jit(solution)/shard_map/ppermute | solution.py:329
  144.6 41.7 %copy-start.3 = (bf16[128]{0:T(256)(128)(2,1)S(1)}, bf16[128]{0:T(256)(128)(2,1)}, u32[]{:S(2)}) copy-start(bf16[128]{0:T(256)(128)(2,1)} %param.15) | copy-start | bytes 772
  (4 other events, 50.8 us)

commit v3 on v2

--- a/solution.py
+++ b/solution.py
@@ -18,53 +18,54 @@
 BF16 = jnp.bfloat16
 
 
-def route_kernel(ids_ref, weight_ref, tok_ref, out_ref, pos_ref, pick_scr):
+def route_kernel(ids_ref, weight_ref, tok_ref, out_ref, rows_ref):
     rows = tok_ref.shape[0]
     half = out_ref.shape[0] // 32
     block = LANES
-    blocks = rows // block
-    lane = lax.broadcasted_iota(jnp.int32, (block, LANES), 1).astype(F32)
-    lower = (
+    expert = lax.broadcasted_iota(jnp.int32, (16, block), 0)
+    sooner = (
         (
             lax.broadcasted_iota(jnp.int32, (block, block), 0)
-            > lax.broadcasted_iota(jnp.int32, (block, block), 1)
+            < lax.broadcasted_iota(jnp.int32, (block, block), 1)
         )
         .astype(F32)
         .astype(BF16)
     )
-    before = jnp.zeros((1, LANES), F32)
-    fill = jnp.zeros((4, block), F32)
-    for b in range(blocks):
+    before = jnp.zeros((16, 1), F32)
+    first_row = expert.astype(F32) * half
+    pad = jnp.zeros((4, block), F32)
+    for b in range(rows // block):
         span = slice(b * block, (b + 1) * block)
-        given = jnp.concatenate(
-            [ids_ref[:, span].astype(F32), weight_ref[:, span], fill], axis=0
-        )
-        turned = jnp.concatenate([given] * (LANES // 8), axis=0).T
-        is_first = lane == turned[:, 0:1]
-        is_second = lane == turned[:, 1:2]
+        is_first = expert == ids_ref[0:1, span]
+        is_second = expert == ids_ref[1:2, span]
         named = jnp.where(is_first | is_second, 1.0, 0.0)
-        rank = jnp.dot(lower, named.astype(BF16), preferred_element_type=F32) + before
-        before = before + jnp.sum(named, axis=0, keepdims=True)
-        place = rank + lane * half + jnp.where(rank >= half, 15.0 * half, 0.0)
-        place0 = jnp.sum(jnp.where(is_first, place, 0.0), axis=1, keepdims=True)
-        place1 = jnp.sum(jnp.where(is_second, place, 0.0), axis=1, keepdims=True)
-        both = jnp.where(lane == 0, place0, jnp.where(lane == 1, place1, turned))
-        pos_ref[span, :] = both
-        pick_scr[:, span] = both.T[0:8, :]
+        rank = jnp.dot(named.astype(BF16), sooner, preferred_element_type=F32) + before
+        before = before + jnp.sum(named, axis=1, keepdims=True)
+        place = rank + first_row + jnp.where(rank >= half, 15.0 * half, 0.0)
+        place0 = jnp.sum(jnp.where(is_first, place, 0.0), axis=0, keepdims=True)
+        place1 = jnp.sum(jnp.where(is_second, place, 0.0), axis=0, keepdims=True)
+        rows_ref[:, span] = jnp.concatenate([place0, place1, weight_ref[:, span], pad], axis=0)
     step = 2 * half
-    row0 = pick_scr[0:1, :]
-    row1 = pick_scr[1:2, :]
+    row0 = rows_ref[0:1, :]
+    row1 = rows_ref[1:2, :]
     base = lax.broadcasted_iota(jnp.int32, (step, rows), 0).astype(F32)
     tok = tok_ref[...]
 
     def one(b, carry):
         start = pl.multiple_of(b * step, step)
-        at = base + start.astype(F32)
-        pick = jnp.where((at == row0) | (at == row1), 1.0, 0.0).astype(BF16)
+        low = start.astype(F32)
+        pick = jnp.where((base == row0 - low) | (base == row1 - low), 1.0, 0.0).astype(BF16)
         out_ref[pl.ds(start, step), :] = jnp.dot(pick, tok, preferred_element_type=F32).astype(BF16)
         return carry
 
-    lax.fori_loop(0, out_ref.shape[0] // step, one, 0, unroll=4)
+    lax.fori_loop(0, out_ref.shape[0] // step, one, 0, unroll=8)
+
+
+def turn_kernel(rows_ref, pos_ref):
+    for b in range(pos_ref.shape[0] // LANES):
+        span = slice(b * LANES, (b + 1) * LANES)
+        given = rows_ref[:, span]
+        pos_ref[span, :] = jnp.concatenate([given] * (LANES // 8), axis=0).T
 
 
 def combine_kernel(ret_ref, pos_ref, out_ref, square_ref):
@@ -377,16 +378,21 @@
         c == 0, jnp.stack([gain_rows, gain_other]), jnp.stack([gain_other, gain_rows])
     )
 
-    outgoing, places = pl.pallas_call(
+    outgoing, slot_rows = pl.pallas_call(
         route_kernel,
         name="route",
         compiler_params=pltpu.CompilerParams(vmem_limit_bytes=60 * MIB),
         out_shape=[
             jax.ShapeDtypeStruct((total, LANES), BF16),
-            jax.ShapeDtypeStruct((tok_rows, LANES), F32),
-        ],
-        scratch_shapes=[pltpu.VMEM((8, tok_rows), F32)],
+            jax.ShapeDtypeStruct((8, tok_rows), F32),
+        ],
     )(route_ids.T, route_weights.T, tokens)
+    places = pl.pallas_call(
+        turn_kernel,
+        name="places",
+        compiler_params=pltpu.CompilerParams(vmem_limit_bytes=SMALL_VMEM),
+        out_shape=jax.ShapeDtypeStruct((tok_rows, LANES), F32),
+    )(slot_rows)
     exchange = ("c", "y", "x")
     arrived = lax.all_to_all(
         outgoing.reshape(2 * groups, half, LANES), exchange, 0, 0, tiled=True
@@ -412,7 +418,7 @@
             jax.ShapeDtypeStruct((everyone, tok_rows // LANES, LANES), F32),
         ],
     )(returned, places)
-    gathered = lax.all_to_all(squares, ("z", "c"), 0, 0, tiled=True)
+    gathered = lax.all_to_all(squares, ("c", "z"), 0, 0, tiled=True)
     return pl.pallas_call(
         finish_kernel,
         name="finish",

time: 188 us -> 186 us (0.989)
  blocking collectives: 38.5 us -> 14.4 us
  starting transfers between devices: 52.5 us -> 64.5 us
  waiting for transfers between devices: 50.7 us -> 62.3 us
  Pallas kernels: 42.3 us -> 40.1 us
    all_to_all x2 -> x1, blocking collectives: 38.5 us -> 14.4 us  [layer(): gathered = lax.all_to_all(squares, ('c', 'z'), 0, 0, tiled=True)]
    all_to_all x0 -> x1, starting transfers between devices: none -> 12 us  [layer(): lax.all_to_all(result.reshape(2 * groups, half, LANES), exchange, 0, 0, t...]
    all_to_all x0 -> x1, waiting for transfers between devices: none -> 11.5 us  [layer(): lax.all_to_all(result.reshape(2 * groups, half, LANES), exchange, 0, 0, t...]
    pallas_call x1, Pallas kernels: 6.53 us -> 4.17 us  [layer(): pl.pallas_call(route_kernel, name='route', compiler_params=pltpu.Compiler...]
  transfers between devices with their start and end apart: 31 -> 32, of which waited for: 15 -> 16; matrix products, arithmetic and copies ran while one was open for 1% -> 1% of each run, Pallas kernels for 18% -> 17%
where the time goes in v3:
time: 186 us; the launch traced here: 185 us
  starting transfers between devices  64.5 us (35%)
  waiting for transfers between devices  62.3 us (33%)
  Pallas kernels  40.1 us (22%)
  blocking collectives  14.4 us (8%)
  other arithmetic  1.96 us (1%)
    ppermute x30, starting transfers between devices, turn(): lax.ppermute(value, axis, [(i, (i + by) % count) for i in range(count)])  47 us
    ppermute x30, waiting for transfers between devices, turn(): lax.ppermute(value, axis, [(i, (i + by) % count) for i in range(count)])  40.3 us
    all_to_all x1, blocking collectives, layer(): gathered = lax.all_to_all(squares, ('c', 'z'), 0, 0, tiled=True)  14.4 us
    pallas_call x2, Pallas kernels, ffn(): pl.pallas_call(up_kernel, name='ffn_up', in_specs=[sm] + [vm] * (late + 2...  13.8 us
    pallas_call x2, Pallas kernels, ffn(): pl.pallas_call(part_kernel, name='ffn_part', in_specs=[sm] + [hbm] * (ear...  13.6 us
    all_to_all x1, starting transfers between devices, layer(): lax.all_to_all(result.reshape(2 * groups, half, LANES), exchange, 0, 0, t...  12 us
    all_to_all x1, waiting for transfers between devices, layer(): lax.all_to_all(result.reshape(2 * groups, half, LANES), exchange, 0, 0, t...  11.5 us
    all_to_all x1, waiting for transfers between devices, layer(): lax.all_to_all(outgoing.reshape(2 * groups, half, LANES), exchange, 0, 0,...  10.4 us
  transfers between devices with their start and end apart: 32, of which 16 were waited for; matrix products, arithmetic and copies ran while one was open for 1% of the time, Pallas kernels for 17%

profile of v3, /device:TPU:1, one launch (start us, length us, event | category | flops | bytes accessed | tf_op | source)
XLA Modules:
  0.0 185.2 jit_solution(7986213488726139431)
XLA Ops:
  0.0 4.2 %join.1 = bf16[1344,2048]{1,0:T(8,128)(2,1)} custom-call(bf16[448,2048]{1,0:T(8,128)(2,1)} %bitcast.25, bf16[448,2048]{1,0:T(8,128)(2,1)} %bitcast.26, bf16[448,2048]{1,0:T(8,128)(2,1)} %bitcast.27), custom_call_target="tpu_custom_call" | custom-call | tf_op jit(solution)/shard_map/join/pallas_call | solution.py:313
  4.3 3.3 %collective-permute-start.8 = (bf16[1344,2048]{1,0:T(8,128)(2,1)}, bf16[1344,2048]{1,0:T(8,128)(2,1)}, u32[]{:S(2)}, u32[]{:S(2)}) collective-permute-start(bf16[1344,2048]{1,0:T(8,128)(2,1)} %join.1), channel_id=1, source_target_pairs={{0,1},{1,0},{2,3},{3,2},{4,5},{5,4},{6,7},{7,6},{8,9},{9,8},{10,11... | collective-permute-start | bytes 16515080 | tf_op jit(solution)/shard_map/ppermute | solution.py:330
  7.5 4.2 %route.1 = (bf16[2304,128]{1,0:T(8,128)(2,1)}, f32[8,1024]{1,0:T(8,128)}) custom-call(s32[2,1024]{1,0:T(2,128)} %bitcast.29, f32[2,1024]{1,0:T(2,128)} %bitcast.30, bf16[1024,128]{1,0:T(8,128)(2,1)} %tok_ref.1), custom_call_target="tpu_custom_call" | custom-call | tf_op jit(solution)/shard_map/route/pallas_call | solution.py:381
  11.7 5.5 %all-to-all-start = ((bf16[32,72,128]{2,1,0:T(8,128)(2,1)}), bf16[32,72,128]{2,1,0:T(8,128)(2,1)S(1)}, u32[]{:S(2)}, u32[]{:S(2)}) async-start(bf16[32,72,128]{2,1,0:T(8,128)(2,1)} %bitcast.28), calls=%async_computation | async-start | bytes 1179648 | tf_op jit(solution)/shard_map/all_to_all | solution.py:397
  18.5 10.4 %all-to-all-done = bf16[32,72,128]{2,1,0:T(8,128)(2,1)S(1)} async-done(((bf16[32,72,128]{2,1,0:T(8,128)(2,1)}), bf16[32,72,128]{2,1,0:T(8,128)(2,1)S(1)}, u32[]{:S(2)}, u32[]{:S(2)}) %all-to-all-start) | async-done | bytes 589856 | tf_op jit(solution)/shard_map/all_to_all | solution.py:397
  30.8 4.0 %collective-permute-start.19 = (bf16[2,584,128]{2,1,0:T(8,128)(2,1)S(1)}, bf16[2,584,128]{2,1,0:T(8,128)(2,1)S(1)}, u32[]{:S(2)}, u32[]{:S(2)}) collective-permute-start(bf16[2,584,128]{2,1,0:T(8,128)(2,1)S(1)} %get-tuple-element.56.x0), channel_id=1, source_target_pairs={{0,14},{2,0},{4,2},{6,4},{8,6},{10,8},{12,10},{14,12},{1,15},{3,1}... | collective-permute-start | bytes 897032 | tf_op jit(solution)/shard_map/ppermute | solution.py:330
  36.2 4.9 %collective-permute-done.1.p1 = bf16[2,584,128]{2,1,0:T(8,128)(2,1)S(1)} collective-permute-done((bf16[2,584,128]{2,1,0:T(8,128)(2,1)S(1)}, bf16[2,584,128]{2,1,0:T(8,128)(2,1)S(1)}, u32[]{:S(2)}, u32[]{:S(2)}) %collective-permute-start.1) | collective-permute-done | bytes 299040 | tf_op jit(solution)/shard_map/ppermute | solution.py:330
  41.0 2.7 %collective-permute-start.20 = (bf16[2,584,128]{2,1,0:T(8,128)(2,1)S(1)}, bf16[2,584,128]{2,1,0:T(8,128)(2,1)S(1)}, u32[]{:S(2)}, u32[]{:S(2)}) collective-permute-start(bf16[2,584,128]{2,1,0:T(8,128)(2,1)S(1)} %collective-permute-done.19.m1), channel_id=1, source_target_pairs={{0,14},{2,0},{4,2},{6,4},{8,6},{10,8},{12,10},{14,12},{1,15},{3,1}... | collective-permute-start | bytes 897032 | tf_op jit(solution)/shard_map/ppermute | solution.py:330
  43.7 2.8 %collective-permute-done.4.m1 = bf16[2,584,128]{2,1,0:T(8,128)(2,1)S(1)} collective-permute-done((bf16[2,584,128]{2,1,0:T(8,128)(2,1)S(1)}, bf16[2,584,128]{2,1,0:T(8,128)(2,1)S(1)}, u32[]{:S(2)}, u32[]{:S(2)}) %collective-permute-start.4) | collective-permute-done | bytes 299040 | tf_op jit(solution)/shard_map/ppermute | solution.py:330
  46.5 3.4 %collective-permute-start.5 = (bf16[2,584,128]{2,1,0:T(8,128)(2,1)S(1)}, bf16[2,584,128]{2,1,0:T(8,128)(2,1)}, u32[]{:S(2)}, u32[]{:S(2)}) collective-permute-start(bf16[2,584,128]{2,1,0:T(8,128)(2,1)S(1)} %collective-permute-done.4.m1), channel_id=1, source_target_pairs={{0,14},{2,0},{4,2},{6,4},{8,6},{10,8},{12,10},{14,12},{1,15},{3,1}... | collective-permute-start | bytes 897032 | tf_op jit(solution)/shard_map/ppermute | solution.py:330
  50.6 4.9 %collective-permute-done.16.p1 = bf16[2,584,128]{2,1,0:T(8,128)(2,1)S(1)} collective-permute-done((bf16[2,584,128]{2,1,0:T(8,128)(2,1)S(1)}, bf16[2,584,128]{2,1,0:T(8,128)(2,1)S(1)}, u32[]{:S(2)}, u32[]{:S(2)}) %collective-permute-start.16) | collective-permute-done | bytes 299040 | tf_op jit(solution)/shard_map/ppermute | solution.py:330
  55.6 2.7 %collective-permute-start.21 = (bf16[2,584,128]{2,1,0:T(8,128)(2,1)S(1)}, bf16[2,584,128]{2,1,0:T(8,128)(2,1)S(1)}, u32[]{:S(2)}, u32[]{:S(2)}) collective-permute-start(bf16[2,584,128]{2,1,0:T(8,128)(2,1)S(1)} %collective-permute-done.20.m2), channel_id=1, source_target_pairs={{0,14},{2,0},{4,2},{6,4},{8,6},{10,8},{12,10},{14,12},{1,15},{3,1}... | collective-permute-start | bytes 897032 | tf_op jit(solution)/shard_map/ppermute | solution.py:330
  59.3 3.5 %collective-permute-start.6 = (bf16[2,584,128]{2,1,0:T(8,128)(2,1)}, bf16[2,584,128]{2,1,0:T(8,128)(2,1)S(1)}, u32[]{:S(2)}, u32[]{:S(2)}) collective-permute-start(bf16[2,584,128]{2,1,0:T(8,128)(2,1)} %collective-permute-done.5.m2), channel_id=1, source_target_pairs={{0,14},{2,0},{4,2},{6,4},{8,6},{10,8},{12,10},{14,12},{1,15},{3,1}... | collective-permute-start | bytes 897032 | tf_op jit(solution)/shard_map/ppermute | solution.py:330
  62.8 5.6 %collective-permute-done.17.p2 = bf16[2,584,128]{2,1,0:T(8,128)(2,1)} collective-permute-done((bf16[2,584,128]{2,1,0:T(8,128)(2,1)S(1)}, bf16[2,584,128]{2,1,0:T(8,128)(2,1)}, u32[]{:S(2)}, u32[]{:S(2)}) %collective-permute-start.17) | collective-permute-done | bytes 299040 | tf_op jit(solution)/shard_map/ppermute | solution.py:330
  72.1 6.8 %ffn_part.2 = (f32[7,576,256]{2,1,0:T(8,128)S(1)}, f32[576,128]{1,0:T(8,128)S(1)}) custom-call(s32[1]{0:T(128)} %bitcast.z_ref, bf16[2,584,128]{2,1,0:T(8,128)(2,1)S(1)} %get-tuple-element.55.x0, bf16[2,584,128]{2,1,0:T(8,128)(2,1)S(1)} %collective-permute-done.1.p1, bf16[2,584,128]{2,1,0:T(8,128)(2,1)S(1)} %collective-permute-done.4.m1, ...), custom_call_target="tpu_custom_call" | custom-call | flops 2642411520 | bytes 9306112 | tf_op jit(solution)/shard_map/ffn_part/pallas_call | solution.py:242
  79.0 6.9 %ffn_up.2 = (bf16[2,576,128]{2,1,0:T(8,128)(2,1)S(1)}, bf16[2,576,128]{2,1,0:T(8,128)(2,1)S(1)}, bf16[2,576,128]{2,1,0:T(8,128)(2,1)S(1)}, bf16[2,576,128]{2,1,0...) custom-call(s32[1]{0:T(128)} %bitcast.z_ref, ...), custom_call_target="tpu_custom_call" | custom-call | flops 3699376128 | bytes 11141120 | tf_op jit(solution)/shard_map/ffn_up/pallas_call | solution.py:264
  88.7 6.8 %ffn_part.3 = (f32[7,576,256]{2,1,0:T(8,128)S(1)}, f32[576,128]{1,0:T(8,128)S(1)}) custom-call(s32[1]{0:T(128)} %bitcast.z_ref, bf16[2,584,128]{2,1,0:T(8,128)(2,1)S(1)} %get-tuple-element.56.x0, bf16[2,584,128]{2,1,0:T(8,128)(2,1)S(1)} %collective-permute-done.16.p1, bf16[2,584,128]{2,1,0:T(8,128)(2,1)S(1)} %collective-permute-done.19.m1, ...), custom_call_target="tpu_custom_call" | custom-call | flops 2642411520 | bytes 9306112 | tf_op jit(solution)/shard_map/ffn_part/pallas_call | solution.py:242
  95.5 6.9 %ffn_up.3 = (bf16[2,576,128]{2,1,0:T(8,128)(2,1)S(1)}, bf16[2,576,128]{2,1,0:T(8,128)(2,1)S(1)}, bf16[2,576,128]{2,1,0:T(8,128)(2,1)S(1)}, bf16[2,576,128]{2,1,0...) custom-call(s32[1]{0:T(128)} %bitcast.z_ref, ...), custom_call_target="tpu_custom_call" | custom-call | flops 3699376128 | bytes 11141120 | tf_op jit(solution)/shard_map/ffn_up/pallas_call | solution.py:264
  105.4 2.9 %collective-permute-start.14 = (bf16[2,576,128]{2,1,0:T(8,128)(2,1)S(1)}, bf16[2,576,128]{2,1,0:T(8,128)(2,1)S(1)}, u32[]{:S(2)}, u32[]{:S(2)}) collective-permute-start(bf16[2,576,128]{2,1,0:T(8,128)(2,1)S(1)} %add_convert_fusion.8), channel_id=1, source_target_pairs={{0,14},{2,0},{4,2},{6,4},{8,6},{10,8},{12,10},{14,12},{1,15},{3,1}... | collective-permute-start | bytes 884744 | tf_op jit(solution)/shard_map/ppermute | solution.py:330
  109.5 2.7 %collective-permute-start.27 = (bf16[2,576,128]{2,1,0:T(8,128)(2,1)S(1)}, bf16[2,576,128]{2,1,0:T(8,128)(2,1)S(1)}, u32[]{:S(2)}, u32[]{:S(2)}) collective-permute-start(bf16[2,576,128]{2,1,0:T(8,128)(2,1)S(1)} %add_convert_fusion.3), channel_id=1, source_target_pairs={{0,14},{2,0},{4,2},{6,4},{8,6},{10,8},{12,10},{14,12},{1,15},{3,1}... | collective-permute-start | bytes 884744 | tf_op jit(solution)/shard_map/ppermute | solution.py:330
  112.7 2.7 %collective-permute-start.15 = (bf16[2,576,128]{2,1,0:T(8,128)(2,1)S(1)}, bf16[2,576,128]{2,1,0:T(8,128)(2,1)S(1)}, u32[]{:S(2)}, u32[]{:S(2)}) collective-permute-start(bf16[2,576,128]{2,1,0:T(8,128)(2,1)S(1)} %add_convert_fusion.7), channel_id=1, source_target_pairs={{0,14},{2,0},{4,2},{6,4},{8,6},{10,8},{12,10},{14,12},{1,15},{3,1}... | collective-permute-start | bytes 884744 | tf_op jit(solution)/shard_map/ppermute | solution.py:330
  115.4 3.7 %collective-permute-done.27 = bf16[2,576,128]{2,1,0:T(8,128)(2,1)S(1)} collective-permute-done((bf16[2,576,128]{2,1,0:T(8,128)(2,1)S(1)}, bf16[2,576,128]{2,1,0:T(8,128)(2,1)S(1)}, u32[]{:S(2)}, u32[]{:S(2)}) %collective-permute-start.27) | collective-permute-done | bytes 294944 | tf_op jit(solution)/shard_map/ppermute | solution.py:330
  119.2 3.5 %collective-permute-start.28 = (bf16[2,576,128]{2,1,0:T(8,128)(2,1)S(1)}, bf16[2,576,128]{2,1,0:T(8,128)(2,1)S(1)}, u32[]{:S(2)}, u32[]{:S(2)}) collective-permute-start(bf16[2,576,128]{2,1,0:T(8,128)(2,1)S(1)} %add_convert_fusion.2), channel_id=1, source_target_pairs={{0,14},{2,0},{4,2},{6,4},{8,6},{10,8},{12,10},{14,12},{1,15},{3,1}... | collective-permute-start | bytes 884744 | tf_op jit(solution)/shard_map/ppermute | solution.py:330
  122.6 3.3 %collective-permute-done.11 = bf16[2,576,128]{2,1,0:T(8,128)(2,1)S(1)} collective-permute-done((bf16[2,576,128]{2,1,0:T(8,128)(2,1)S(1)}, bf16[2,576,128]{2,1,0:T(8,128)(2,1)S(1)}, u32[]{:S(2)}, u32[]{:S(2)}) %collective-permute-start.11) | collective-permute-done | bytes 294944 | tf_op jit(solution)/shard_map/ppermute | solution.py:330
  126.3 5.4 %collective-permute-done.28 = bf16[2,576,128]{2,1,0:T(8,128)(2,1)S(1)} collective-permute-done((bf16[2,576,128]{2,1,0:T(8,128)(2,1)S(1)}, bf16[2,576,128]{2,1,0:T(8,128)(2,1)S(1)}, u32[]{:S(2)}, u32[]{:S(2)}) %collective-permute-start.28) | collective-permute-done | bytes 294944 | tf_op jit(solution)/shard_map/ppermute | solution.py:330
  131.8 3.5 %collective-permute-start.29 = (bf16[2,576,128]{2,1,0:T(8,128)(2,1)S(1)}, bf16[2,576,128]{2,1,0:T(8,128)(2,1)S(1)}, u32[]{:S(2)}, u32[]{:S(2)}) collective-permute-start(bf16[2,576,128]{2,1,0:T(8,128)(2,1)S(1)} %add_convert_fusion.1), channel_id=1, source_target_pairs={{0,14},{2,0},{4,2},{6,4},{8,6},{10,8},{12,10},{14,12},{1,15},{3,1}... | collective-permute-start | bytes 884744 | tf_op jit(solution)/shard_map/ppermute | solution.py:330
  135.9 3.0 %collective-permute-done.25 = bf16[2,576,128]{2,1,0:T(8,128)(2,1)S(1)} collective-permute-done((bf16[2,576,128]{2,1,0:T(8,128)(2,1)S(1)}, bf16[2,576,128]{2,1,0:T(8,128)(2,1)S(1)}, u32[]{:S(2)}, u32[]{:S(2)}) %collective-permute-start.25) | collective-permute-done | bytes 294944 | tf_op jit(solution)/shard_map/ppermute | solution.py:330
  138.9 3.2 %collective-permute-done.29 = bf16[2,576,128]{2,1,0:T(8,128)(2,1)S(1)} collective-permute-done((bf16[2,576,128]{2,1,0:T(8,128)(2,1)S(1)}, bf16[2,576,128]{2,1,0:T(8,128)(2,1)S(1)}, u32[]{:S(2)}, u32[]{:S(2)}) %collective-permute-start.29) | collective-permute-done | bytes 294944 | tf_op jit(solution)/shard_map/ppermute | solution.py:330
  143.1 12.0 %all-to-all-start.1 = ((bf16[32,72,128]{2,1,0:T(8,128)(2,1)}), bf16[32,72,128]{2,1,0:T(8,128)(2,1)S(1)}, u32[]{:S(2)}, u32[]{:S(2)}) async-start(bf16[32,72,128]{2,1,0:T(8,128)(2,1)} %bitcast.13), calls=%async_computation.1 | async-start | bytes 1179648 | tf_op jit(solution)/shard_map/all_to_all | solution.py:408
  155.3 11.5 %all-to-all-done.1 = bf16[32,72,128]{2,1,0:T(8,128)(2,1)S(1)} async-done(((bf16[32,72,128]{2,1,0:T(8,128)(2,1)}), bf16[32,72,128]{2,1,0:T(8,128)(2,1)S(1)}, u32[]{:S(2)}, u32[]{:S(2)}) %all-to-all-start.1) | async-done | bytes 589856 | tf_op jit(solution)/shard_map/all_to_all | solution.py:408
  166.8 3.1 %combine.1 = (f32[1024,128]{1,0:T(8,128)S(1)}, f32[16,8,128]{2,1,0:T(8,128)S(1)}) custom-call(bf16[2304,128]{1,0:T(8,128)(2,1)S(1)} %bitcast.18, f32[1024,128]{1,0:T(8,128)S(1)} %places.1.pos_ref), custom_call_target="tpu_custom_call" | custom-call | tf_op jit(solution)/shard_map/combine/pallas_call | solution.py:412
  169.9 14.4 %all_to_all.15.squares_ref = f32[16,8,128]{2,1,0:T(8,128)S(1)} all-to-all(f32[16,8,128]{2,1,0:T(8,128)S(1)} %get-tuple-element.52), channel_id=1, replica_groups=mesh['y'=4,'x'=4,'z'=8,'c'=2] {'c','z'}, dimensions={0} | all-to-all | bytes 131072 | tf_op jit(solution)/shard_map/all_to_all | solution.py:421
  (70 shorter events, 20.4 us)
Async XLA Ops:
  4.3 66.9 %collective-permute-start.8 = (bf16[1344,2048]{1,0:T(8,128)(2,1)}, bf16[1344,2048]{1,0:T(8,128)(2,1)}, u32[]{:S(2)}, u32[]{:S(2)}) collective-permute-start(bf16[1344,2048]{1,0:T(8,128)(2,1)} %join.1), channel_id=1, source_target_pairs={{0,1},{1,0},{2,3},{3,2},{4,5},{5,4},{6,7},{7,6},{8,9},{9,8},{10,11... | collective-permute-start | bytes 16515080 | tf_op jit(solution)/shard_map/ppermute | solution.py:330
  11.7 17.2 %all-to-all-start = ((bf16[32,72,128]{2,1,0:T(8,128)(2,1)}), bf16[32,72,128]{2,1,0:T(8,128)(2,1)S(1)}, u32[]{:S(2)}, u32[]{:S(2)}) async-start(bf16[32,72,128]{2,1,0:T(8,128)(2,1)} %bitcast.28), calls=%async_computation | async-start | bytes 1179648 | tf_op jit(solution)/shard_map/all_to_all | solution.py:397
  17.2 1.3 collective-permute-start
  29.0 12.0 %collective-permute-start.1 = (bf16[2,584,128]{2,1,0:T(8,128)(2,1)S(1)}, bf16[2,584,128]{2,1,0:T(8,128)(2,1)S(1)}, u32[]{:S(2)}, u32[]{:S(2)}) collective-permute-start(bf16[2,584,128]{2,1,0:T(8,128)(2,1)S(1)} %get-tuple-element.55.x0), channel_id=1, source_target_pairs={{0,2},{2,4},{4,6},{6,8},{8,10},{10,12},{12,14},{14,0},{1,3},{3,5},... | collective-permute-start | bytes 897032 | tf_op jit(solution)/shard_map/ppermute | solution.py:330
  30.8 10.3 %collective-permute-start.19 = (bf16[2,584,128]{2,1,0:T(8,128)(2,1)S(1)}, bf16[2,584,128]{2,1,0:T(8,128)(2,1)S(1)}, u32[]{:S(2)}, u32[]{:S(2)}) collective-permute-start(bf16[2,584,128]{2,1,0:T(8,128)(2,1)S(1)} %get-tuple-element.56.x0), channel_id=1, source_target_pairs={{0,14},{2,0},{4,2},{6,4},{8,6},{10,8},{12,10},{14,12},{1,15},{3,1}... | collective-permute-start | bytes 897032 | tf_op jit(solution)/shard_map/ppermute | solution.py:330
  34.8 11.7 %collective-permute-start.4 = (bf16[2,584,128]{2,1,0:T(8,128)(2,1)S(1)}, bf16[2,584,128]{2,1,0:T(8,128)(2,1)S(1)}, u32[]{:S(2)}, u32[]{:S(2)}) collective-permute-start(bf16[2,584,128]{2,1,0:T(8,128)(2,1)S(1)} %get-tuple-element.55.x0), channel_id=1, source_target_pairs={{0,14},{2,0},{4,2},{6,4},{8,6},{10,8},{12,10},{14,12},{1,15},{3,1}... | collective-permute-start | bytes 897032 | tf_op jit(solution)/shard_map/ppermute | solution.py:330
  41.0 8.9 %collective-permute-start.2 = (bf16[2,584,128]{2,1,0:T(8,128)(2,1)S(1)}, bf16[2,584,128]{2,1,0:T(8,128)(2,1)S(1)}, u32[]{:S(2)}, u32[]{:S(2)}) collective-permute-start(bf16[2,584,128]{2,1,0:T(8,128)(2,1)S(1)} %collective-permute-done.1.p1), channel_id=1, source_target_pairs={{0,2},{2,4},{4,6},{6,8},{8,10},{10,12},{12,14},{14,0},{1,3},{3,5},... | collective-permute-start | bytes 897032 | tf_op jit(solution)/shard_map/ppermute | solution.py:330
  41.0 14.5 %collective-permute-start.16 = (bf16[2,584,128]{2,1,0:T(8,128)(2,1)S(1)}, bf16[2,584,128]{2,1,0:T(8,128)(2,1)S(1)}, u32[]{:S(2)}, u32[]{:S(2)}) collective-permute-start(bf16[2,584,128]{2,1,0:T(8,128)(2,1)S(1)} %get-tuple-element.56.x0), channel_id=1, source_target_pairs={{0,2},{2,4},{4,6},{6,8},{8,10},{10,12},{12,14},{14,0},{1,3},{3,5},... | collective-permute-start | bytes 897032 | tf_op jit(solution)/shard_map/ppermute | solution.py:330
  41.0 14.5 %collective-permute-start.20 = (bf16[2,584,128]{2,1,0:T(8,128)(2,1)S(1)}, bf16[2,584,128]{2,1,0:T(8,128)(2,1)S(1)}, u32[]{:S(2)}, u32[]{:S(2)}) collective-permute-start(bf16[2,584,128]{2,1,0:T(8,128)(2,1)S(1)} %collective-permute-done.19.m1), channel_id=1, source_target_pairs={{0,14},{2,0},{4,2},{6,4},{8,6},{10,8},{12,10},{14,12},{1,15},{3,1}... | collective-permute-start | bytes 897032 | tf_op jit(solution)/shard_map/ppermute | solution.py:330
  46.5 12.8 %collective-permute-start.5 = (bf16[2,584,128]{2,1,0:T(8,128)(2,1)S(1)}, bf16[2,584,128]{2,1,0:T(8,128)(2,1)}, u32[]{:S(2)}, u32[]{:S(2)}) collective-permute-start(bf16[2,584,128]{2,1,0:T(8,128)(2,1)S(1)} %collective-permute-done.4.m1), channel_id=1, source_target_pairs={{0,14},{2,0},{4,2},{6,4},{8,6},{10,8},{12,10},{14,12},{1,15},{3,1}... | collective-permute-start | bytes 897032 | tf_op jit(solution)/shard_map/ppermute | solution.py:330
  49.9 12.9 %collective-permute-start.3 = (bf16[2,584,128]{2,1,0:T(8,128)(2,1)S(1)}, bf16[2,584,128]{2,1,0:T(8,128)(2,1)S(1)}, u32[]{:S(2)}, u32[]{:S(2)}) collective-permute-start(bf16[2,584,128]{2,1,0:T(8,128)(2,1)S(1)} %collective-permute-done.2.p2), channel_id=1, source_target_pairs={{0,2},{2,4},{4,6},{6,8},{8,10},{10,12},{12,14},{14,0},{1,3},{3,5},... | collective-permute-start | bytes 897032 | tf_op jit(solution)/shard_map/ppermute | solution.py:330
  55.5 12.9 %collective-permute-start.17 = (bf16[2,584,128]{2,1,0:T(8,128)(2,1)S(1)}, bf16[2,584,128]{2,1,0:T(8,128)(2,1)}, u32[]{:S(2)}, u32[]{:S(2)}) collective-permute-start(bf16[2,584,128]{2,1,0:T(8,128)(2,1)S(1)} %collective-permute-done.16.p1), channel_id=1, source_target_pairs={{0,2},{2,4},{4,6},{6,8},{8,10},{10,12},{12,14},{14,0},{1,3},{3,5},... | collective-permute-start | bytes 897032 | tf_op jit(solution)/shard_map/ppermute | solution.py:330
  55.6 12.9 %collective-permute-start.21 = (bf16[2,584,128]{2,1,0:T(8,128)(2,1)S(1)}, bf16[2,584,128]{2,1,0:T(8,128)(2,1)S(1)}, u32[]{:S(2)}, u32[]{:S(2)}) collective-permute-start(bf16[2,584,128]{2,1,0:T(8,128)(2,1)S(1)} %collective-permute-done.20.m2), channel_id=1, source_target_pairs={{0,14},{2,0},{4,2},{6,4},{8,6},{10,8},{12,10},{14,12},{1,15},{3,1}... | collective-permute-start | bytes 897032 | tf_op jit(solution)/shard_map/ppermute | solution.py:330
  59.3 19.7 %collective-permute-start.6 = (bf16[2,584,128]{2,1,0:T(8,128)(2,1)}, bf16[2,584,128]{2,1,0:T(8,128)(2,1)S(1)}, u32[]{:S(2)}, u32[]{:S(2)}) collective-permute-start(bf16[2,584,128]{2,1,0:T(8,128)(2,1)} %collective-permute-done.5.m2), channel_id=1, source_target_pairs={{0,14},{2,0},{4,2},{6,4},{8,6},{10,8},{12,10},{14,12},{1,15},{3,1}... | collective-permute-start | bytes 897032 | tf_op jit(solution)/shard_map/ppermute | solution.py:330
  62.8 16.2 %collective-permute-start.7 = (bf16[2,584,128]{2,1,0:T(8,128)(2,1)S(1)}, bf16[2,584,128]{2,1,0:T(8,128)(2,1)S(1)}, u32[]{:S(2)}, u32[]{:S(2)}) collective-permute-start(bf16[2,584,128]{2,1,0:T(8,128)(2,1)S(1)} %collective-permute-done.3.p3), channel_id=1, source_target_pairs={{0,2},{2,4},{4,6},{6,8},{8,10},{10,12},{12,14},{14,0},{1,3},{3,5},... | collective-permute-start | bytes 897032 | tf_op jit(solution)/shard_map/ppermute | solution.py:330
  68.5 27.0 %collective-permute-start.18 = (bf16[2,584,128]{2,1,0:T(8,128)(2,1)}, bf16[2,584,128]{2,1,0:T(8,128)(2,1)S(1)}, u32[]{:S(2)}, u32[]{:S(2)}) collective-permute-start(bf16[2,584,128]{2,1,0:T(8,128)(2,1)} %collective-permute-done.17.p2), channel_id=1, source_target_pairs={{0,2},{2,4},{4,6},{6,8},{8,10},{10,12},{12,14},{14,0},{1,3},{3,5},... | collective-permute-start | bytes 897032 | tf_op jit(solution)/shard_map/ppermute | solution.py:330
  68.5 27.0 %collective-permute-start.22 = (bf16[2,584,128]{2,1,0:T(8,128)(2,1)S(1)}, bf16[2,584,128]{2,1,0:T(8,128)(2,1)S(1)}, u32[]{:S(2)}, u32[]{:S(2)}) collective-permute-start(bf16[2,584,128]{2,1,0:T(8,128)(2,1)S(1)} %collective-permute-done.21.m3), channel_id=1, source_target_pairs={{0,14},{2,0},{4,2},{6,4},{8,6},{10,8},{12,10},{14,12},{1,15},{3,1}... | collective-permute-start | bytes 897032 | tf_op jit(solution)/shard_map/ppermute | solution.py:330
  85.9 19.2 %collective-permute-start.9 = (bf16[2,576,128]{2,1,0:T(8,128)(2,1)S(1)}, bf16[2,576,128]{2,1,0:T(8,128)(2,1)S(1)}, u32[]{:S(2)}, u32[]{:S(2)}) collective-permute-start(bf16[2,576,128]{2,1,0:T(8,128)(2,1)S(1)} %get-tuple-element.36), channel_id=1, source_target_pairs={{0,2},{2,4},{4,6},{6,8},{8,10},{10,12},{12,14},{14,0},{1,3},{3,5},... | collective-permute-start | bytes 884744 | tf_op jit(solution)/shard_map/ppermute | solution.py:330
  86.0 19.3 %collective-permute-start.13 = (bf16[2,576,128]{2,1,0:T(8,128)(2,1)S(1)}, bf16[2,576,128]{2,1,0:T(8,128)(2,1)S(1)}, u32[]{:S(2)}, u32[]{:S(2)}) collective-permute-start(bf16[2,576,128]{2,1,0:T(8,128)(2,1)S(1)} %get-tuple-element.39), channel_id=1, source_target_pairs={{0,14},{2,0},{4,2},{6,4},{8,6},{10,8},{12,10},{14,12},{1,15},{3,1}... | collective-permute-start | bytes 884744 | tf_op jit(solution)/shard_map/ppermute | solution.py:330
  102.4 6.9 %collective-permute-start.23 = (bf16[2,576,128]{2,1,0:T(8,128)(2,1)S(1)}, bf16[2,576,128]{2,1,0:T(8,128)(2,1)S(1)}, u32[]{:S(2)}, u32[]{:S(2)}) collective-permute-start(bf16[2,576,128]{2,1,0:T(8,128)(2,1)S(1)} %get-tuple-element.45), channel_id=1, source_target_pairs={{0,2},{2,4},{4,6},{6,8},{8,10},{10,12},{12,14},{14,0},{1,3},{3,5},... | collective-permute-start | bytes 884744 | tf_op jit(solution)/shard_map/ppermute | solution.py:330
  102.5 6.9 %collective-permute-start.26 = (bf16[2,576,128]{2,1,0:T(8,128)(2,1)S(1)}, bf16[2,576,128]{2,1,0:T(8,128)(2,1)S(1)}, u32[]{:S(2)}, u32[]{:S(2)}) collective-permute-start(bf16[2,576,128]{2,1,0:T(8,128)(2,1)S(1)} %get-tuple-element.49), channel_id=1, source_target_pairs={{0,14},{2,0},{4,2},{6,4},{8,6},{10,8},{12,10},{14,12},{1,15},{3,1}... | collective-permute-start | bytes 884744 | tf_op jit(solution)/shard_map/ppermute | solution.py:330
  105.2 7.2 %collective-permute-start.10 = (bf16[2,576,128]{2,1,0:T(8,128)(2,1)S(1)}, bf16[2,576,128]{2,1,0:T(8,128)(2,1)S(1)}, u32[]{:S(2)}, u32[]{:S(2)}) collective-permute-start(bf16[2,576,128]{2,1,0:T(8,128)(2,1)S(1)} %add_convert_fusion.11), channel_id=1, source_target_pairs={{0,2},{2,4},{4,6},{6,8},{8,10},{10,12},{12,14},{14,0},{1,3},{3,5},... | collective-permute-start | bytes 884744 | tf_op jit(solution)/shard_map/ppermute | solution.py:330
  105.4 7.2 %collective-permute-start.14 = (bf16[2,576,128]{2,1,0:T(8,128)(2,1)S(1)}, bf16[2,576,128]{2,1,0:T(8,128)(2,1)S(1)}, u32[]{:S(2)}, u32[]{:S(2)}) collective-permute-start(bf16[2,576,128]{2,1,0:T(8,128)(2,1)S(1)} %add_convert_fusion.8), channel_id=1, source_target_pairs={{0,14},{2,0},{4,2},{6,4},{8,6},{10,8},{12,10},{14,12},{1,15},{3,1}... | collective-permute-start | bytes 884744 | tf_op jit(solution)/shard_map/ppermute | solution.py:330
  109.3 16.8 %collective-permute-start.24 = (bf16[2,576,128]{2,1,0:T(8,128)(2,1)S(1)}, bf16[2,576,128]{2,1,0:T(8,128)(2,1)S(1)}, u32[]{:S(2)}, u32[]{:S(2)}) collective-permute-start(bf16[2,576,128]{2,1,0:T(8,128)(2,1)S(1)} %add_convert_fusion.5), channel_id=1, source_target_pairs={{0,2},{2,4},{4,6},{6,8},{8,10},{10,12},{12,14},{14,0},{1,3},{3,5},... | collective-permute-start | bytes 884744 | tf_op jit(solution)/shard_map/ppermute | solution.py:330
  109.5 9.6 %collective-permute-start.27 = (bf16[2,576,128]{2,1,0:T(8,128)(2,1)S(1)}, bf16[2,576,128]{2,1,0:T(8,128)(2,1)S(1)}, u32[]{:S(2)}, u32[]{:S(2)}) collective-permute-start(bf16[2,576,128]{2,1,0:T(8,128)(2,1)S(1)} %add_convert_fusion.3), channel_id=1, source_target_pairs={{0,14},{2,0},{4,2},{6,4},{8,6},{10,8},{12,10},{14,12},{1,15},{3,1}... | collective-permute-start | bytes 884744 | tf_op jit(solution)/shard_map/ppermute | solution.py:330
  112.5 13.5 %collective-permute-start.11 = (bf16[2,576,128]{2,1,0:T(8,128)(2,1)S(1)}, bf16[2,576,128]{2,1,0:T(8,128)(2,1)S(1)}, u32[]{:S(2)}, u32[]{:S(2)}) collective-permute-start(bf16[2,576,128]{2,1,0:T(8,128)(2,1)S(1)} %add_convert_fusion.10), channel_id=1, source_target_pairs={{0,2},{2,4},{4,6},{6,8},{8,10},{10,12},{12,14},{14,0},{1,3},{3,5},... | collective-permute-start | bytes 884744 | tf_op jit(solution)/shard_map/ppermute | solution.py:330
  112.7 22.6 %collective-permute-start.15 = (bf16[2,576,128]{2,1,0:T(8,128)(2,1)S(1)}, bf16[2,576,128]{2,1,0:T(8,128)(2,1)S(1)}, u32[]{:S(2)}, u32[]{:S(2)}) collective-permute-start(bf16[2,576,128]{2,1,0:T(8,128)(2,1)S(1)} %add_convert_fusion.7), channel_id=1, source_target_pairs={{0,14},{2,0},{4,2},{6,4},{8,6},{10,8},{12,10},{14,12},{1,15},{3,1}... | collective-permute-start | bytes 884744 | tf_op jit(solution)/shard_map/ppermute | solution.py:330
  119.2 12.6 %collective-permute-start.28 = (bf16[2,576,128]{2,1,0:T(8,128)(2,1)S(1)}, bf16[2,576,128]{2,1,0:T(8,128)(2,1)S(1)}, u32[]{:S(2)}, u32[]{:S(2)}) collective-permute-start(bf16[2,576,128]{2,1,0:T(8,128)(2,1)S(1)} %add_convert_fusion.2), channel_id=1, source_target_pairs={{0,14},{2,0},{4,2},{6,4},{8,6},{10,8},{12,10},{14,12},{1,15},{3,1}... | collective-permute-start | bytes 884744 | tf_op jit(solution)/shard_map/ppermute | solution.py:330
  126.1 9.7 %collective-permute-start.12 = (bf16[2,576,128]{2,1,0:T(8,128)(2,1)S(1)}, bf16[2,576,128]{2,1,0:T(8,128)(2,1)S(1)}, u32[]{:S(2)}, u32[]{:S(2)}) collective-permute-start(bf16[2,576,128]{2,1,0:T(8,128)(2,1)S(1)} %add_convert_fusion.9), channel_id=1, source_target_pairs={{0,2},{2,4},{4,6},{6,8},{8,10},{10,12},{12,14},{14,0},{1,3},{3,5},... | collective-permute-start | bytes 884744 | tf_op jit(solution)/shard_map/ppermute | solution.py:330
  126.2 12.7 %collective-permute-start.25 = (bf16[2,576,128]{2,1,0:T(8,128)(2,1)S(1)}, bf16[2,576,128]{2,1,0:T(8,128)(2,1)S(1)}, u32[]{:S(2)}, u32[]{:S(2)}) collective-permute-start(bf16[2,576,128]{2,1,0:T(8,128)(2,1)S(1)} %add_convert_fusion.4), channel_id=1, source_target_pairs={{0,2},{2,4},{4,6},{6,8},{8,10},{10,12},{12,14},{14,0},{1,3},{3,5},... | collective-permute-start | bytes 884744 | tf_op jit(solution)/shard_map/ppermute | solution.py:330
  131.8 10.3 %collective-permute-start.29 = (bf16[2,576,128]{2,1,0:T(8,128)(2,1)S(1)}, bf16[2,576,128]{2,1,0:T(8,128)(2,1)S(1)}, u32[]{:S(2)}, u32[]{:S(2)}) collective-permute-start(bf16[2,576,128]{2,1,0:T(8,128)(2,1)S(1)} %add_convert_fusion.1), channel_id=1, source_target_pairs={{0,14},{2,0},{4,2},{6,4},{8,6},{10,8},{12,10},{14,12},{1,15},{3,1}... | collective-permute-start | bytes 884744 | tf_op jit(solution)/shard_map/ppermute | solution.py:330
  143.1 23.7 %all-to-all-start.1 = ((bf16[32,72,128]{2,1,0:T(8,128)(2,1)}), bf16[32,72,128]{2,1,0:T(8,128)(2,1)S(1)}, u32[]{:S(2)}, u32[]{:S(2)}) async-start(bf16[32,72,128]{2,1,0:T(8,128)(2,1)} %bitcast.13), calls=%async_computation.1 | async-start | bytes 1179648 | tf_op jit(solution)/shard_map/all_to_all | solution.py:408
  (5 other events, 80.2 us)
